TPU v7x, 32 devices: a whole 2x2x4 slice. The times are simulated.
32 devices in a mesh: fs: 16 (over z, y, core), tp: 2 (over x).
Axes of the slice: x: 2, y: 2, z: 4, core: 2. Of those that a mesh axis runs over, the one named last changes fastest.
Arguments:
- tokens: bfloat16 [16384, 2048], P(('fs', 'tp')), may hold values from -8 to 8
- pre_mix_gain: float32 [2048], replicated, may hold values from 0.1 to 1.9
- post_mix_gain: float32 [2048], replicated, may hold values from 0.1 to 1.9
- pre_ffn_gain: float32 [2048], replicated, may hold values from 0.1 to 1.9
- post_ffn_gain: float32 [2048], replicated, may hold values from 0.1 to 1.9
- w_branch: bfloat16 [2048, 1024], P('fs', 'tp'), may hold values from -0.125 to 0.125
- w_gelu: bfloat16 [2048, 1024], P('fs', 'tp'), may hold values from -0.125 to 0.125
- conv_weight: bfloat16 [4, 1024], P(None, 'tp'), may hold values from -3 to 3
- w_rec: bfloat16 [2, 8, 128, 128], P(None, 'tp'), may hold values from -0.5 to 0.5
- w_inp: bfloat16 [2, 8, 128, 128], P(None, 'tp'), may hold values from -0.5 to 0.5
- decay: float32 [2, 1024], P(None, 'tp'), may hold values from 3 to 10
- out_weight_t: bfloat16 [2048, 1024], P('fs', 'tp'), may hold values from -0.1875 to 0.1875
- w_gate: bfloat16 [2048, 3072], P('fs', 'tp'), may hold values from -0.125 to 0.125
- w_up: bfloat16 [2048, 3072], P('fs', 'tp'), may hold values from -0.125 to 0.125
- down_weight_t: bfloat16 [2048, 3072], P('fs', 'tp'), may hold values from -0.109375 to 0.109375
Outputs:
- layer_out: bfloat16 [16384, 2048], P(('fs', 'tp'))
All inputs are finite; a program needn't handle non-finite values.
Results may differ from a plain program's by a relative error of at most 0.014.
Values may be sent and summed in bfloat16 or wider, within the bound.
A program may use at most 128 MiB of HBM per device.

v0:
```python
import functools

import jax
import jax.numpy as jnp
from jax import lax
from jax.experimental import pallas as pl
from jax.experimental.pallas import tpu as pltpu
from jax.sharding import PartitionSpec as P

EPS = 1e-06
SEGMENTS = 8
PIECES = 4
VMEM_BYTES = 60 * 1024 * 1024


def normed(values, gain):
    factor = lax.rsqrt(jnp.mean(values * values, axis=-1, keepdims=True) + EPS)
    return values * factor * gain


def one_minus_exp(y, exp_y):
    series = 1.0 + y * (1.0 / 8.0)
    for order in (7, 6, 5, 4, 3, 2):
        series = 1.0 + y * (1.0 / order) * series
    return jnp.where(y > -0.5, -y * series, 1.0 - exp_y)


def mixer_kernel(
    paired, x_ref, y_ref, wb_ref, wg_ref, conv_ref, gates_ref, coef_ref, out_ref, pad, gel, a0, u0, a1, u1
):
    length, width = out_ref.shape
    group = gates_ref.shape[1]
    rows = 256
    pad[0:8, :] = jnp.zeros((8, width), jnp.float32)
    pad[8 + length : 16 + length, :] = jnp.zeros((8, width), jnp.float32)
    if paired:
        own_start = lax.axis_index("tp") * x_ref.shape[0]
        sources = ((x_ref, own_start), (y_ref, x_ref.shape[0] - own_start))
    else:
        sources = ((x_ref, 0),)
    for source, base in sources:
        for start in range(0, source.shape[0], rows):
            piece = source[start : start + rows, :]
            branch = jnp.dot(piece, wb_ref[...], preferred_element_type=jnp.float32)
            gelu_in = jnp.dot(piece, wg_ref[...], preferred_element_type=jnp.float32)
            at = pl.multiple_of(base + start, rows)
            pad[pl.ds(8 + at, rows), :] = branch.astype(jnp.bfloat16).astype(jnp.float32)
            gel[pl.ds(at, rows), :] = jax.nn.gelu(
                gelu_in.astype(jnp.bfloat16).astype(jnp.float32)
            )

    for part in range(width // group):
        cols = slice(part * group, (part + 1) * group)
        taps = conv_ref[:, cols].astype(jnp.float32)
        coef = coef_ref[:, cols]
        for start in range(0, length, rows):
            summed = taps[0:1] * pad[6 + start : 6 + start + rows, cols]
            for j in range(1, 4):
                summed = summed + taps[j : j + 1] * pad[6 + j + start : 6 + j + start + rows, cols]
            conv = summed.astype(jnp.bfloat16)
            wide = conv.astype(jnp.float32)
            for d, (a_ref, u_ref) in enumerate(((a0, u0), (a1, u1))):
                gate = jnp.dot(
                    conv,
                    gates_ref[part, :, 2 * d * group : 2 * (d + 1) * group],
                    preferred_element_type=jnp.float32,
                )
                rate = jax.nn.sigmoid(gate[:, :group])
                inflow = jax.nn.sigmoid(gate[:, group:])
                log_retain = rate * coef[d : d + 1]
                retain = jnp.exp(log_retain)
                left = one_minus_exp(2.0 * log_retain, retain * retain)
                a_ref[part, start : start + rows, :] = retain
                u_ref[part, start : start + rows, :] = jnp.sqrt(left) * inflow * wide

    steps = length // SEGMENTS

    def step(t, carry):
        out = []
        for (state, decayed), (a_ref, u_ref), at in (
            (carry[0], (a0, u0), t),
            (carry[1], (a1, u1), steps - 1 - t),
        ):
            where = pl.ds(at, SEGMENTS, stride=steps)
            nstate, ndecayed = [], []
            for c in range(n):
                retain = a_ref[c, where, :]
                h = retain * state[c] + u_ref[c, where, :]
                p = retain * decayed[c]
                u_ref[c, where, :] = h
                a_ref[c, where, :] = p
                nstate.append(h)
                ndecayed.append(p)
            out.append((tuple(nstate), tuple(ndecayed)))
        return tuple(out)

    n = width // group
    zero = tuple(jnp.zeros((SEGMENTS, group), jnp.float32) for c in range(n))
    one = tuple(jnp.ones((SEGMENTS, group), jnp.float32) for c in range(n))
    ended = lax.fori_loop(0, steps, step, ((zero, one), (zero, one)), unroll=8)
    for c in range(n):
        lanes = slice(c * group, (c + 1) * group)
        blank = jnp.zeros((1, group), jnp.float32)
        entry = [[None] * SEGMENTS, [None] * SEGMENTS]
        for d, order in ((0, range(SEGMENTS)), (1, range(SEGMENTS - 1, -1, -1))):
            carry = blank
            for s in order:
                entry[d][s] = carry
                carry = ended[d][0][c][s : s + 1] + ended[d][1][c][s : s + 1] * carry
        for s in range(SEGMENTS):
            span = slice(s * steps, (s + 1) * steps)
            forward = u0[c, span, :] + a0[c, span, :] * entry[0][s]
            backward = u1[c, span, :] + a1[c, span, :] * entry[1][s]
            out_ref[span, lanes] = (gel[span, lanes] * (forward + backward)).astype(jnp.bfloat16)


def mixer(paired, x, y, weights, conv_weight, w_rec, w_inp, decay):
    length, model = x.shape
    x_spec = pl.BlockSpec((length, model), lambda j: (0, 0))
    length = 2 * length if paired else length
    channels = conv_weight.shape[1]
    group = w_rec.shape[2]
    width = min(256, channels)
    count = channels // width
    gates = jnp.concatenate([w_rec[0], w_inp[0], w_rec[1], w_inp[1]], axis=-1)
    coef = -8.0 * jax.nn.softplus(-decay)
    f32 = functools.partial(pltpu.VMEM, dtype=jnp.float32)
    return pl.pallas_call(
        functools.partial(mixer_kernel, paired),
        grid=(count,),
        out_shape=jax.ShapeDtypeStruct((length, channels), jnp.bfloat16),
        in_specs=[
            x_spec,
            x_spec if paired else pl.BlockSpec((8, model), lambda j: (0, 0)),
            pl.BlockSpec((model, width), lambda j: (0, j)),
            pl.BlockSpec((model, width), lambda j: (0, count + j)),
            pl.BlockSpec((4, width), lambda j: (0, j)),
            pl.BlockSpec((width // group, group, 4 * group), lambda j: (j, 0, 0)),
            pl.BlockSpec((2, width), lambda j: (0, j)),
        ],
        out_specs=pl.BlockSpec((length, width), lambda j: (0, j)),
        scratch_shapes=[f32((length + 16, width)), f32((length, width))]
        + [f32((width // group, length, group)) for i in range(4)],
        compiler_params=pltpu.CompilerParams(vmem_limit_bytes=VMEM_BYTES),
        cost_estimate=pl.CostEstimate(
            flops=4 * length * model * channels + 16 * length * group * channels * 8,
            bytes_accessed=2 * (length * model + 2 * model * channels + length * channels),
            transcendentals=12 * length * channels,
        ),
    )(x, y, weights, weights, conv_weight, gates, coef)


def ffn_kernel(x_ref, gate_ref, up_ref, down_ref, out_ref, total):
    step = pl.program_id(0)
    gate = jnp.dot(x_ref[...], gate_ref[...], preferred_element_type=jnp.float32)
    up = jnp.dot(x_ref[...], up_ref[...], preferred_element_type=jnp.float32)
    hidden = (jax.nn.silu(gate) * up).astype(jnp.bfloat16)
    partial = lax.dot_general(
        hidden, down_ref[...], (((1,), (1,)), ((), ())), preferred_element_type=jnp.float32
    )

    @pl.when(step == 0)
    def _():
        total[...] = partial

    @pl.when(step > 0)
    def _():
        total[...] += partial

    @pl.when(step == pl.num_programs(0) - 1)
    def _():
        out_ref[...] = total[...].astype(jnp.bfloat16)


def ffn(x, weights):
    rows, model = x.shape
    units = weights.shape[1] // 3
    width = 256 if units % 256 == 0 else 128
    count = units // width
    return pl.pallas_call(
        ffn_kernel,
        grid=(count,),
        out_shape=jax.ShapeDtypeStruct((rows, model), jnp.bfloat16),
        in_specs=[
            pl.BlockSpec((rows, model), lambda j: (0, 0)),
            pl.BlockSpec((model, width), lambda j: (0, j)),
            pl.BlockSpec((model, width), lambda j: (0, count + j)),
            pl.BlockSpec((model, width), lambda j: (0, 2 * count + j)),
        ],
        out_specs=pl.BlockSpec((rows, model), lambda j: (0, 0)),
        scratch_shapes=[pltpu.VMEM((rows, model), jnp.float32)],
        compiler_params=pltpu.CompilerParams(vmem_limit_bytes=VMEM_BYTES),
        cost_estimate=pl.CostEstimate(
            flops=6 * rows * model * units,
            bytes_accessed=2 * (2 * rows * model + 3 * model * units),
            transcendentals=rows * units,
        ),
    )(x, weights, weights, weights)


def ring_chip(place, chips):
    half = chips // 2
    turned = place // half
    row = place * (1 - turned) + (chips - 1 - place) * turned
    return row * 2 + turned


def ring_kernel(
    size, shard_ref, x_ref, out_ref, other_ref, own_sem, send, recv, near_send, near_recv, swap_sem
):
    chips = size // 2
    me = lax.axis_index("fs")
    core = me % 2
    turned = (me // 2) % 2
    row = me // 4
    place = row * (1 - turned) + (chips - 1 - row) * turned
    partner = me + 1 - 2 * core
    after = ring_chip((place + 1) % chips, chips) * 2 + core
    before = ring_chip((place + chips - 1) % chips, chips) * 2 + core
    targets = ({"fs": after}, {"fs": before})
    partner = {"fs": partner}
    column = lax.axis_index("tp")
    across = {"tp": 1 - column}

    barrier = pltpu.get_barrier_semaphore()
    for device in (*targets, partner, across):
        pl.semaphore_signal(
            barrier, inc=1, device_id=device, device_id_type=pl.DeviceIdType.MESH
        )
    pl.semaphore_wait(barrier, 4)

    depth = shard_ref.shape[0]
    piece_rows = depth // (2 * PIECES)

    def remote(src, dst, sent, landed, device):
        copy = pltpu.make_async_remote_copy(
            src_ref=src,
            dst_ref=dst,
            send_sem=sent,
            recv_sem=landed,
            device_id=device,
            device_id_type=pl.DeviceIdType.MESH,
        )
        copy.start()
        return copy

    def rows_of(origin, at):
        start = pl.multiple_of(origin * depth + at * piece_rows, piece_rows)
        return out_ref.at[pl.ds(start, piece_rows), :]

    moving = []
    for at in range(2 * PIECES):
        moving.append(
            remote(
                shard_ref.at[pl.ds(at * piece_rows, piece_rows), :],
                rows_of(me, at),
                send.at[at, 0],
                recv.at[at, 0],
                targets[at % 2],
            )
        )
    waiting = list(moving)
    near = [remote(x_ref, other_ref, swap_sem.at[0], swap_sem.at[1], across)]
    mine = out_ref.at[pl.ds(pl.multiple_of(me * depth, depth), depth), :]
    near.append(remote(shard_ref, mine, near_send.at[0, 0], near_recv.at[0, 0], partner))
    own = pltpu.make_async_copy(shard_ref, mine, own_sem)
    own.start()
    for step in range(chips - 1):
        for at in range(2 * PIECES):
            moving[at].wait_recv()
            back = step + 1 if at % 2 == 0 else chips - 1 - step
            origin = ring_chip((place + chips - back) % chips, chips) * 2 + core
            piece = rows_of(origin, at)
            if step < chips - 2:
                moving[at] = remote(
                    piece,
                    piece,
                    send.at[at, step + 1],
                    recv.at[at, step + 1],
                    targets[at % 2],
                )
                waiting.append(moving[at])
            near.append(
                remote(
                    piece,
                    piece,
                    near_send.at[at, step + 1],
                    near_recv.at[at, step + 1],
                    partner,
                )
            )
    for copy in waiting:
        copy.wait_send()
    for copy in near:
        copy.wait()
    own.wait()


def ring_gather(shard, x, size):
    rows, width = shard.shape
    chips = size // 2
    dma = pltpu.SemaphoreType.DMA
    return pl.pallas_call(
        functools.partial(ring_kernel, size),
        out_shape=(
            jax.ShapeDtypeStruct((rows * size, width), shard.dtype),
            jax.ShapeDtypeStruct(x.shape, x.dtype),
        ),
        in_specs=[
            pl.BlockSpec(memory_space=pltpu.VMEM),
            pl.BlockSpec(memory_space=pl.ANY),
        ],
        out_specs=(pl.BlockSpec(memory_space=pl.ANY), pl.BlockSpec(memory_space=pl.ANY)),
        scratch_shapes=[
            dma,
            dma((2 * PIECES, chips)),
            dma((2 * PIECES, chips)),
            dma((2 * PIECES, chips)),
            dma((2 * PIECES, chips)),
            dma((2,)),
        ],
        compiler_params=pltpu.CompilerParams(collective_id=0, has_side_effects=True),
        cost_estimate=pl.CostEstimate(
            flops=1 << 32, bytes_accessed=2 * rows * size * width, transcendentals=0
        ),
    )(shard, x)


def swap(values):
    return lax.ppermute(values, "tp", [(0, 1), (1, 0)])


def matmul_t(rows, weight_t):
    return lax.dot_general(
        rows, weight_t, (((1,), (1,)), ((), ())), preferred_element_type=jnp.float32
    )


def per_device(
    pair,
    tokens,
    pre_mix_gain,
    post_mix_gain,
    pre_ffn_gain,
    post_ffn_gain,
    w_branch,
    w_gelu,
    conv_weight,
    w_rec,
    w_inp,
    decay,
    out_weight_t,
    w_gate,
    w_up,
    down_weight_t,
):
    own_rows = tokens.shape[0]
    channels = conv_weight.shape[1]
    place = lax.axis_index("tp")
    mix_shard = jnp.concatenate([w_branch, w_gelu, out_weight_t], axis=1)
    ffn_shard = jnp.concatenate([w_gate, w_up, down_weight_t], axis=1)
    stream = tokens.astype(jnp.float32)
    normed_in = normed(stream, pre_mix_gain).astype(jnp.bfloat16)
    if pair:
        fs_size = lax.axis_size("fs")
        mix_all, other = ring_gather(mix_shard, normed_in, fs_size)
        ffn_shard, mix_all, other = lax.optimization_barrier((ffn_shard, mix_all, other))
        sequence = (normed_in, other)
    else:
        mix_all = lax.all_gather(mix_shard, "fs", axis=0, tiled=True)
        whole = lax.all_gather(normed_in, "tp", axis=0, tiled=True)
        sequence = (whole, whole)
    ffn_all = lax.all_gather(ffn_shard, "fs", axis=0, tiled=True)
    out_own = mix_all[:, 2 * channels :]
    if pair:
        core = lax.axis_index("fs") % 2
        span = out_own.shape[0] // 2
        partners = [(i, i + 1 - 2 * (i % 2)) for i in range(fs_size)]
        crossed = swap(lax.dynamic_slice_in_dim(out_own, core * span, span, 0))
    hidden = mixer(pair, *sequence, mix_all, conv_weight, w_rec, w_inp, decay)
    if pair:
        crossed, hidden = lax.optimization_barrier((crossed, hidden))
        shared = lax.ppermute(crossed, "fs", partners)
        out_other = (
            jnp.where(core == 0, crossed, shared),
            jnp.where(core == 0, shared, crossed),
        )
        away = lax.dynamic_slice_in_dim(hidden, (1 - place) * own_rows, own_rows, 0)
        kept = lax.dynamic_slice_in_dim(hidden, place * own_rows, own_rows, 0)
        came = swap(away)
        far = jnp.concatenate(out_other, axis=0)
        mixer_sum = matmul_t(kept, out_own) + matmul_t(came, far)
    else:
        own_hidden = lax.all_to_all(hidden, "tp", split_axis=0, concat_axis=1, tiled=True)
        out_whole = lax.all_gather(out_own, "tp", axis=1, tiled=True)
        mixer_sum = matmul_t(own_hidden, out_whole)
    residual = (stream + normed(mixer_sum, post_mix_gain)).astype(jnp.bfloat16)
    middle = residual.astype(jnp.float32)
    normed_mid = normed(middle, pre_ffn_gain).astype(jnp.bfloat16)
    if pair:
        pieces = 2
        size = own_rows // pieces
        away_rows = [swap(normed_mid[i * size : (i + 1) * size]) for i in range(pieces)]
        back = [swap(ffn(rows, ffn_all)) for rows in away_rows]
        own_part = ffn(normed_mid, ffn_all).astype(jnp.float32)
        ffn_sum = own_part + jnp.concatenate(back, axis=0).astype(jnp.float32)
    else:
        all_mid = lax.all_gather(normed_mid, "tp", axis=0, tiled=True)
        ffn_sum = lax.psum_scatter(
            ffn(all_mid, ffn_all), "tp", scatter_dimension=0, tiled=True
        ).astype(jnp.float32)
    return (middle + normed(ffn_sum, post_ffn_gain)).astype(jnp.bfloat16)


def solution(mesh):
    return jax.shard_map(
        functools.partial(per_device, mesh.shape["tp"] == 2),
        mesh=mesh,
        in_specs=(
            P(("fs", "tp"), None),
            P(),
            P(),
            P(),
            P(),
            P("fs", "tp"),
            P("fs", "tp"),
            P(None, "tp"),
            P(None, "tp", None, None),
            P(None, "tp", None, None),
            P(None, "tp"),
            P("fs", "tp"),
            P("fs", "tp"),
            P("fs", "tp"),
            P("fs", "tp"),
        ),
        out_specs=P(("fs", "tp"), None),
        check_vma=False,
    )
```

profile of v0, /device:TPU:0, one launch (start us, length us, event | category | flops | bytes accessed | tf_op | source)
XLA Modules:
  0.0 241.6 jit_solution(11966726742180400258)
XLA Ops:
  6.5 0.0 copy-start.11
  6.5 0.0 copy-start.10
  6.5 0.0 all-gather.2.cloned.1.call-start
  6.5 2.1 fusion
  8.7 3.5 %fusion.2.x_ref = bf16[512,2048]{1,0:T(8,128)(2,1)} fusion(bf16[512,2048]{1,0:T(8,128)(2,1)} %param.15, f32[2048]{0:T(1024)} %param.16, f32[512]{0:T(512)S(1)} %add_rsqrt_fusion.3), kind=kLoop, calls=%fused_computation.8 | loop fusion | flops 4194304 | bytes 4204544 | tf_op jit(solution)/shard_map/convert_element_type | solution.py:363
  12.1 0.0 copy-done.11
  12.1 0.0 copy-done.10
  12.1 0.0 copy-done.9
  12.1 0.8 pad_maximum_fusion.3.shard_ref
  12.9 53.8 %shard_map.145 = (bf16[2048,1536]{1,0:T(8,128)(2,1)}, bf16[512,2048]{1,0:T(8,128)(2,1)}) custom-call(bf16[128,1536]{1,0:T(8,128)(2,1)} %pad_maximum_fusion.3.shard_ref, bf16[512,2048]{1,0:T(8,128)(2,1)} %fusion.2.x_ref), custom_call_target="tpu_custom_call" | custom-call | flops 4294967296 | bytes 6291456 | tf_op jit(solution)/shard_map/pallas_call | solution.py:303
  66.7 0.0 copy-done.5
  66.7 0.0 copy-done.6
  66.8 0.0 copy-done.7
  66.8 1.1 pad_maximum_fusion.1
  67.9 0.0 all-gather.2.cloned.1.call-update
  67.9 0.0 copy-start.15
  67.9 1.8 slice.21
  69.7 0.1 constant_dynamic-slice_fusion.1
  69.8 0.6 collective-permute-start
  70.4 0.0 copy-done.8
  70.4 1.0 slice_bitcast_fusion.2
  71.4 0.9 pad_maximum_fusion.2.gates_ref
  72.3 0.0 copy-done.15
  72.3 0.6 fusion.13.coef_ref
  72.9 28.5 %shard_map.146 = bf16[1024,512]{1,0:T(8,128)(2,1)} custom-call(bf16[512,2048]{1,0:T(8,128)(2,1)} %fusion.2.x_ref, bf16[512,2048]{1,0:T(8,128)(2,1)} %get-tuple-element.15.y_ref, bf16[2048,1536]{1,0:T(8,128)(2,1)} %get-tuple-element.14.wb_ref.wg_ref, bf16[2048,1536]{1,0:T(8,128)(2,1)} %get-tuple-element.14.wb_ref.wg_ref, bf16[4,512]{1,0:T(4,128)(2,1)} %conv_ref.1, ...), custom_call_target="tpu_custom_call" | custom-call | flops 12884901888 | bytes 9437184 | tf_op jit(solution)/shard_map/pallas_call | solution.py:128
  101.4 0.0 collective-permute-done
  101.4 0.1 collective-permute-start.2
  101.5 1.1 constant_dynamic-slice_fusion
  102.6 1.5 collective-permute-start.1
  104.1 0.4 collective-permute-done.2
  104.6 0.1 broadcast_select_fusion.1
  104.7 0.0 copy-start.4
  104.7 12.3 %collective-permute-done.1 = bf16[512,512]{1,0:T(8,128)(2,1)S(1)} collective-permute-done((bf16[512,512]{1,0:T(8,128)(2,1)S(1)}, bf16[512,512]{1,0:T(8,128)(2,1)S(1)}, u32[]{:S(2)}, u32[]{:S(2)}) %collective-permute-start.1) | collective-permute-done | bytes 524320 | tf_op jit(solution)/shard_map/ppermute | solution.py:330
  117.0 1.3 fusion.8
  118.3 0.0 copy-done.4
  118.3 0.0 copy-start
  118.3 0.0 copy-start.12
  118.3 3.3 %multiply_reduce_fusion.1 = (f32[512]{0:T(512)S(1)}, f32[512,2048]{1,0:T(8,128)S(1)}) fusion(f32[512,2048]{1,0:T(8,128)S(1)} %fusion.8, bf16[2048,1536]{1,0:T(8,128)(2,1)} %get-tuple-element.14.wb_ref.wg_ref, bf16[1024,512]{1,0:T(8,128)(2,1)S(1)} %copy-done.4, s32[]{:T(128)S(6)} %select_n.35), kind=kOutput, calls=%fused_computation.16 | convolution fusion | flops 1076887040 | bytes 11012100 | tf_op jit(solution)/shard_map/dot_general | solution.py:334
  121.6 0.0 copy-done
  121.7 0.0 copy-done.12
  121.7 0.0 copy-start.13
  121.7 1.0 fusion.4
  122.7 0.0 copy-done.13
  122.7 0.5 fusion.6.x_ref
  123.3 0.0 copy-start.1
  123.3 1.3 copy-done.1
  124.6 1.2 fusion.18
  125.8 1.5 collective-permute-start.3
  127.3 0.5 collective-permute-start.5
  127.8 24.0 %collective-permute-done.3.x_ref = bf16[256,2048]{1,0:T(8,128)(2,1)S(1)} collective-permute-done((bf16[256,2048]{1,0:T(8,128)(2,1)S(1)}, bf16[256,2048]{1,0:T(8,128)(2,1)S(1)}, u32[]{:S(2)}, u32[]{:S(2)}) %collective-permute-start.3) | collective-permute-done | bytes 1048608 | tf_op jit(solution)/shard_map/ppermute | solution.py:330
  151.8 15.3 %all-gather.2.cloned.1.call-done.gate_ref.up_ref.down_ref = bf16[2048,4608]{1,0:T(8,128)(2,1)} async-done(((bf16[128,4608]{1,0:T(8,128)(2,1)}), bf16[2048,4608]{1,0:T(8,128)(2,1)}) %all-gather.2.cloned.1.call-update) | async-done | bytes 18874384 | tf_op jit(solution)/shard_map/all_gather | solution.py:373
  167.2 0.0 copy-done.3
  167.2 12.7 %shard_map.148 = bf16[256,2048]{1,0:T(8,128)(2,1)} custom-call(bf16[256,2048]{1,0:T(8,128)(2,1)} %copy-done.3, bf16[2048,4608]{1,0:T(8,128)(2,1)} %all-gather.2.cloned.1.call-done.gate_ref.up_ref.down_ref, bf16[2048,4608]{1,0:T(8,128)(2,1)} %all-gather.2.cloned.1.call-done.gate_ref.up_ref.down_ref, ...), custom_call_target="tpu_custom_call" | custom-call | flops 4831838208 | bytes 20971520 | tf_op jit(solution)/shard_map/pallas_call | solution.py:180
  179.9 1.5 collective-permute-start.4
  181.3 0.0 collective-permute-done.5.x_ref
  181.3 12.7 %shard_map.149 = bf16[256,2048]{1,0:T(8,128)(2,1)} custom-call(bf16[256,2048]{1,0:T(8,128)(2,1)} %collective-permute-done.5.x_ref, bf16[2048,4608]{1,0:T(8,128)(2,1)} %all-gather.2.cloned.1.call-done.gate_ref.up_ref.down_ref, bf16[2048,4608]{1,0:T(8,128)(2,1)} %all-gather.2.cloned.1.call-done.gate_ref.up_ref.down_ref, ...), custom_call_target="tpu_custom_call" | custom-call | flops 4831838208 | bytes 20971520 | tf_op jit(solution)/shard_map/pallas_call | solution.py:180
  194.1 0.6 collective-permute-start.6
  194.6 17.7 %shard_map.147 = bf16[512,2048]{1,0:T(8,128)(2,1)} custom-call(bf16[512,2048]{1,0:T(8,128)(2,1)} %copy-done.1, bf16[2048,4608]{1,0:T(8,128)(2,1)} %all-gather.2.cloned.1.call-done.gate_ref.up_ref.down_ref, bf16[2048,4608]{1,0:T(8,128)(2,1)} %all-gather.2.cloned.1.call-done.gate_ref.up_ref.down_ref, ...), custom_call_target="tpu_custom_call" | custom-call | flops 9663676416 | bytes 23068672 | tf_op jit(solution)/shard_map/pallas_call | solution.py:180
  212.3 0.0 collective-permute-done.4
  212.3 15.6 %collective-permute-done.6 = bf16[256,2048]{1,0:T(8,128)(2,1)} collective-permute-done((bf16[256,2048]{1,0:T(8,128)(2,1)}, bf16[256,2048]{1,0:T(8,128)(2,1)}, u32[]{:S(2)}, u32[]{:S(2)}) %collective-permute-start.6) | collective-permute-done | bytes 1048608 | tf_op jit(solution)/shard_map/ppermute | solution.py:330
  228.0 2.6 %multiply_reduce_fusion = f32[512]{0:T(512)S(1)} fusion(bf16[512,2048]{1,0:T(8,128)(2,1)} %shard_map.147, bf16[256,2048]{1,0:T(8,128)(2,1)} %collective-permute-done.6, bf16[256,2048]{1,0:T(8,128)(2,1)S(1)} %collective-permute-done.4), kind=kLoop, calls=%fused_computation.14 | loop fusion | flops 8388096 | bytes 4196352 | tf_op jit(solution)/shard_map/reduce_sum | solution.py:17
  230.6 0.0 copy-done.2
  230.6 0.0 copy-done.14
  230.6 4.2 %fusion.7 = bf16[512,2048]{1,0:T(8,128)(2,1)} fusion(bf16[512,2048]{1,0:T(8,128)(2,1)S(1)} %get-tuple-element.20, bf16[512,2048]{1,0:T(8,128)(2,1)S(1)} %copy-done.2, f32[2048]{0:T(1024)S(1)} %copy-done.14, f32[512]{0:T(512)S(1)} %add_rsqrt_fusion, bf16[256,2048]{1,0:T(8,128)(2,1)} %collective-permute-done.6, bf16[256,2048]{1,0:T(8,128)(2,1)S(1)} %collective-permute-done.4), kind=kLoop, calls=%fused_computation.13 | loop fusion | flops 11534336 | bytes 8398848 | tf_op jit(solution)/shard_map/convert_element_type | solution.py:412
  (12 shorter events, 0.0 us)
Async XLA Ops:
  6.5 5.6 %copy-start.11 = (bf16[128,512]{1,0:T(8,128)(2,1)S(1)}, bf16[128,512]{1,0:T(8,128)(2,1)}, u32[]{:S(2)}) copy-start(bf16[128,512]{1,0:T(8,128)(2,1)} %param.20) | copy-start | bytes 393220
  6.5 5.6 %copy-start.10 = (bf16[128,512]{1,0:T(8,128)(2,1)S(1)}, bf16[128,512]{1,0:T(8,128)(2,1)}, u32[]{:S(2)}) copy-start(bf16[128,512]{1,0:T(8,128)(2,1)} %param.21) | copy-start | bytes 393220
  6.5 5.6 %copy-start.9 = (bf16[128,512]{1,0:T(8,128)(2,1)S(1)}, bf16[128,512]{1,0:T(8,128)(2,1)}, u32[]{:S(2)}) copy-start(bf16[128,512]{1,0:T(8,128)(2,1)} %param.26) | copy-start | bytes 393220
  6.5 160.6 %all-gather.2.cloned.1.call-start = ((), (), s32[]{:S(2)}) async-start(), calls=%async_computation | async-start | bytes 20054016 | tf_op jit(solution)/shard_map/all_gather | solution.py:373
  12.9 53.8 %copy-start.5 = (bf16[128,1536]{1,0:T(8,128)(2,1)S(1)}, bf16[128,1536]{1,0:T(8,128)(2,1)}, u32[]{:S(2)}) copy-start(bf16[128,1536]{1,0:T(8,128)(2,1)} %param.29) | copy-start | bytes 1179652
  12.9 53.8 %copy-start.6 = (bf16[128,1536]{1,0:T(8,128)(2,1)S(1)}, bf16[128,1536]{1,0:T(8,128)(2,1)}, u32[]{:S(2)}) copy-start(bf16[128,1536]{1,0:T(8,128)(2,1)} %param.28) | copy-start | bytes 1179652
  12.9 53.8 %copy-start.7 = (bf16[128,1536]{1,0:T(8,128)(2,1)S(1)}, bf16[128,1536]{1,0:T(8,128)(2,1)}, u32[]{:S(2)}) copy-start(bf16[128,1536]{1,0:T(8,128)(2,1)} %param.27) | copy-start | bytes 1179652
  67.9 2.5 %copy-start.8 = (bf16[2,4,128,128]{3,2,1,0:T(8,128)(2,1)S(1)}, bf16[2,4,128,128]{3,2,1,0:T(8,128)(2,1)}, u32[]{:S(2)}) copy-start(bf16[2,4,128,128]{3,2,1,0:T(8,128)(2,1)} %param.24) | copy-start | bytes 786436
  67.9 4.4 %copy-start.15 = (f32[2,512]{1,0:T(2,128)S(1)}, f32[2,512]{1,0:T(2,128)}, u32[]{:S(2)}) copy-start(f32[2,512]{1,0:T(2,128)} %param.25) | copy-start | bytes 12292
  69.8 31.7 %collective-permute-start = (bf16[1024,512]{1,0:T(8,128)(2,1)S(1)}, bf16[1024,512]{1,0:T(8,128)(2,1)S(1)}, u32[]{:S(2)}, u32[]{:S(2)}) collective-permute-start(bf16[1024,512]{1,0:T(8,128)(2,1)S(1)} %constant_dynamic-slice_fusion.1), channel_id=1, source_target_pairs={{0,1},{1,0},{2,3},{3,2},{4,5},{5,4},{6,7},{7,6},{8,9},{9,8},{10,11... | collective-permute-start | bytes 3145736 | tf_op jit(solution)/shard_map/ppermute | solution.py:330
  101.4 3.1 %collective-permute-start.2 = (bf16[1024,512]{1,0:T(8,128)(2,1)S(1)}, bf16[1024,512]{1,0:T(8,128)(2,1)S(1)}, u32[]{:S(2)}, u32[]{:S(2)}) collective-permute-start(bf16[1024,512]{1,0:T(8,128)(2,1)S(1)} %collective-permute-done), channel_id=1, source_target_pairs={{0,2},{2,0},{4,6},{6,4},{8,10},{10,8},{12,14},{14,12},{16,18},{18,... | collective-permute-start | bytes 3145736 | tf_op jit(solution)/shard_map/ppermute | solution.py:383
  102.6 14.4 %collective-permute-start.1 = (bf16[512,512]{1,0:T(8,128)(2,1)S(1)}, bf16[512,512]{1,0:T(8,128)(2,1)S(1)}, u32[]{:S(2)}, u32[]{:S(2)}) collective-permute-start(bf16[512,512]{1,0:T(8,128)(2,1)S(1)} %constant_dynamic-slice_fusion), channel_id=1, source_target_pairs={{0,1},{1,0},{2,3},{3,2},{4,5},{5,4},{6,7},{7,6},{8,9},{9,8},{10,11... | collective-permute-start | bytes 1572872 | tf_op jit(solution)/shard_map/ppermute | solution.py:330
  104.7 13.6 %copy-start.4 = (bf16[1024,512]{1,0:T(8,128)(2,1)S(1)}, bf16[1024,512]{1,0:T(8,128)(2,1)}, u32[]{:S(2)}) copy-start(bf16[1024,512]{1,0:T(8,128)(2,1)} %shard_map.146) | copy-start | bytes 3145732
  118.3 3.3 %copy-start = (bf16[512,2048]{1,0:T(8,128)(2,1)S(1)}, bf16[512,2048]{1,0:T(8,128)(2,1)}, u32[]{:S(2)}) copy-start(bf16[512,2048]{1,0:T(8,128)(2,1)} %param.15) | copy-start | bytes 6291460
  118.3 3.3 %copy-start.12 = (f32[2048]{0:T(1024)S(1)}, f32[2048]{0:T(1024)}, u32[]{:S(2)}) copy-start(f32[2048]{0:T(1024)} %param.17) | copy-start | bytes 24580
  121.7 1.1 copy-start.13
  123.3 1.3 copy-start.1
  125.8 26.0 %collective-permute-start.3 = (bf16[256,2048]{1,0:T(8,128)(2,1)S(1)}, bf16[256,2048]{1,0:T(8,128)(2,1)S(1)}, u32[]{:S(2)}, u32[]{:S(2)}) collective-permute-start(bf16[256,2048]{1,0:T(8,128)(2,1)S(1)} %get-tuple-element.21), channel_id=1, source_target_pairs={{0,1},{1,0},{2,3},{3,2},{4,5},{5,4},{6,7},{7,6},{8,9},{9,8},{10,11... | collective-permute-start | bytes 3145736 | tf_op jit(solution)/shard_map/ppermute | solution.py:330
  127.3 54.1 %collective-permute-start.5 = (bf16[256,2048]{1,0:T(8,128)(2,1)}, bf16[256,2048]{1,0:T(8,128)(2,1)}, u32[]{:S(2)}, u32[]{:S(2)}) collective-permute-start(bf16[256,2048]{1,0:T(8,128)(2,1)} %get-tuple-element.22), channel_id=1, source_target_pairs={{0,1},{1,0},{2,3},{3,2},{4,5},{5,4},{6,7},{7,6},{8,9},{9,8},{10,11... | collective-permute-start | bytes 3145736 | tf_op jit(solution)/shard_map/ppermute | solution.py:330
  151.8 15.3 %copy-start.3 = (bf16[256,2048]{1,0:T(8,128)(2,1)}, bf16[256,2048]{1,0:T(8,128)(2,1)S(1)}, u32[]{:S(2)}) copy-start(bf16[256,2048]{1,0:T(8,128)(2,1)S(1)} %collective-permute-done.3.x_ref) | copy-start | bytes 3145732
  179.9 32.5 %collective-permute-start.4 = (bf16[256,2048]{1,0:T(8,128)(2,1)}, bf16[256,2048]{1,0:T(8,128)(2,1)S(1)}, u32[]{:S(2)}, u32[]{:S(2)}) collective-permute-start(bf16[256,2048]{1,0:T(8,128)(2,1)} %shard_map.148), channel_id=1, source_target_pairs={{0,1},{1,0},{2,3},{3,2},{4,5},{5,4},{6,7},{7,6},{8,9},{9,8},{10,11... | collective-permute-start | bytes 3145736 | tf_op jit(solution)/shard_map/ppermute | solution.py:330
  194.1 33.9 %collective-permute-start.6 = (bf16[256,2048]{1,0:T(8,128)(2,1)}, bf16[256,2048]{1,0:T(8,128)(2,1)}, u32[]{:S(2)}, u32[]{:S(2)}) collective-permute-start(bf16[256,2048]{1,0:T(8,128)(2,1)} %shard_map.149), channel_id=1, source_target_pairs={{0,1},{1,0},{2,3},{3,2},{4,5},{5,4},{6,7},{7,6},{8,9},{9,8},{10,11... | collective-permute-start | bytes 3145736 | tf_op jit(solution)/shard_map/ppermute | solution.py:330
  212.3 18.3 %copy-start.2 = (bf16[512,2048]{1,0:T(8,128)(2,1)S(1)}, bf16[512,2048]{1,0:T(8,128)(2,1)}, u32[]{:S(2)}) copy-start(bf16[512,2048]{1,0:T(8,128)(2,1)} %shard_map.147) | copy-start | bytes 6291460
  212.3 18.3 %copy-start.14 = (f32[2048]{0:T(1024)S(1)}, f32[2048]{0:T(1024)}, u32[]{:S(2)}) copy-start(f32[2048]{0:T(1024)} %param.19) | copy-start | bytes 24580
Sparse Core Ops, SparseCore 0:
  68.0 99.0 all-gather.1
where the time goes:
time: 242 us
  Pallas kernels  125 us (52%)
  waiting for transfers between devices  67.7 us (28%)
  other arithmetic  17.5 us (7%)
  between operations  13.6 us (6%)
  local copies, waits for them, and re-layouts  6.49 us (3%)
  starting transfers between devices  6.26 us (3%)
  matrix products  4.58 us (2%)
    pallas_call x1, Pallas kernels, ring_gather(): pl.pallas_call(functools.partial(ring_kernel, size), out_shape=(jax.Shape...  53.8 us
    ppermute x6, waiting for transfers between devices, swap(): return lax.ppermute(values, 'tp', [(0, 1), (1, 0)])  51.9 us
    pallas_call x3, Pallas kernels, ffn(): pl.pallas_call(ffn_kernel, grid=(count,), out_shape=jax.ShapeDtypeStruct(...  43.1 us
    pallas_call x1, Pallas kernels, mixer(): pl.pallas_call(functools.partial(mixer_kernel, paired), grid=(count,), ou...  28.5 us
    all_gather x1, waiting for transfers between devices, per_device(): ffn_all = lax.all_gather(ffn_shard, 'fs', axis=0, tiled=True)  15.3 us
    ppermute x6, starting transfers between devices, swap(): return lax.ppermute(values, 'tp', [(0, 1), (1, 0)])  6.19 us
    reduce_sum x3, other arithmetic, normed(): factor = lax.rsqrt(jnp.mean(values * values, axis=-1, keepdims=True) + EPS)  5.76 us
  transfers between devices with their start and end apart: 8, of which 5 were waited for; matrix products, arithmetic and copies ran while one was open for 5% of the time, Pallas kernels for 30%

commit v1 on v0

v1 whole, which is shorter than its diff:
```python
import functools

import jax
import jax.numpy as jnp
from jax import lax
from jax.experimental import pallas as pl
from jax.experimental.pallas import tpu as pltpu
from jax.sharding import PartitionSpec as P

EPS = 1e-06
SEGMENTS = 8
DOWN_PIECES = 2
VMEM_BYTES = 60 * 1024 * 1024


def normed(values, gain):
    factor = lax.rsqrt(jnp.mean(values * values, axis=-1, keepdims=True) + EPS)
    return values * factor * gain


def one_minus_exp(y, exp_y):
    series = 1.0 + y * (1.0 / 8.0)
    for order in (7, 6, 5, 4, 3, 2):
        series = 1.0 + y * (1.0 / order) * series
    return jnp.where(y > -0.5, -y * series, 1.0 - exp_y)


def mixer_kernel(
    x_ref, wb_ref, wg_ref, conv_ref, gates_ref, coef_ref, out_ref, pad, gel, a0, u0, a1, u1
):
    length, width = out_ref.shape
    group = gates_ref.shape[1]
    rows = 256
    pad[0:8, :] = jnp.zeros((8, width), jnp.float32)
    pad[8 + length : 16 + length, :] = jnp.zeros((8, width), jnp.float32)
    sources = ((x_ref, 0),)
    for source, base in sources:
        for start in range(0, source.shape[0], rows):
            piece = source[start : start + rows, :]
            branch = jnp.dot(piece, wb_ref[...], preferred_element_type=jnp.float32)
            gelu_in = jnp.dot(piece, wg_ref[...], preferred_element_type=jnp.float32)
            at = pl.multiple_of(base + start, rows)
            pad[pl.ds(8 + at, rows), :] = branch.astype(jnp.bfloat16).astype(jnp.float32)
            gel[pl.ds(at, rows), :] = jax.nn.gelu(
                gelu_in.astype(jnp.bfloat16).astype(jnp.float32)
            )

    for part in range(width // group):
        cols = slice(part * group, (part + 1) * group)
        taps = conv_ref[:, cols].astype(jnp.float32)
        coef = coef_ref[:, cols]
        for start in range(0, length, rows):
            summed = taps[0:1] * pad[6 + start : 6 + start + rows, cols]
            for j in range(1, 4):
                summed = summed + taps[j : j + 1] * pad[6 + j + start : 6 + j + start + rows, cols]
            conv = summed.astype(jnp.bfloat16)
            wide = conv.astype(jnp.float32)
            for d, (a_ref, u_ref) in enumerate(((a0, u0), (a1, u1))):
                gate = jnp.dot(
                    conv,
                    gates_ref[part, :, 2 * d * group : 2 * (d + 1) * group],
                    preferred_element_type=jnp.float32,
                )
                rate = jax.nn.sigmoid(gate[:, :group])
                inflow = jax.nn.sigmoid(gate[:, group:])
                log_retain = rate * coef[d : d + 1]
                retain = jnp.exp(log_retain)
                left = one_minus_exp(2.0 * log_retain, retain * retain)
                a_ref[part, start : start + rows, :] = retain
                u_ref[part, start : start + rows, :] = jnp.sqrt(left) * inflow * wide

    steps = length // SEGMENTS

    def step(t, carry):
        out = []
        for (state, decayed), (a_ref, u_ref), at in (
            (carry[0], (a0, u0), t),
            (carry[1], (a1, u1), steps - 1 - t),
        ):
            where = pl.ds(at, SEGMENTS, stride=steps)
            nstate, ndecayed = [], []
            for c in range(n):
                retain = a_ref[c, where, :]
                h = retain * state[c] + u_ref[c, where, :]
                p = retain * decayed[c]
                u_ref[c, where, :] = h
                a_ref[c, where, :] = p
                nstate.append(h)
                ndecayed.append(p)
            out.append((tuple(nstate), tuple(ndecayed)))
        return tuple(out)

    n = width // group
    zero = tuple(jnp.zeros((SEGMENTS, group), jnp.float32) for c in range(n))
    one = tuple(jnp.ones((SEGMENTS, group), jnp.float32) for c in range(n))
    ended = lax.fori_loop(0, steps, step, ((zero, one), (zero, one)), unroll=8)
    for c in range(n):
        lanes = slice(c * group, (c + 1) * group)
        blank = jnp.zeros((1, group), jnp.float32)
        entry = [[None] * SEGMENTS, [None] * SEGMENTS]
        for d, order in ((0, range(SEGMENTS)), (1, range(SEGMENTS - 1, -1, -1))):
            carry = blank
            for s in order:
                entry[d][s] = carry
                carry = ended[d][0][c][s : s + 1] + ended[d][1][c][s : s + 1] * carry
        for s in range(SEGMENTS):
            span = slice(s * steps, (s + 1) * steps)
            forward = u0[c, span, :] + a0[c, span, :] * entry[0][s]
            backward = u1[c, span, :] + a1[c, span, :] * entry[1][s]
            out_ref[span, lanes] = (gel[span, lanes] * (forward + backward)).astype(jnp.bfloat16)


def mixer(x, weights, conv_weight, w_rec, w_inp, decay):
    length, model = x.shape
    channels = conv_weight.shape[1]
    group = w_rec.shape[2]
    width = min(256, channels)
    count = channels // width
    gates = jnp.concatenate([w_rec[0], w_inp[0], w_rec[1], w_inp[1]], axis=-1)
    coef = -8.0 * jax.nn.softplus(-decay)
    f32 = functools.partial(pltpu.VMEM, dtype=jnp.float32)
    return pl.pallas_call(
        mixer_kernel,
        grid=(count,),
        out_shape=jax.ShapeDtypeStruct((length, channels), jnp.bfloat16),
        in_specs=[
            pl.BlockSpec((length, model), lambda j: (0, 0)),
            pl.BlockSpec((model, width), lambda j: (0, j)),
            pl.BlockSpec((model, width), lambda j: (0, count + j)),
            pl.BlockSpec((4, width), lambda j: (0, j)),
            pl.BlockSpec((width // group, group, 4 * group), lambda j: (j, 0, 0)),
            pl.BlockSpec((2, width), lambda j: (0, j)),
        ],
        out_specs=pl.BlockSpec((length, width), lambda j: (0, j)),
        scratch_shapes=[f32((length + 16, width)), f32((length, width))]
        + [f32((width // group, length, group)) for i in range(4)],
        compiler_params=pltpu.CompilerParams(vmem_limit_bytes=VMEM_BYTES),
        cost_estimate=pl.CostEstimate(
            flops=4 * length * model * channels + 16 * length * group * channels * 8,
            bytes_accessed=2 * (length * model + 2 * model * channels + length * channels),
            transcendentals=12 * length * channels,
        ),
    )(x, weights, weights, conv_weight, gates, coef)


def ffn_kernel(x_ref, gate_ref, up_ref, down_ref, out_ref, total):
    step = pl.program_id(0)
    gate = jnp.dot(x_ref[...], gate_ref[...], preferred_element_type=jnp.float32)
    up = jnp.dot(x_ref[...], up_ref[...], preferred_element_type=jnp.float32)
    hidden = (jax.nn.silu(gate) * up).astype(jnp.bfloat16)
    partial = lax.dot_general(
        hidden, down_ref[...], (((1,), (1,)), ((), ())), preferred_element_type=jnp.float32
    )

    @pl.when(step == 0)
    def _():
        total[...] = partial

    @pl.when(step > 0)
    def _():
        total[...] += partial

    @pl.when(step == pl.num_programs(0) - 1)
    def _():
        out_ref[...] = total[...].astype(jnp.bfloat16)


def ffn(x, weights):
    rows, model = x.shape
    units = weights.shape[1] // 3
    width = 256 if units % 256 == 0 else 128
    count = units // width
    return pl.pallas_call(
        ffn_kernel,
        grid=(count,),
        out_shape=jax.ShapeDtypeStruct((rows, model), jnp.bfloat16),
        in_specs=[
            pl.BlockSpec((rows, model), lambda j: (0, 0)),
            pl.BlockSpec((model, width), lambda j: (0, j)),
            pl.BlockSpec((model, width), lambda j: (0, count + j)),
            pl.BlockSpec((model, width), lambda j: (0, 2 * count + j)),
        ],
        out_specs=pl.BlockSpec((rows, model), lambda j: (0, 0)),
        scratch_shapes=[pltpu.VMEM((rows, model), jnp.float32)],
        compiler_params=pltpu.CompilerParams(vmem_limit_bytes=VMEM_BYTES),
        cost_estimate=pl.CostEstimate(
            flops=6 * rows * model * units,
            bytes_accessed=2 * (2 * rows * model + 3 * model * units),
            transcendentals=rows * units,
        ),
    )(x, weights, weights, weights)


def swap(values):
    return lax.ppermute(values, "tp", [(0, 1), (1, 0)])


def matmul_t(rows, weight_t):
    return lax.dot_general(
        rows, weight_t, (((1,), (1,)), ((), ())), preferred_element_type=jnp.float32
    )


def project_kernel(x_ref, gain_ref, weight_ref, branch_ref, gel_ref):
    width = branch_ref.shape[1]
    x = normed(x_ref[...].astype(jnp.float32), gain_ref[...]).astype(jnp.bfloat16)
    both = jnp.dot(x, weight_ref[...], preferred_element_type=jnp.float32)
    branch_ref[...] = both[:, :width].astype(jnp.bfloat16)
    gelu_in = both[:, width:].astype(jnp.bfloat16).astype(jnp.float32)
    gel_ref[...] = jax.nn.gelu(gelu_in).astype(jnp.bfloat16)


def project(tokens, gain, weights):
    rows, model = tokens.shape
    channels = weights.shape[1] // 2
    block = min(256, rows)
    return pl.pallas_call(
        project_kernel,
        grid=(rows // block,),
        out_shape=(jax.ShapeDtypeStruct((rows, channels), jnp.bfloat16),) * 2,
        in_specs=[
            pl.BlockSpec((block, model), lambda i: (i, 0)),
            pl.BlockSpec((1, model), lambda i: (0, 0)),
            pl.BlockSpec((model, 2 * channels), lambda i: (0, 0)),
        ],
        out_specs=(pl.BlockSpec((block, channels), lambda i: (i, 0)),) * 2,
        compiler_params=pltpu.CompilerParams(vmem_limit_bytes=VMEM_BYTES),
        cost_estimate=pl.CostEstimate(
            flops=4 * rows * model * channels,
            bytes_accessed=2 * (rows * model + 2 * model * channels + 2 * rows * channels),
            transcendentals=rows * channels,
        ),
    )(tokens, gain.reshape(1, model), weights)


def scan_kernel(
    own_b, peer_b, own_g, peer_g, conv_ref, gates_ref, coef_ref, out_ref, pad, gel_ref, a0, u0, a1, u1
):
    half, width = own_b.shape
    length = 2 * half
    group = gates_ref.shape[1]
    rows = 256
    place = lax.axis_index("tp")
    pad[0:8, :] = jnp.zeros((8, width), jnp.float32)
    pad[8 + length : 16 + length, :] = jnp.zeros((8, width), jnp.float32)
    for source, base in ((own_b, place * half), (peer_b, (1 - place) * half)):
        at = pl.multiple_of(base, half)
        pad[pl.ds(8 + at, half), :] = source[...].astype(jnp.float32)

    gel_ref[0] = own_g[...]
    gel_ref[1] = peer_g[...]

    for part in range(width // group):
        cols = slice(part * group, (part + 1) * group)
        taps = conv_ref[:, cols].astype(jnp.float32)
        coef = coef_ref[:, cols]
        for start in range(0, length, rows):
            summed = taps[0:1] * pad[6 + start : 6 + start + rows, cols]
            for j in range(1, 4):
                summed = summed + taps[j : j + 1] * pad[6 + j + start : 6 + j + start + rows, cols]
            conv = summed.astype(jnp.bfloat16)
            wide = conv.astype(jnp.float32)
            for d, (a_ref, u_ref) in enumerate(((a0, u0), (a1, u1))):
                gate = jnp.dot(
                    conv,
                    gates_ref[part, :, 2 * d * group : 2 * (d + 1) * group],
                    preferred_element_type=jnp.float32,
                )
                rate = jax.nn.sigmoid(gate[:, :group])
                inflow = jax.nn.sigmoid(gate[:, group:])
                log_retain = rate * coef[d : d + 1]
                retain = jnp.exp(log_retain)
                left = one_minus_exp(2.0 * log_retain, retain * retain)
                a_ref[part, start : start + rows, :] = retain
                u_ref[part, start : start + rows, :] = jnp.sqrt(left) * inflow * wide

    steps = length // SEGMENTS

    def step(t, carry):
        out = []
        for (state, decayed), (a_ref, u_ref), at in (
            (carry[0], (a0, u0), t),
            (carry[1], (a1, u1), steps - 1 - t),
        ):
            where = pl.ds(at, SEGMENTS, stride=steps)
            nstate, ndecayed = [], []
            for c in range(n):
                retain = a_ref[c, where, :]
                h = retain * state[c] + u_ref[c, where, :]
                p = retain * decayed[c]
                u_ref[c, where, :] = h
                a_ref[c, where, :] = p
                nstate.append(h)
                ndecayed.append(p)
            out.append((tuple(nstate), tuple(ndecayed)))
        return tuple(out)

    n = width // group
    zero = tuple(jnp.zeros((SEGMENTS, group), jnp.float32) for c in range(n))
    one = tuple(jnp.ones((SEGMENTS, group), jnp.float32) for c in range(n))
    ended = lax.fori_loop(0, steps, step, ((zero, one), (zero, one)), unroll=8)
    per_half = SEGMENTS // 2
    for c in range(n):
        lanes = slice(c * group, (c + 1) * group)
        blank = jnp.zeros((1, group), jnp.float32)
        entry = [[None] * SEGMENTS, [None] * SEGMENTS]
        for d, order in ((0, range(SEGMENTS)), (1, range(SEGMENTS - 1, -1, -1))):
            carry = blank
            for s in order:
                entry[d][s] = carry
                carry = ended[d][0][c][s : s + 1] + ended[d][1][c][s : s + 1] * carry
        for s in range(SEGMENTS):
            span = slice(s * steps, (s + 1) * steps)
            side = s // per_half
            local = slice((s % per_half) * steps, (s % per_half + 1) * steps)
            which = jnp.where(place == side, 0, 1)
            forward = u0[c, span, :] + a0[c, span, :] * entry[0][s]
            backward = u1[c, span, :] + a1[c, span, :] * entry[1][s]
            gel = gel_ref[which, local, lanes].astype(jnp.float32)
            out_ref[which, local, lanes] = (gel * (forward + backward)).astype(jnp.bfloat16)


def gated_scan(own, peer, block, width, conv_weight, gates, coef):
    half = own[0].shape[0]
    length = 2 * half
    group = gates.shape[1]
    f32 = functools.partial(pltpu.VMEM, dtype=jnp.float32)
    rows_spec = pl.BlockSpec((half, width), lambda i: (0, block))
    return pl.pallas_call(
        scan_kernel,
        grid=(1,),
        out_shape=jax.ShapeDtypeStruct((2, half, width), jnp.bfloat16),
        in_specs=[
            rows_spec,
            rows_spec,
            rows_spec,
            rows_spec,
            pl.BlockSpec((4, width), lambda i: (0, block)),
            pl.BlockSpec((width // group, group, 4 * group), lambda i: (block, 0, 0)),
            pl.BlockSpec((2, width), lambda i: (0, block)),
        ],
        out_specs=pl.BlockSpec((2, half, width), lambda i: (0, 0, 0)),
        scratch_shapes=[f32((length + 16, width)), pltpu.VMEM((2, half, width), jnp.bfloat16)]
        + [f32((width // group, length, group)) for i in range(4)],
        compiler_params=pltpu.CompilerParams(vmem_limit_bytes=VMEM_BYTES),
        cost_estimate=pl.CostEstimate(
            flops=80 * length * group * width,
            bytes_accessed=6 * length * width,
            transcendentals=12 * length * width,
        ),
    )(own[0], peer[0], own[1], peer[1], conv_weight, gates, coef)


def mix_out_kernel(
    keep, ha, hb, ra, rb, own_ref, near_ref, far_ref, tokens_ref, post_ref, pre_ref, *rest
):
    total = rest[-1]
    span = near_ref.shape[0]
    core = lax.axis_index("fs") % 2
    width = ha.shape[2]
    total[...] = matmul_t(ha[0], own_ref[:, :width]) + matmul_t(hb[0], own_ref[:, width:])
    for part, at in ((near_ref, core * span), (far_ref, (1 - core) * span)):
        cols = pl.ds(pl.multiple_of(at, span), span)
        total[:, cols] += matmul_t(ra[0], part[:, :width]) + matmul_t(rb[0], part[:, width:])
    stream = tokens_ref[...].astype(jnp.float32)
    residual = (stream + normed(total[...], post_ref[...])).astype(jnp.bfloat16)
    if keep:
        rest[1][...] = residual
    rest[0][...] = normed(residual.astype(jnp.float32), pre_ref[...]).astype(jnp.bfloat16)


def mix_out(keep, hidden, came, out_own, near, far, tokens, post_gain, pre_gain):
    rows, model = tokens.shape
    width = hidden[0].shape[2]
    channels = out_own.shape[1]
    block = min(256, rows)
    mine, theirs = (0, 1) if keep else (1, 0)
    h_spec = pl.BlockSpec((1, block, width), lambda i: (mine, i, 0))
    r_spec = pl.BlockSpec((1, block, width), lambda i: (theirs, i, 0))
    row_spec = pl.BlockSpec((block, model), lambda i: (i, 0))
    gain_spec = pl.BlockSpec((1, model), lambda i: (0, 0))
    half_spec = pl.BlockSpec((model // 2, channels), lambda i: (0, 0))
    shape = jax.ShapeDtypeStruct((rows, model), jnp.bfloat16)
    count = 2 if keep else 1
    return pl.pallas_call(
        functools.partial(mix_out_kernel, keep),
        grid=(rows // block,),
        out_shape=(shape,) * count,
        in_specs=[
            h_spec,
            h_spec,
            r_spec,
            r_spec,
            pl.BlockSpec((model, channels), lambda i: (0, 0)),
            half_spec,
            half_spec,
            row_spec,
            gain_spec,
            gain_spec,
        ],
        out_specs=(row_spec,) * count,
        scratch_shapes=[pltpu.VMEM((block, model), jnp.float32)],
        compiler_params=pltpu.CompilerParams(vmem_limit_bytes=VMEM_BYTES),
        cost_estimate=pl.CostEstimate(
            flops=4 * rows * model * channels,
            bytes_accessed=2 * (3 * rows * model + 2 * model * channels),
            transcendentals=rows,
        ),
    )(
        *hidden,
        *came,
        out_own,
        near,
        far,
        tokens,
        post_gain.reshape(1, model),
        pre_gain.reshape(1, model),
    )


def expand_kernel(x_ref, gate_ref, up_ref, out_ref):
    gate = jnp.dot(x_ref[...], gate_ref[...], preferred_element_type=jnp.float32)
    up = jnp.dot(x_ref[...], up_ref[...], preferred_element_type=jnp.float32)
    out_ref[...] = (jax.nn.silu(gate) * up).astype(jnp.bfloat16)


def expand(x, weights):
    rows, model = x.shape
    units = weights.shape[1] // 2
    width = 256 if units % 256 == 0 else 128
    count = units // width
    return pl.pallas_call(
        expand_kernel,
        grid=(count,),
        out_shape=jax.ShapeDtypeStruct((rows, units), jnp.bfloat16),
        in_specs=[
            pl.BlockSpec((rows, model), lambda j: (0, 0)),
            pl.BlockSpec((model, width), lambda j: (0, j)),
            pl.BlockSpec((model, width), lambda j: (0, count + j)),
        ],
        out_specs=pl.BlockSpec((rows, width), lambda j: (0, j)),
        compiler_params=pltpu.CompilerParams(vmem_limit_bytes=VMEM_BYTES),
        cost_estimate=pl.CostEstimate(
            flops=4 * rows * model * units,
            bytes_accessed=2 * (rows * model + 2 * model * units + rows * units),
            transcendentals=rows * units,
        ),
    )(x, weights, weights)


def contract_kernel(x_ref, weight_ref, out_ref):
    out_ref[...] = matmul_t(x_ref[...], weight_ref[...]).astype(jnp.bfloat16)


def contract(x, weight_t):
    rows, units = x.shape
    model = weight_t.shape[0]
    width = min(256, model)
    return pl.pallas_call(
        contract_kernel,
        grid=(model // width,),
        out_shape=jax.ShapeDtypeStruct((rows, model), jnp.bfloat16),
        in_specs=[
            pl.BlockSpec((rows, units), lambda j: (0, 0)),
            pl.BlockSpec((width, units), lambda j: (j, 0)),
        ],
        out_specs=pl.BlockSpec((rows, width), lambda j: (0, j)),
        compiler_params=pltpu.CompilerParams(vmem_limit_bytes=VMEM_BYTES),
        cost_estimate=pl.CostEstimate(
            flops=2 * rows * model * units,
            bytes_accessed=2 * (rows * model + model * units + rows * units),
            transcendentals=0,
        ),
    )(x, weight_t)


def finish_kernel(pieces, size, *refs):
    own, back = refs[:pieces], refs[pieces : 2 * pieces]
    residual_ref, gain_ref, out_ref, total = refs[2 * pieces :]
    model = total.shape[1]
    shards = model // (pieces * size)
    for piece in range(pieces):
        summed = own[piece][...].astype(jnp.float32) + back[piece][...].astype(jnp.float32)
        for shard in range(shards):
            at = (shard * pieces + piece) * size
            total[:, at : at + size] = summed[:, shard * size : (shard + 1) * size]
    middle = residual_ref[...].astype(jnp.float32)
    out_ref[...] = (middle + normed(total[...], gain_ref[...])).astype(jnp.bfloat16)


def finish(own, back, size, residual, gain):
    rows, model = residual.shape
    pieces = len(own)
    block = min(128, rows)
    part_spec = pl.BlockSpec((block, model // pieces), lambda i: (i, 0))
    row_spec = pl.BlockSpec((block, model), lambda i: (i, 0))
    return pl.pallas_call(
        functools.partial(finish_kernel, pieces, size),
        grid=(rows // block,),
        out_shape=jax.ShapeDtypeStruct((rows, model), jnp.bfloat16),
        in_specs=[part_spec] * (2 * pieces) + [row_spec, pl.BlockSpec((1, model), lambda i: (0, 0))],
        out_specs=row_spec,
        scratch_shapes=[pltpu.VMEM((block, model), jnp.float32)],
        compiler_params=pltpu.CompilerParams(vmem_limit_bytes=VMEM_BYTES),
        cost_estimate=pl.CostEstimate(
            flops=8 * rows * model, bytes_accessed=8 * rows * model, transcendentals=rows
        ),
    )(*own, *back, residual, gain.reshape(1, model))


def paired_device(
    tokens,
    pre_mix_gain,
    post_mix_gain,
    pre_ffn_gain,
    post_ffn_gain,
    w_branch,
    w_gelu,
    conv_weight,
    w_rec,
    w_inp,
    decay,
    out_weight_t,
    w_gate,
    w_up,
    down_weight_t,
):
    channels = conv_weight.shape[1]
    core = lax.axis_index("fs") % 2
    fs_size = lax.axis_size("fs")
    gather = functools.partial(lax.all_gather, axis_name="fs", axis=0, tiled=True)
    other = swap(tokens)
    mix_all = gather(jnp.concatenate([w_branch, w_gelu], axis=1))
    out_own = gather(out_weight_t)
    up_all = gather(jnp.concatenate([w_gate, w_up], axis=1))
    size = down_weight_t.shape[0] // DOWN_PIECES
    down_all = [gather(down_weight_t[i * size : (i + 1) * size]) for i in range(DOWN_PIECES)]
    gates = jnp.concatenate([w_rec[0], w_inp[0], w_rec[1], w_inp[1]], axis=-1)
    coef = -8.0 * jax.nn.softplus(-decay)

    own = project(tokens, pre_mix_gain, mix_all)
    other, own, out_own = lax.optimization_barrier((other, own, out_own))
    span = out_own.shape[0] // 2
    partners = [(i, i + 1 - 2 * (i % 2)) for i in range(fs_size)]
    near = swap(lax.dynamic_slice_in_dim(out_own, core * span, span, 0))
    peer = project(other, pre_mix_gain, mix_all)
    width = min(256, channels)
    hidden, came = [], []
    for block in range(channels // width):
        hidden.append(gated_scan(own, peer, block, width, conv_weight, gates, coef))
        came.append(swap(hidden[-1]))
    far = lax.ppermute(near, "fs", partners)
    shared = (hidden, came, out_own, near, far)
    (away_mid,) = mix_out(False, *shared, other, post_mix_gain, pre_ffn_gain)
    away_hidden = expand(away_mid, up_all)
    back = []
    for piece in down_all:
        back.append(swap(contract(away_hidden, piece)))
    own_mid, residual = mix_out(True, *shared, tokens, post_mix_gain, pre_ffn_gain)
    own_hidden = expand(own_mid, up_all)
    kept = [contract(own_hidden, piece) for piece in down_all]
    return finish(kept, back, size, residual, post_ffn_gain)


def wide_device(
    tokens,
    pre_mix_gain,
    post_mix_gain,
    pre_ffn_gain,
    post_ffn_gain,
    w_branch,
    w_gelu,
    conv_weight,
    w_rec,
    w_inp,
    decay,
    out_weight_t,
    w_gate,
    w_up,
    down_weight_t,
):
    channels = conv_weight.shape[1]
    mix_shard = jnp.concatenate([w_branch, w_gelu, out_weight_t], axis=1)
    ffn_shard = jnp.concatenate([w_gate, w_up, down_weight_t], axis=1)
    stream = tokens.astype(jnp.float32)
    normed_in = normed(stream, pre_mix_gain).astype(jnp.bfloat16)
    mix_all = lax.all_gather(mix_shard, "fs", axis=0, tiled=True)
    whole = lax.all_gather(normed_in, "tp", axis=0, tiled=True)
    ffn_all = lax.all_gather(ffn_shard, "fs", axis=0, tiled=True)
    out_own = mix_all[:, 2 * channels :]
    hidden = mixer(whole, mix_all, conv_weight, w_rec, w_inp, decay)
    own_hidden = lax.all_to_all(hidden, "tp", split_axis=0, concat_axis=1, tiled=True)
    out_whole = lax.all_gather(out_own, "tp", axis=1, tiled=True)
    mixer_sum = matmul_t(own_hidden, out_whole)
    residual = (stream + normed(mixer_sum, post_mix_gain)).astype(jnp.bfloat16)
    middle = residual.astype(jnp.float32)
    normed_mid = normed(middle, pre_ffn_gain).astype(jnp.bfloat16)
    all_mid = lax.all_gather(normed_mid, "tp", axis=0, tiled=True)
    ffn_sum = lax.psum_scatter(
        ffn(all_mid, ffn_all), "tp", scatter_dimension=0, tiled=True
    ).astype(jnp.float32)
    return (middle + normed(ffn_sum, post_ffn_gain)).astype(jnp.bfloat16)


def solution(mesh):
    return jax.shard_map(
        paired_device if mesh.shape["tp"] == 2 else wide_device,
        mesh=mesh,
        in_specs=(
            P(("fs", "tp"), None),
            P(),
            P(),
            P(),
            P(),
            P("fs", "tp"),
            P("fs", "tp"),
            P(None, "tp"),
            P(None, "tp", None, None),
            P(None, "tp", None, None),
            P(None, "tp"),
            P("fs", "tp"),
            P("fs", "tp"),
            P("fs", "tp"),
            P("fs", "tp"),
        ),
        out_specs=P(("fs", "tp"), None),
        check_vma=False,
    )
```

time: 242 us -> 351 us (1.45)
  waiting for transfers between devices: 67.7 us -> 212 us
  Pallas kernels: 125 us -> 105 us
  other arithmetic: 17.5 us -> 5.31 us
  matrix products: 4.58 us -> 0 us
    all_gather x1 -> x5, waiting for transfers between devices: 15.3 us -> 165 us  [the longest x2 72.8 us: paired_device(): gather(down_weight_t[i * size:(i + 1) * size])]
    pallas_call x5 -> x13, Pallas kernels: 125 us -> 105 us  [the longest x2 23.9 us: expand(): pl.pallas_call(expand_kernel, grid=(count,), out_shape=jax.ShapeDtypeStru...]
    convert_element_type x3 -> x0, other arithmetic: 8.17 us -> none  [the longest x1 4.17 us: per_device(): return (middle + normed(ffn_sum, post_ffn_gain)).astype(jnp.bfloat16)]
    ppermute x6, waiting for transfers between devices: 51.9 us -> 45.7 us  [swap(): return lax.ppermute(values, 'tp', [(0, 1), (1, 0)])]
    reduce_sum x3 -> x0, other arithmetic: 5.76 us -> none  [normed(): factor = lax.rsqrt(jnp.mean(values * values, axis=-1, keepdims=True) + EPS)]
    dot_general x2 -> x0, matrix products: 4.58 us -> none  [matmul_t(): lax.dot_general(rows, weight_t, (((1,), (1,)), ((), ())), preferred_eleme...]
  transfers between devices with their start and end apart: 8 -> 12, of which waited for: 5 -> 8; matrix products, arithmetic and copies ran while one was open for 5% -> 2% of each run, Pallas kernels for 30% -> 28%
where the time goes in v1:
time: 351 us; the launch traced here: 350 us
  waiting for transfers between devices  212 us (60%)
  Pallas kernels  105 us (30%)
  between operations  13.2 us (4%)
  starting transfers between devices  9.71 us (3%)
  other arithmetic  5.31 us (2%)
  local copies, waits for them, and re-layouts  4.69 us (1%)
    all_gather x2, waiting for transfers between devices, paired_device(): gather(down_weight_t[i * size:(i + 1) * size])  72.8 us
    all_gather x1, waiting for transfers between devices, paired_device(): mix_all = gather(jnp.concatenate([w_branch, w_gelu], axis=1))  46.9 us
    ppermute x6, waiting for transfers between devices, swap(): return lax.ppermute(values, 'tp', [(0, 1), (1, 0)])  45.7 us
    all_gather x1, waiting for transfers between devices, paired_device(): out_own = gather(out_weight_t)  35.7 us
    pallas_call x2, Pallas kernels, expand(): pl.pallas_call(expand_kernel, grid=(count,), out_shape=jax.ShapeDtypeStru...  23.9 us
    pallas_call x2, Pallas kernels, gated_scan(): pl.pallas_call(scan_kernel, grid=(1,), out_shape=jax.ShapeDtypeStruct((2,...  23.4 us
    pallas_call x4, Pallas kernels, contract(): pl.pallas_call(contract_kernel, grid=(model // width,), out_shape=jax.Sha...  22.1 us
    pallas_call x2, Pallas kernels, mix_out(): pl.pallas_call(functools.partial(mix_out_kernel, keep), grid=(rows // blo...  16.9 us
  transfers between devices with their start and end apart: 12, of which 8 were waited for; matrix products, arithmetic and copies ran while one was open for 2% of the time, Pallas kernels for 28%

profile of v1, /device:TPU:0, one launch (start us, length us, event | category | flops | bytes accessed | tf_op | source)
XLA Modules:
  0.0 350.1 jit_solution(7703944878230509661)
XLA Ops:
  6.5 0.0 copy-start.8
  6.5 0.0 all-gather.6.cloned.1.call-start
  6.5 1.7 pad_maximum_fusion.2
  8.3 0.0 all-gather.6.cloned.1.call-update
  8.3 0.0 all-gather.8.cloned.1.call-start
  8.4 0.7 all-gather.8.cloned.1.call-update
  9.1 0.0 all-gather.10.cloned.1.call-start
  9.1 2.1 pad_maximum_fusion
  11.2 0.0 all-gather.10.cloned.1.call-update
  11.2 0.0 all-gather.12.cloned.1.call-start
  11.3 0.0 copy-done.8
  11.3 0.8 fusion.1
  12.1 0.0 all-gather.12.cloned.1.call-update
  12.1 0.0 all-gather.14.cloned.1.call-start
  12.1 0.5 all-gather.14.cloned.1.call-update
  12.7 3.0 collective-permute-start
  15.7 46.9 %all-gather.6.cloned.1.call-done.weight_ref = bf16[2048,1024]{1,0:T(8,128)(2,1)} async-done(((bf16[128,1024]{1,0:T(8,128)(2,1)}), bf16[2048,1024]{1,0:T(8,128)(2,1)}) %all-gather.6.cloned.1.call-update) | async-done | bytes 4194320 | tf_op jit(solution)/shard_map/all_gather | solution.py:533
  62.6 6.5 %shard_map.145 = (bf16[512,512]{1,0:T(8,128)(2,1)}, bf16[512,512]{1,0:T(8,128)(2,1)}) custom-call(bf16[512,2048]{1,0:T(8,128)(2,1)} %tokens_ref.1, f32[1,2048]{1,0:T(1,128)} %bitcast.17, bf16[2048,1024]{1,0:T(8,128)(2,1)} %all-gather.6.cloned.1.call-done.weight_ref), custom_call_target="tpu_custom_call" | custom-call | flops 2147483648 | bytes 7340032 | tf_op jit(solution)/shard_map/pallas_call | solution.py:217
  69.1 0.0 copy-start.9
  69.1 0.0 collective-permute-done.x_ref.tokens_ref
  69.1 0.0 copy-start.2
  69.1 35.7 %all-gather.8.cloned.1.call-done.own_ref = bf16[2048,512]{1,0:T(8,128)(2,1)} async-done(((bf16[128,512]{1,0:T(8,128)(2,1)}), bf16[2048,512]{1,0:T(8,128)(2,1)}) %all-gather.8.cloned.1.call-update) | async-done | bytes 2097168 | tf_op jit(solution)/shard_map/all_gather | solution.py:534
  104.8 0.0 copy-done.2
  104.8 1.3 constant_dynamic-slice_fusion
  106.1 1.5 collective-permute-start.3
  107.6 0.0 copy-done.9
  107.7 0.0 copy-done.10
  107.7 0.9 pad_maximum_fusion.1.gates_ref
  108.6 0.0 copy-done.11
  108.6 0.6 fusion.coef_ref
  109.2 22.3 %collective-permute-done.3.near_ref = bf16[1024,512]{1,0:T(8,128)(2,1)S(1)} collective-permute-done((bf16[1024,512]{1,0:T(8,128)(2,1)S(1)}, bf16[1024,512]{1,0:T(8,128)(2,1)S(1)}, u32[]{:S(2)}, u32[]{:S(2)}) %collective-permute-start.3) | collective-permute-done | bytes 1048608 | tf_op jit(solution)/shard_map/ppermute | solution.py:195
  131.5 0.0 collective-permute-start.4
  131.5 6.9 %shard_map.146 = (bf16[512,512]{1,0:T(8,128)(2,1)}, bf16[512,512]{1,0:T(8,128)(2,1)}) custom-call(bf16[512,2048]{1,0:T(8,128)(2,1)} %copy-done.2, f32[1,2048]{1,0:T(1,128)} %bitcast.18, bf16[2048,1024]{1,0:T(8,128)(2,1)} %all-gather.6.cloned.1.call-done.weight_ref), custom_call_target="tpu_custom_call" | custom-call | flops 2147483648 | bytes 7340032 | tf_op jit(solution)/shard_map/pallas_call | solution.py:217
  138.4 0.0 copy-done
  138.4 11.6 %shard_map.148.hb = bf16[2,512,256]{2,1,0:T(8,128)(2,1)} custom-call(bf16[512,512]{1,0:T(8,128)(2,1)} %get-tuple-element.17.own_b, bf16[512,512]{1,0:T(8,128)(2,1)} %get-tuple-element.19.peer_b, bf16[512,512]{1,0:T(8,128)(2,1)} %get-tuple-element.20.own_g, bf16[512,512]{1,0:T(8,128)(2,1)} %get-tuple-element.21.peer_g, bf16[4,512]{1,0:T(4,128)(2,1)} %conv_ref.3, ...), custom_call_target="tpu_custom_call" | custom-call | flops 2684354560 | bytes 1572864 | tf_op jit(solution)/shard_map/pallas_call | solution.py:329
  150.0 11.8 %shard_map.147.ha = bf16[2,512,256]{2,1,0:T(8,128)(2,1)} custom-call(bf16[512,512]{1,0:T(8,128)(2,1)} %get-tuple-element.17.own_b, bf16[512,512]{1,0:T(8,128)(2,1)} %get-tuple-element.19.peer_b, bf16[512,512]{1,0:T(8,128)(2,1)} %get-tuple-element.20.own_g, bf16[512,512]{1,0:T(8,128)(2,1)} %get-tuple-element.21.peer_g, bf16[4,512]{1,0:T(4,128)(2,1)} %conv_ref.3, ...), custom_call_target="tpu_custom_call" | custom-call | flops 2684354560 | bytes 1572864 | tf_op jit(solution)/shard_map/pallas_call | solution.py:329
  161.8 1.5 collective-permute-start.1
  163.3 0.0 copy-done.3
  163.3 0.6 collective-permute-start.2
  163.9 13.0 %collective-permute-done.1.ra = bf16[2,512,256]{2,1,0:T(8,128)(2,1)S(1)} collective-permute-done((bf16[2,512,256]{2,1,0:T(8,128)(2,1)}, bf16[2,512,256]{2,1,0:T(8,128)(2,1)S(1)}, u32[]{:S(2)}, u32[]{:S(2)}) %collective-permute-start.1) | collective-permute-done | bytes 524320 | tf_op jit(solution)/shard_map/ppermute | solution.py:195
  176.8 10.4 %collective-permute-done.2.rb = bf16[2,512,256]{2,1,0:T(8,128)(2,1)S(1)} collective-permute-done((bf16[2,512,256]{2,1,0:T(8,128)(2,1)S(1)}, bf16[2,512,256]{2,1,0:T(8,128)(2,1)S(1)}, u32[]{:S(2)}, u32[]{:S(2)}) %collective-permute-start.2) | collective-permute-done | bytes 524320 | tf_op jit(solution)/shard_map/ppermute | solution.py:195
  187.3 0.0 collective-permute-done.4.far_ref
  187.3 0.0 copy-done.4
  187.3 0.8 copy-done.5
  188.1 0.4 copy-done.1
  188.4 8.4 %shard_map.153.x_ref = bf16[512,2048]{1,0:T(8,128)(2,1)} custom-call(bf16[2,512,256]{2,1,0:T(8,128)(2,1)} %shard_map.147.ha, bf16[2,512,256]{2,1,0:T(8,128)(2,1)} %shard_map.148.hb, bf16[2,512,256]{2,1,0:T(8,128)(2,1)} %copy-done.4, bf16[2,512,256]{2,1,0:T(8,128)(2,1)} %copy-done.5, bf16[2048,512]{1,0:T(8,128)(2,1)} %all-gather.8.cloned.1.call-done.own_ref, ...), custom_call_target="tpu_custom_call" | custom-call | flops 2147483648 | bytes 10485760 | tf_op jit(solution)/shard_map/pallas_call | solution.py:385
  196.8 9.5 %all-gather.10.cloned.1.call-done.gate_ref.up_ref = bf16[2048,3072]{1,0:T(8,128)(2,1)} async-done(((bf16[128,3072]{1,0:T(8,128)(2,1)}), bf16[2048,3072]{1,0:T(8,128)(2,1)}) %all-gather.10.cloned.1.call-update) | async-done | bytes 12582928 | tf_op jit(solution)/shard_map/all_gather | solution.py:535
  206.3 11.9 %shard_map.154.x_ref = bf16[512,1536]{1,0:T(8,128)(2,1)} custom-call(bf16[512,2048]{1,0:T(8,128)(2,1)} %shard_map.153.x_ref, bf16[2048,3072]{1,0:T(8,128)(2,1)} %all-gather.10.cloned.1.call-done.gate_ref.up_ref, bf16[2048,3072]{1,0:T(8,128)(2,1)} %all-gather.10.cloned.1.call-done.gate_ref.up_ref), custom_call_target="tpu_custom_call" | custom-call | flops 6442450944 | bytes 16252928 | tf_op jit(solution)/shard_map/pallas_call | solution.py:432
  218.2 33.9 %all-gather.12.cloned.1.call-done.weight_ref = bf16[1024,1536]{1,0:T(8,128)(2,1)} async-done(((bf16[64,1536]{1,0:T(8,128)(2,1)}), bf16[1024,1536]{1,0:T(8,128)(2,1)}) %all-gather.12.cloned.1.call-update) | async-done | bytes 3145744 | tf_op jit(solution)/shard_map/all_gather | solution.py:537
  252.1 5.5 %shard_map.155 = bf16[512,1024]{1,0:T(8,128)(2,1)} custom-call(bf16[512,1536]{1,0:T(8,128)(2,1)} %shard_map.154.x_ref, bf16[1024,1536]{1,0:T(8,128)(2,1)} %all-gather.12.cloned.1.call-done.weight_ref), custom_call_target="tpu_custom_call" | custom-call | flops 1610612736 | bytes 5767168 | tf_op jit(solution)/shard_map/pallas_call | solution.py:459
  257.7 1.5 collective-permute-start.5
  259.1 38.8 %all-gather.14.cloned.1.call-done.weight_ref = bf16[1024,1536]{1,0:T(8,128)(2,1)} async-done(((bf16[64,1536]{1,0:T(8,128)(2,1)}), bf16[1024,1536]{1,0:T(8,128)(2,1)}) %all-gather.14.cloned.1.call-update) | async-done | bytes 3145744 | tf_op jit(solution)/shard_map/all_gather | solution.py:537
  298.0 5.5 %shard_map.156 = bf16[512,1024]{1,0:T(8,128)(2,1)} custom-call(bf16[512,1536]{1,0:T(8,128)(2,1)} %shard_map.154.x_ref, bf16[1024,1536]{1,0:T(8,128)(2,1)} %all-gather.14.cloned.1.call-done.weight_ref), custom_call_target="tpu_custom_call" | custom-call | flops 1610612736 | bytes 5767168 | tf_op jit(solution)/shard_map/pallas_call | solution.py:459
  303.5 1.5 collective-permute-start.6
  304.9 8.5 %shard_map.149 = (bf16[512,2048]{1,0:T(8,128)(2,1)}, bf16[512,2048]{1,0:T(8,128)(2,1)}) custom-call(bf16[2,512,256]{2,1,0:T(8,128)(2,1)} %shard_map.147.ha, bf16[2,512,256]{2,1,0:T(8,128)(2,1)} %shard_map.148.hb, bf16[2,512,256]{2,1,0:T(8,128)(2,1)} %copy-done.4, bf16[2,512,256]{2,1,0:T(8,128)(2,1)} %copy-done.5, ...), custom_call_target="tpu_custom_call" | custom-call | flops 2147483648 | bytes 10485760 | tf_op jit(solution)/shard_map/pallas_call | solution.py:385
  313.4 11.9 %shard_map.150.x_ref = bf16[512,1536]{1,0:T(8,128)(2,1)} custom-call(bf16[512,2048]{1,0:T(8,128)(2,1)} %get-tuple-element.23.x_ref, bf16[2048,3072]{1,0:T(8,128)(2,1)} %all-gather.10.cloned.1.call-done.gate_ref.up_ref, bf16[2048,3072]{1,0:T(8,128)(2,1)} %all-gather.10.cloned.1.call-done.gate_ref.up_ref), custom_call_target="tpu_custom_call" | custom-call | flops 6442450944 | bytes 16252928 | tf_op jit(solution)/shard_map/pallas_call | solution.py:432
  325.4 5.5 %shard_map.152.refs_1_ = bf16[512,1024]{1,0:T(8,128)(2,1)} custom-call(bf16[512,1536]{1,0:T(8,128)(2,1)} %shard_map.150.x_ref, bf16[1024,1536]{1,0:T(8,128)(2,1)} %all-gather.14.cloned.1.call-done.weight_ref), custom_call_target="tpu_custom_call" | custom-call | flops 1610612736 | bytes 5767168 | tf_op jit(solution)/shard_map/pallas_call | solution.py:459
  330.9 5.5 %shard_map.151.refs_0_ = bf16[512,1024]{1,0:T(8,128)(2,1)} custom-call(bf16[512,1536]{1,0:T(8,128)(2,1)} %shard_map.150.x_ref, bf16[1024,1536]{1,0:T(8,128)(2,1)} %all-gather.12.cloned.1.call-done.weight_ref), custom_call_target="tpu_custom_call" | custom-call | flops 1610612736 | bytes 5767168 | tf_op jit(solution)/shard_map/pallas_call | solution.py:459
  336.4 0.0 collective-permute-done.5.refs_2_
  336.4 0.0 collective-permute-done.6.refs_3_
  336.4 0.0 copy-start.7
  336.4 1.0 copy-done.6
  337.4 0.3 copy-done.7
  337.8 5.8 %shard_map.157 = bf16[512,2048]{1,0:T(8,128)(2,1)} custom-call(bf16[512,1024]{1,0:T(8,128)(2,1)} %shard_map.151.refs_0_, bf16[512,1024]{1,0:T(8,128)(2,1)} %shard_map.152.refs_1_, bf16[512,1024]{1,0:T(8,128)(2,1)} %copy-done.6, bf16[512,1024]{1,0:T(8,128)(2,1)} %copy-done.7, bf16[512,2048]{1,0:T(8,128)(2,1)} %get-tuple-element.24.refs_4_, f32[1,2048]{1,0:T(1,128)} %bitcast.16), custom_call_target="tpu_custom_call" | custom-call | flops 8388608 | bytes 8388608 | tf_op jit(solution)/shard_map/pallas_call | solution.py:497
  (9 shorter events, 0.0 us)
Async XLA Ops:
  6.5 4.7 %copy-start.8 = (bf16[128,1536]{1,0:T(8,128)(2,1)S(1)}, bf16[128,1536]{1,0:T(8,128)(2,1)}, u32[]{:S(2)}) copy-start(bf16[128,1536]{1,0:T(8,128)(2,1)} %param.29) | copy-start | bytes 1179652
  6.5 56.1 %all-gather.6.cloned.1.call-start = ((), (), s32[]{:S(2)}) async-start(), calls=%async_computation | async-start | bytes 4456448 | tf_op jit(solution)/shard_map/all_gather | solution.py:533
  8.3 96.5 %all-gather.8.cloned.1.call-start = ((), (), s32[]{:S(2)}) async-start(), calls=%async_computation.1 | async-start | bytes 2228224 | tf_op jit(solution)/shard_map/all_gather | solution.py:534
  9.1 197.2 %all-gather.10.cloned.1.call-start = ((), (), s32[]{:S(2)}) async-start(), calls=%async_computation.2 | async-start | bytes 13369344 | tf_op jit(solution)/shard_map/all_gather | solution.py:535
  11.2 240.9 %all-gather.12.cloned.1.call-start = ((), (), s32[]{:S(2)}) async-start(), calls=%async_computation.3 | async-start | bytes 3342336 | tf_op jit(solution)/shard_map/all_gather | solution.py:537
  12.1 285.9 %all-gather.14.cloned.1.call-start = ((), (), s32[]{:S(2)}) async-start(), calls=%async_computation.4 | async-start | bytes 3342336 | tf_op jit(solution)/shard_map/all_gather | solution.py:537
  12.7 56.4 %collective-permute-start = (bf16[512,2048]{1,0:T(8,128)(2,1)}, bf16[512,2048]{1,0:T(8,128)(2,1)S(1)}, u32[]{:S(2)}, u32[]{:S(2)}) collective-permute-start(bf16[512,2048]{1,0:T(8,128)(2,1)} %tokens_ref.1), channel_id=1, source_target_pairs={{0,1},{1,0},{2,3},{3,2},{4,5},{5,4},{6,7},{7,6},{8,9},{9,8},{10,11... | collective-permute-start | bytes 6291464 | tf_op jit(solution)/shard_map/ppermute | solution.py:195
  69.1 38.5 %copy-start.9 = (bf16[2,4,128,128]{3,2,1,0:T(8,128)(2,1)S(1)}, bf16[2,4,128,128]{3,2,1,0:T(8,128)(2,1)}, u32[]{:S(2)}) copy-start(bf16[2,4,128,128]{3,2,1,0:T(8,128)(2,1)} %param.24) | copy-start | bytes 786436
  69.1 38.5 %copy-start.10 = (bf16[2,4,128,128]{3,2,1,0:T(8,128)(2,1)S(1)}, bf16[2,4,128,128]{3,2,1,0:T(8,128)(2,1)}, u32[]{:S(2)}) copy-start(bf16[2,4,128,128]{3,2,1,0:T(8,128)(2,1)} %param.23) | copy-start | bytes 786436
  69.1 35.7 %copy-start.2 = (bf16[512,2048]{1,0:T(8,128)(2,1)}, bf16[512,2048]{1,0:T(8,128)(2,1)S(1)}, u32[]{:S(2)}) copy-start(bf16[512,2048]{1,0:T(8,128)(2,1)S(1)} %collective-permute-done.x_ref.tokens_ref) | copy-start | bytes 6291460
  104.8 3.8 %copy-start.11 = (f32[2,512]{1,0:T(2,128)S(1)}, f32[2,512]{1,0:T(2,128)}, u32[]{:S(2)}) copy-start(f32[2,512]{1,0:T(2,128)} %param.25) | copy-start | bytes 12292
  106.1 25.4 %collective-permute-start.3 = (bf16[1024,512]{1,0:T(8,128)(2,1)S(1)}, bf16[1024,512]{1,0:T(8,128)(2,1)S(1)}, u32[]{:S(2)}, u32[]{:S(2)}) collective-permute-start(bf16[1024,512]{1,0:T(8,128)(2,1)S(1)} %constant_dynamic-slice_fusion), channel_id=1, source_target_pairs={{0,1},{1,0},{2,3},{3,2},{4,5},{5,4},{6,7},{7,6},{8,9},{9,8},{10,11... | collective-permute-start | bytes 3145736 | tf_op jit(solution)/shard_map/ppermute | solution.py:195
  131.5 6.9 %copy-start = (bf16[1024,512]{1,0:T(8,128)(2,1)}, bf16[1024,512]{1,0:T(8,128)(2,1)S(1)}, u32[]{:S(2)}) copy-start(bf16[1024,512]{1,0:T(8,128)(2,1)S(1)} %collective-permute-done.3.near_ref) | copy-start | bytes 3145732
  131.5 55.8 %collective-permute-start.4 = (bf16[1024,512]{1,0:T(8,128)(2,1)S(1)}, bf16[1024,512]{1,0:T(8,128)(2,1)S(1)}, u32[]{:S(2)}, u32[]{:S(2)}) collective-permute-start(bf16[1024,512]{1,0:T(8,128)(2,1)S(1)} %collective-permute-done.3.near_ref), channel_id=1, source_target_pairs={{0,2},{2,0},{4,6},{6,4},{8,10},{10,8},{12,14},{14,12},{16,18},{18,... | collective-permute-start | bytes 3145736 | tf_op jit(solution)/shard_map/ppermute | solution.py:552
  150.0 13.3 %copy-start.3 = (bf16[2,512,256]{2,1,0:T(8,128)(2,1)S(1)}, bf16[2,512,256]{2,1,0:T(8,128)(2,1)}, u32[]{:S(2)}) copy-start(bf16[2,512,256]{2,1,0:T(8,128)(2,1)} %shard_map.148.hb) | copy-start | bytes 1572868
  161.8 15.0 %collective-permute-start.1 = (bf16[2,512,256]{2,1,0:T(8,128)(2,1)}, bf16[2,512,256]{2,1,0:T(8,128)(2,1)S(1)}, u32[]{:S(2)}, u32[]{:S(2)}) collective-permute-start(bf16[2,512,256]{2,1,0:T(8,128)(2,1)} %shard_map.147.ha), channel_id=1, source_target_pairs={{0,1},{1,0},{2,3},{3,2},{4,5},{5,4},{6,7},{7,6},{8,9},{9,8},{10,11... | collective-permute-start | bytes 1572872 | tf_op jit(solution)/shard_map/ppermute | solution.py:195
  163.3 23.9 %collective-permute-start.2 = (bf16[2,512,256]{2,1,0:T(8,128)(2,1)S(1)}, bf16[2,512,256]{2,1,0:T(8,128)(2,1)S(1)}, u32[]{:S(2)}, u32[]{:S(2)}) collective-permute-start(bf16[2,512,256]{2,1,0:T(8,128)(2,1)S(1)} %copy-done.3), channel_id=1, source_target_pairs={{0,1},{1,0},{2,3},{3,2},{4,5},{5,4},{6,7},{7,6},{8,9},{9,8},{10,11... | collective-permute-start | bytes 1572872 | tf_op jit(solution)/shard_map/ppermute | solution.py:195
  176.8 10.4 %copy-start.4 = (bf16[2,512,256]{2,1,0:T(8,128)(2,1)}, bf16[2,512,256]{2,1,0:T(8,128)(2,1)S(1)}, u32[]{:S(2)}) copy-start(bf16[2,512,256]{2,1,0:T(8,128)(2,1)S(1)} %collective-permute-done.1.ra) | copy-start | bytes 1572868
  187.2 0.8 copy-start.5
  187.3 1.2 copy-start.1
  257.7 78.8 %collective-permute-start.5 = (bf16[512,1024]{1,0:T(8,128)(2,1)}, bf16[512,1024]{1,0:T(8,128)(2,1)S(1)}, u32[]{:S(2)}, u32[]{:S(2)}) collective-permute-start(bf16[512,1024]{1,0:T(8,128)(2,1)} %shard_map.155), channel_id=1, source_target_pairs={{0,1},{1,0},{2,3},{3,2},{4,5},{5,4},{6,7},{7,6},{8,9},{9,8},{10,11... | collective-permute-start | bytes 3145736 | tf_op jit(solution)/shard_map/ppermute | solution.py:195
  303.5 33.0 %collective-permute-start.6 = (bf16[512,1024]{1,0:T(8,128)(2,1)}, bf16[512,1024]{1,0:T(8,128)(2,1)S(1)}, u32[]{:S(2)}, u32[]{:S(2)}) collective-permute-start(bf16[512,1024]{1,0:T(8,128)(2,1)} %shard_map.156), channel_id=1, source_target_pairs={{0,1},{1,0},{2,3},{3,2},{4,5},{5,4},{6,7},{7,6},{8,9},{9,8},{10,11... | collective-permute-start | bytes 3145736 | tf_op jit(solution)/shard_map/ppermute | solution.py:195
  336.4 1.0 copy-start.6
  336.4 1.3 copy-start.7
Sparse Core Ops, SparseCore 0:
  9.5 53.0 all-gather.5
  64.8 39.9 all-gather.7
  107.1 99.1 all-gather.9
  208.4 43.6 all-gather.11
  254.3 43.6 all-gather.13

commit v2 on v0

v2 whole, which is shorter than its diff:
```python
import functools

import jax
import jax.numpy as jnp
from jax import lax
from jax.experimental import pallas as pl
from jax.experimental.pallas import tpu as pltpu
from jax.sharding import PartitionSpec as P

EPS = 1e-06
SEGMENTS = 8
PIECES = 4
TOKEN_PIECES = 4
SCAN_TICKS = 8
MOST_VMEM = 67043328
VMEM_BYTES = 60 * 1024 * 1024


def normed(values, gain):
    factor = lax.rsqrt(jnp.mean(values * values, axis=-1, keepdims=True) + EPS)
    return values * factor * gain


def one_minus_exp(y, exp_y):
    series = 1.0 + y * (1.0 / 8.0)
    for order in (7, 6, 5, 4, 3, 2):
        series = 1.0 + y * (1.0 / order) * series
    return jnp.where(y > -0.5, -y * series, 1.0 - exp_y)


def mixer_kernel(
    x_ref, wb_ref, wg_ref, conv_ref, gates_ref, coef_ref, out_ref, pad, gel, a0, u0, a1, u1
):
    length, width = out_ref.shape
    group = gates_ref.shape[1]
    rows = 256
    pad[0:8, :] = jnp.zeros((8, width), jnp.float32)
    pad[8 + length : 16 + length, :] = jnp.zeros((8, width), jnp.float32)
    sources = ((x_ref, 0),)
    for source, base in sources:
        for start in range(0, source.shape[0], rows):
            piece = source[start : start + rows, :]
            branch = jnp.dot(piece, wb_ref[...], preferred_element_type=jnp.float32)
            gelu_in = jnp.dot(piece, wg_ref[...], preferred_element_type=jnp.float32)
            at = pl.multiple_of(base + start, rows)
            pad[pl.ds(8 + at, rows), :] = branch.astype(jnp.bfloat16).astype(jnp.float32)
            gel[pl.ds(at, rows), :] = jax.nn.gelu(
                gelu_in.astype(jnp.bfloat16).astype(jnp.float32)
            )

    for part in range(width // group):
        cols = slice(part * group, (part + 1) * group)
        taps = conv_ref[:, cols].astype(jnp.float32)
        coef = coef_ref[:, cols]
        for start in range(0, length, rows):
            summed = taps[0:1] * pad[6 + start : 6 + start + rows, cols]
            for j in range(1, 4):
                summed = summed + taps[j : j + 1] * pad[6 + j + start : 6 + j + start + rows, cols]
            conv = summed.astype(jnp.bfloat16)
            wide = conv.astype(jnp.float32)
            for d, (a_ref, u_ref) in enumerate(((a0, u0), (a1, u1))):
                gate = jnp.dot(
                    conv,
                    gates_ref[part, :, 2 * d * group : 2 * (d + 1) * group],
                    preferred_element_type=jnp.float32,
                )
                rate = jax.nn.sigmoid(gate[:, :group])
                inflow = jax.nn.sigmoid(gate[:, group:])
                log_retain = rate * coef[d : d + 1]
                retain = jnp.exp(log_retain)
                left = one_minus_exp(2.0 * log_retain, retain * retain)
                a_ref[part, start : start + rows, :] = retain
                u_ref[part, start : start + rows, :] = jnp.sqrt(left) * inflow * wide

    steps = length // SEGMENTS

    def step(t, carry):
        out = []
        for (state, decayed), (a_ref, u_ref), at in (
            (carry[0], (a0, u0), t),
            (carry[1], (a1, u1), steps - 1 - t),
        ):
            where = pl.ds(at, SEGMENTS, stride=steps)
            nstate, ndecayed = [], []
            for c in range(n):
                retain = a_ref[c, where, :]
                h = retain * state[c] + u_ref[c, where, :]
                p = retain * decayed[c]
                u_ref[c, where, :] = h
                a_ref[c, where, :] = p
                nstate.append(h)
                ndecayed.append(p)
            out.append((tuple(nstate), tuple(ndecayed)))
        return tuple(out)

    n = width // group
    zero = tuple(jnp.zeros((SEGMENTS, group), jnp.float32) for c in range(n))
    one = tuple(jnp.ones((SEGMENTS, group), jnp.float32) for c in range(n))
    ended = lax.fori_loop(0, steps, step, ((zero, one), (zero, one)), unroll=8)
    for c in range(n):
        lanes = slice(c * group, (c + 1) * group)
        blank = jnp.zeros((1, group), jnp.float32)
        entry = [[None] * SEGMENTS, [None] * SEGMENTS]
        for d, order in ((0, range(SEGMENTS)), (1, range(SEGMENTS - 1, -1, -1))):
            carry = blank
            for s in order:
                entry[d][s] = carry
                carry = ended[d][0][c][s : s + 1] + ended[d][1][c][s : s + 1] * carry
        for s in range(SEGMENTS):
            span = slice(s * steps, (s + 1) * steps)
            forward = u0[c, span, :] + a0[c, span, :] * entry[0][s]
            backward = u1[c, span, :] + a1[c, span, :] * entry[1][s]
            out_ref[span, lanes] = (gel[span, lanes] * (forward + backward)).astype(jnp.bfloat16)


def mixer(x, weights, conv_weight, w_rec, w_inp, decay):
    length, model = x.shape
    channels = conv_weight.shape[1]
    group = w_rec.shape[2]
    width = min(256, channels)
    count = channels // width
    gates = jnp.concatenate([w_rec[0], w_inp[0], w_rec[1], w_inp[1]], axis=-1)
    coef = -8.0 * jax.nn.softplus(-decay)
    f32 = functools.partial(pltpu.VMEM, dtype=jnp.float32)
    return pl.pallas_call(
        mixer_kernel,
        grid=(count,),
        out_shape=jax.ShapeDtypeStruct((length, channels), jnp.bfloat16),
        in_specs=[
            pl.BlockSpec((length, model), lambda j: (0, 0)),
            pl.BlockSpec((model, width), lambda j: (0, j)),
            pl.BlockSpec((model, width), lambda j: (0, count + j)),
            pl.BlockSpec((4, width), lambda j: (0, j)),
            pl.BlockSpec((width // group, group, 4 * group), lambda j: (j, 0, 0)),
            pl.BlockSpec((2, width), lambda j: (0, j)),
        ],
        out_specs=pl.BlockSpec((length, width), lambda j: (0, j)),
        scratch_shapes=[f32((length + 16, width)), f32((length, width))]
        + [f32((width // group, length, group)) for i in range(4)],
        compiler_params=pltpu.CompilerParams(vmem_limit_bytes=VMEM_BYTES),
        cost_estimate=pl.CostEstimate(
            flops=4 * length * model * channels + 16 * length * group * channels * 8,
            bytes_accessed=2 * (length * model + 2 * model * channels + length * channels),
            transcendentals=12 * length * channels,
        ),
    )(x, weights, weights, conv_weight, gates, coef)


def ffn_kernel(x_ref, gate_ref, up_ref, down_ref, out_ref, total):
    step = pl.program_id(0)
    gate = jnp.dot(x_ref[...], gate_ref[...], preferred_element_type=jnp.float32)
    up = jnp.dot(x_ref[...], up_ref[...], preferred_element_type=jnp.float32)
    hidden = (jax.nn.silu(gate) * up).astype(jnp.bfloat16)
    partial = lax.dot_general(
        hidden, down_ref[...], (((1,), (1,)), ((), ())), preferred_element_type=jnp.float32
    )

    @pl.when(step == 0)
    def _():
        total[...] = partial

    @pl.when(step > 0)
    def _():
        total[...] += partial

    @pl.when(step == pl.num_programs(0) - 1)
    def _():
        out_ref[...] = total[...].astype(jnp.bfloat16)


def ffn(x, weights):
    rows, model = x.shape
    units = weights.shape[1] // 3
    width = 256 if units % 256 == 0 else 128
    count = units // width
    return pl.pallas_call(
        ffn_kernel,
        grid=(count,),
        out_shape=jax.ShapeDtypeStruct((rows, model), jnp.bfloat16),
        in_specs=[
            pl.BlockSpec((rows, model), lambda j: (0, 0)),
            pl.BlockSpec((model, width), lambda j: (0, j)),
            pl.BlockSpec((model, width), lambda j: (0, count + j)),
            pl.BlockSpec((model, width), lambda j: (0, 2 * count + j)),
        ],
        out_specs=pl.BlockSpec((rows, model), lambda j: (0, 0)),
        scratch_shapes=[pltpu.VMEM((rows, model), jnp.float32)],
        compiler_params=pltpu.CompilerParams(vmem_limit_bytes=VMEM_BYTES),
        cost_estimate=pl.CostEstimate(
            flops=6 * rows * model * units,
            bytes_accessed=2 * (2 * rows * model + 3 * model * units),
            transcendentals=rows * units,
        ),
    )(x, weights, weights, weights)


def matmul_t(rows, weight_t):
    return lax.dot_general(
        rows, weight_t, (((1,), (1,)), ((), ())), preferred_element_type=jnp.float32
    )


def ring_chip(place, chips):
    half = chips // 2
    turned = place // half
    row = place * (1 - turned) + (chips - 1 - place) * turned
    return row * 2 + turned


def remote(src, dst, sent, landed, device):
    return pltpu.make_async_remote_copy(
        src_ref=src,
        dst_ref=dst,
        send_sem=sent,
        recv_sem=landed,
        device_id=device,
        device_id_type=pl.DeviceIdType.MESH,
    )


def branch_on(condition, body):
    if isinstance(condition, bool):
        if condition:
            body()
    else:
        pl.when(condition)(body)


def both(first, second):
    if isinstance(first, bool) and isinstance(second, bool):
        return first and second
    return jnp.logical_and(first, second)


def either(first, second):
    if isinstance(first, bool) and isinstance(second, bool):
        return first or second
    return jnp.logical_or(first, second)


def layer_kernel(
    size,
    tokens_ref,
    shards_ref,
    gains_ref,
    conv_ref,
    gates_ref,
    coef_ref,
    out_ref,
    full,
    far_out,
    other,
    xm,
    pad,
    gel,
    a0,
    u0,
    a1,
    u1,
    hid,
    got,
    total,
    hf,
    part,
    back,
    ring_send,
    ring_recv,
    near_send,
    near_recv,
    own_sem,
    tok_send,
    tok_recv,
    cross_send,
    cross_recv,
    share_send,
    share_recv,
    hid_send,
    hid_recv,
    back_send,
    back_recv,
):
    chips = size // 2
    reach = chips // 2
    stages, depth, cols = shards_ref.shape
    prow = depth // PIECES
    half, model = tokens_ref.shape
    blocks, width = conv_ref.shape[0], conv_ref.shape[2]
    channels = blocks * width
    group = gates_ref.shape[1]
    units = hf.shape[2]
    span = 2 * depth

    me = lax.axis_index("fs")
    core = me % 2
    turned = (me // 2) % 2
    row = me // 4
    place = row * (1 - turned) + (chips - 1 - row) * turned
    column = lax.axis_index("tp")

    def chip_at(offset):
        return ring_chip((place + chips + offset) % chips, chips)

    targets = ({"fs": chip_at(1) * 2 + core}, {"fs": chip_at(-1) * 2 + core})
    partner = {"fs": me + 1 - 2 * core}
    across = {"tp": 1 - column}

    barrier = pltpu.get_barrier_semaphore()
    for device in (*targets, partner, across):
        pl.semaphore_signal(barrier, inc=1, device_id=device, device_id_type=pl.DeviceIdType.MESH)
    pl.semaphore_wait(barrier, 4)

    def piece(g, chip, p):
        start = pl.multiple_of((chip * 2 + core) * depth + p * prow, prow)
        return full.at[g, pl.ds(start, prow), :]

    def shard_rows(g, chip, which):
        start = pl.multiple_of((chip * 2 + which) * depth, depth)
        return full.at[g, pl.ds(start, depth), :]

    def start_piece(g, p):
        src = shards_ref.at[g, pl.ds(pl.multiple_of(p * prow, prow), prow), :]
        dst = piece(g, me // 2, p)
        for way in range(2):
            remote(src, dst, ring_send.at[way, g, 0], ring_recv.at[way, g, 0, p], targets[way]).start()
        remote(src, dst, near_send.at[g, 0], near_recv.at[g, 0], partner).start()

    def pass_piece(g, s, p):
        for way in range(2):
            ref = piece(g, chip_at(-s if way == 0 else s), p)
            slot = 2 * s - 1 + way
            remote(
                ref, ref, ring_send.at[way, g, s], ring_recv.at[way, g, s - 1, p], targets[way]
            ).wait_recv()

            def forward():
                remote(
                    ref, ref, ring_send.at[way, g, s], ring_recv.at[way, g, s, p], targets[way]
                ).start()

            mine = p < PIECES // 2 if way == 0 else p >= PIECES // 2
            branch_on(either(s < reach - 1, mine), forward)
            remote(ref, ref, near_send.at[g, slot], near_recv.at[g, slot], partner).start()

    def last_piece(g, q):
        for way in range(2):
            p = q + way * (PIECES // 2)
            ref = piece(g, chip_at(reach), p)
            remote(
                ref,
                ref,
                ring_send.at[way, g, reach - 1],
                ring_recv.at[way, g, reach - 1, p],
                targets[way],
            ).wait_recv()
            remote(ref, ref, near_send.at[g, chips - 1], near_recv.at[g, chips - 1], partner).start()

    head = PIECES + PIECES // 2
    per_stage = head + (reach - 1) * PIECES

    def tick(e):
        g = e // per_stage
        k = e % per_stage
        branch_on(both(k < PIECES, g < stages), lambda: start_piece(g, k))
        branch_on(
            both(both(k >= PIECES, k < head), g > 0), lambda: last_piece(g - 1, k - PIECES)
        )
        branch_on(
            both(k >= head, g < stages),
            lambda: pass_piece(g, (k - head) // PIECES + 1, (k - head) % PIECES),
        )

    def ticks(first, last):
        @pl.loop(first, last)
        def _(e):
            tick(e)

    def near_wait(g, slot):
        ref = shard_rows(g, 0, 0)
        remote(ref, ref, near_send.at[g, slot], near_recv.at[g, slot], partner).wait_recv()

    token_rows = half // TOKEN_PIECES
    for i in range(TOKEN_PIECES):
        rows = pl.ds(i * token_rows, token_rows)
        remote(tokens_ref.at[rows, :], other.at[rows, :], tok_send.at[0], tok_recv.at[i], across).start()
    ticks(0, PIECES)
    own_copies = [
        pltpu.make_async_copy(shards_ref.at[g], shard_rows(g, me // 2, core), own_sem.at[g])
        for g in range(stages)
    ]
    for copy in own_copies:
        copy.start()

    chunk = 128

    def norm_rows(source, h, at):
        rows = pl.ds(at, chunk)
        values = source[rows, :].astype(jnp.float32)
        xm[h, rows, :] = normed(values, gains_ref[0:1, :]).astype(jnp.bfloat16)

    @pl.loop(0, half // chunk)
    def _(i):
        norm_rows(tokens_ref, 0, pl.multiple_of(i * chunk, chunk))

    length = 2 * half
    for b in range(blocks):
        pad[b, 0:8, :] = jnp.zeros((8, width), jnp.float32)
        pad[b, 8 + length : 16 + length, :] = jnp.zeros((8, width), jnp.float32)

    done0 = per_stage + head
    ticks(PIECES, done0)
    for copy in own_copies:
        copy.wait()

    @pl.loop(0, chips)
    def _(slot):
        near_wait(0, slot)

    @pl.loop(0, chips)
    def _(chip):
        src = shard_rows(0, chip, core).at[:, pl.ds(2 * channels, channels)]
        dst = far_out.at[pl.ds(pl.multiple_of((chip * 2 + core) * depth, depth), depth), :]
        remote(src, dst, cross_send.at[0], cross_recv.at[0], across).start()

    prows = 256

    @pl.loop(0, 2)
    def _(h):
        @pl.loop(0, half // prows)
        def _(i):
            at = pl.multiple_of(i * prows, prows)

            @pl.when(h == 1)
            def _():
                @pl.loop(0, prows // token_rows)
                def _(q):
                    n = i * (prows // token_rows) + q
                    rows = pl.ds(pl.multiple_of(n * token_rows, token_rows), token_rows)
                    remote(
                        tokens_ref.at[rows, :],
                        other.at[rows, :],
                        tok_send.at[0],
                        tok_recv.at[n],
                        across,
                    ).wait_recv()

                @pl.loop(0, prows // chunk)
                def _(q):
                    norm_rows(other, 1, pl.multiple_of(at + q * chunk, chunk))

            x = xm[h, pl.ds(at, prows), :]
            side = jnp.where(h == 0, column, 1 - column)
            base = pl.multiple_of(8 + side * half + at, 8)
            for b in range(blocks):
                lanes = slice(b * width, (b + 1) * width)
                branch = jnp.dot(x, full[0, :, lanes], preferred_element_type=jnp.float32)
                pad[b, pl.ds(base, prows), :] = branch.astype(jnp.bfloat16).astype(jnp.float32)
                lanes = slice(channels + b * width, channels + (b + 1) * width)
                gelu_in = jnp.dot(x, full[0, :, lanes], preferred_element_type=jnp.float32)
                gelu_in = gelu_in.astype(jnp.bfloat16).astype(jnp.float32)
                gel[h, b, pl.ds(at, prows), :] = jax.nn.gelu(gelu_in).astype(jnp.bfloat16)
            tick(done0 + h * 4 + i * 2)
            tick(done0 + h * 4 + i * 2 + 1)

    scan0 = done0 + 8
    parts = width // group
    steps = length // SEGMENTS
    crows = 256

    def hid_copy(b):
        return remote(hid.at[b], got.at[b], hid_send.at[b], hid_recv.at[b], across)

    @pl.loop(0, blocks)
    def _(b):
        at = scan0 + b * SCAN_TICKS
        count = 0
        for n in range(parts):
            lanes = slice(n * group, (n + 1) * group)
            taps = conv_ref[b, :, lanes].astype(jnp.float32)
            coef = coef_ref[b, :, lanes]
            for start in range(0, length, crows):
                summed = taps[0:1] * pad[b, 6 + start : 6 + start + crows, lanes]
                for j in range(1, 4):
                    first = 6 + j + start
                    summed = summed + taps[j : j + 1] * pad[b, first : first + crows, lanes]
                conv = summed.astype(jnp.bfloat16)
                wide = conv.astype(jnp.float32)
                for d, (a_ref, u_ref) in enumerate(((a0, u0), (a1, u1))):
                    gate = jnp.dot(
                        conv,
                        gates_ref[b * parts + n, :, 2 * d * group : 2 * (d + 1) * group],
                        preferred_element_type=jnp.float32,
                    )
                    rate = jax.nn.sigmoid(gate[:, :group])
                    inflow = jax.nn.sigmoid(gate[:, group:])
                    log_retain = rate * coef[d : d + 1]
                    retain = jnp.exp(log_retain)
                    left = one_minus_exp(2.0 * log_retain, retain * retain)
                    a_ref[n, start : start + crows, :] = retain
                    u_ref[n, start : start + crows, :] = jnp.sqrt(left) * inflow * wide
                if (start // crows) % 2 == 1 and count < SCAN_TICKS:
                    tick(at + count)
                    count += 1

        def step(t, carry):
            out = []
            for (state, decayed), (a_ref, u_ref), when in (
                (carry[0], (a0, u0), t),
                (carry[1], (a1, u1), steps - 1 - t),
            ):
                where = pl.ds(when, SEGMENTS, stride=steps)
                nstate, ndecayed = [], []
                for n in range(parts):
                    retain = a_ref[n, where, :]
                    h = retain * state[n] + u_ref[n, where, :]
                    p = retain * decayed[n]
                    u_ref[n, where, :] = h
                    a_ref[n, where, :] = p
                    nstate.append(h)
                    ndecayed.append(p)
                out.append((tuple(nstate), tuple(ndecayed)))
            return tuple(out)

        zero = tuple(jnp.zeros((SEGMENTS, group), jnp.float32) for n in range(parts))
        one = tuple(jnp.ones((SEGMENTS, group), jnp.float32) for n in range(parts))
        ended = ((zero, one), (zero, one))
        for run in range(2):
            low, high = run * steps // 2, (run + 1) * steps // 2
            ended = lax.fori_loop(low, high, step, ended, unroll=8)
            tick(at + count)
            count += 1
        per_half = SEGMENTS // 2
        for n in range(parts):
            lanes = slice(n * group, (n + 1) * group)
            blank = jnp.zeros((1, group), jnp.float32)
            entry = [[None] * SEGMENTS, [None] * SEGMENTS]
            for d, order in ((0, range(SEGMENTS)), (1, range(SEGMENTS - 1, -1, -1))):
                carry = blank
                for s in order:
                    entry[d][s] = carry
                    carry = ended[d][0][n][s : s + 1] + ended[d][1][n][s : s + 1] * carry
            for s in range(SEGMENTS):
                rows = slice(s * steps, (s + 1) * steps)
                local = slice((s % per_half) * steps, (s % per_half + 1) * steps)
                which = jnp.where(column == s // per_half, 0, 1)
                forward = u0[n, rows, :] + a0[n, rows, :] * entry[0][s]
                backward = u1[n, rows, :] + a1[n, rows, :] * entry[1][s]
                gate = gel[which, b, local, lanes].astype(jnp.float32)
                hid[b, which, local, lanes] = (gate * (forward + backward)).astype(jnp.bfloat16)
            tick(at + count)
            count += 1
        hid_copy(b).start()
        assert count == SCAN_TICKS

    out0 = scan0 + blocks * SCAN_TICKS

    ref = far_out.at[pl.ds(0, chips * depth), :]
    remote(ref, ref, cross_send.at[0], cross_recv.at[0], across).wait_recv()

    @pl.loop(0, chips)
    def _(chip):
        ref = far_out.at[pl.ds(pl.multiple_of((chip * 2 + core) * depth, depth), depth), :]
        remote(ref, ref, share_send.at[0], share_recv.at[0], partner).start()

    ocols = 256

    def mixed(h, use_own, use_far, e0):
        mine = jnp.concatenate([hid[b, h] for b in range(blocks)], axis=1)
        theirs = jnp.concatenate([got[b, 1 - h] for b in range(blocks)], axis=1)

        @pl.loop(0, model // ocols)
        def _(n):
            rows = pl.ds(pl.multiple_of(n * ocols, ocols), ocols)
            lanes = rows
            summed = 0.0
            if use_own:
                summed = matmul_t(mine, full[0, rows, 2 * channels : 3 * channels])
            else:
                summed = total[:, lanes]
            if use_far:
                summed = summed + matmul_t(theirs, far_out[rows, :])
            total[:, lanes] = summed
            if e0 is not None:

                @pl.when(n % 2 == 1)
                def _():
                    tick(e0 + n // 2)

    def settle(h, source):
        @pl.loop(0, half // chunk)
        def _(i):
            rows = pl.ds(pl.multiple_of(i * chunk, chunk), chunk)
            stream = source[rows, :].astype(jnp.float32)
            residual = stream + normed(total[rows, :], gains_ref[1:2, :])
            residual = residual.astype(jnp.bfloat16)
            if h == 0:
                out_ref[rows, :] = residual
            middle = normed(residual.astype(jnp.float32), gains_ref[2:3, :])
            xm[h, rows, :] = middle.astype(jnp.bfloat16)

    mixed(1, True, False, out0)
    ref = far_out.at[pl.ds(0, chips * depth), :]
    remote(ref, ref, share_send.at[0], share_recv.at[0], partner).wait_recv()
    for b in range(blocks):
        hid_copy(b).wait_recv()
    mixed(1, False, True, out0 + 4)
    settle(1, other)
    ffn0 = out0 + 8

    ucols = 256
    unit_chunks = units // 2 // ucols

    def expand(g, h, c):
        x = xm[h]
        lanes = pl.ds(pl.multiple_of(c * ucols, ucols), ucols)
        gate = jnp.dot(x, full[g, :, lanes], preferred_element_type=jnp.float32)
        lanes = pl.ds(pl.multiple_of(units // 2 + c * ucols, ucols), ucols)
        up = jnp.dot(x, full[g, :, lanes], preferred_element_type=jnp.float32)
        lanes = pl.ds(pl.multiple_of((g - 1) * (units // 2) + c * ucols, ucols), ucols)
        hf[h, :, lanes] = (jax.nn.silu(gate) * up).astype(jnp.bfloat16)

    first_done = 2 * per_stage + head
    second_done = 3 * per_stage + head
    ticks(ffn0, first_done) if ffn0 < first_done else None
    ffn1 = max(ffn0, first_done)

    @pl.loop(0, chips)
    def _(slot):
        near_wait(1, slot)

    @pl.loop(0, unit_chunks)
    def _(c):
        expand(1, 1, c)
        tick(ffn1 + c)

    ffn2 = ffn1 + unit_chunks
    ticks(ffn2, second_done)

    @pl.loop(0, chips)
    def _(slot):
        near_wait(2, slot)

    @pl.loop(0, unit_chunks)
    def _(c):
        expand(2, 1, c)
        tick(second_done + c)

    def feature_chip(slot):
        d = (slot + 1) // 2
        return chip_at(jnp.where(slot % 2 == 1, -d, d))

    def partial_of(h, chip):
        weight = full[stages - 1, pl.ds(pl.multiple_of(chip * span, span), span), :]
        return matmul_t(hf[h], weight)

    def back_copy(slot):
        chip = feature_chip(slot)
        return remote(part.at[chip], back.at[chip], back_send.at[slot], back_recv.at[slot], across)

    down0 = second_done + unit_chunks
    distance1 = (stages - 1) * per_stage + head + PIECES

    @pl.loop(0, chips)
    def _(slot):
        @pl.when(slot == 1)
        def _():
            ticks(down0, distance1)

        @pl.when(jnp.logical_and(slot % 2 == 1, jnp.logical_and(slot > 1, slot < chips - 1)))
        def _():
            @pl.loop(0, PIECES)
            def _(i):
                tick(distance1 + (slot // 2 - 1) * PIECES + i)

        @pl.when(slot == chips - 1)
        def _():
            ticks(stages * per_stage + PIECES, stages * per_stage + head)

        near_wait(stages - 1, slot)
        chip = feature_chip(slot)
        part[chip] = partial_of(1, chip).astype(jnp.bfloat16)
        back_copy(slot).start()

    mixed(0, True, True, None)
    settle(0, tokens_ref)

    @pl.loop(0, 2 * unit_chunks)
    def _(c):
        expand(1 + c // unit_chunks, 0, c % unit_chunks)

    @pl.loop(0, chips)
    def _(chip):
        lanes = pl.ds(pl.multiple_of(chip * span, span), span)
        total[:, lanes] = partial_of(0, chip).astype(jnp.bfloat16).astype(jnp.float32)

    @pl.loop(0, chips)
    def _(slot):
        back_copy(slot).wait_recv()

    @pl.loop(0, half // chunk)
    def _(i):
        rows = pl.ds(pl.multiple_of(i * chunk, chunk), chunk)
        came = jnp.concatenate([back[chip, rows, :] for chip in range(chips)], axis=1)
        summed = total[rows, :] + came.astype(jnp.float32)
        middle = out_ref[rows, :].astype(jnp.float32)
        out_ref[rows, :] = (middle + normed(summed, gains_ref[3:4, :])).astype(jnp.bfloat16)

    for g in range(stages):
        ref = shard_rows(g, 0, 0)
        for way in range(2):
            for s in range(reach):
                sent = ref if s < reach - 1 else full.at[g, pl.ds(0, depth // 2), :]
                remote(
                    sent, sent, ring_send.at[way, g, s], ring_recv.at[way, g, s, 0], targets[way]
                ).wait_send()
        for slot in range(chips):
            remote(ref, ref, near_send.at[g, slot], near_recv.at[g, slot], partner).wait_send()
    remote(tokens_ref, other, tok_send.at[0], tok_recv.at[0], across).wait_send()
    ref = far_out.at[pl.ds(0, chips * depth), :]
    remote(ref, ref, cross_send.at[0], cross_recv.at[0], across).wait_send()
    remote(ref, ref, share_send.at[0], share_recv.at[0], partner).wait_send()
    for b in range(blocks):
        hid_copy(b).wait_send()
    for slot in range(chips):
        back_copy(slot).wait_send()


def paired_device(
    tokens,
    pre_mix_gain,
    post_mix_gain,
    pre_ffn_gain,
    post_ffn_gain,
    w_branch,
    w_gelu,
    conv_weight,
    w_rec,
    w_inp,
    decay,
    out_weight_t,
    w_gate,
    w_up,
    down_weight_t,
):
    half, model = tokens.shape
    depth, channels = w_branch.shape
    units = w_gate.shape[1]
    size = lax.axis_size("fs")
    chips = size // 2
    group = w_rec.shape[2]
    width = min(256, channels)
    blocks = channels // width
    length = 2 * half
    cut = units // 2
    shards = jnp.stack(
        [
            jnp.concatenate([w_branch, w_gelu, out_weight_t], axis=1),
            jnp.concatenate([w_gate[:, :cut], w_up[:, :cut]], axis=1),
            jnp.concatenate([w_gate[:, cut:], w_up[:, cut:]], axis=1),
            down_weight_t,
        ]
    )
    gains = jnp.stack([pre_mix_gain, post_mix_gain, pre_ffn_gain, post_ffn_gain])
    conv = conv_weight.reshape(4, blocks, width).swapaxes(0, 1)
    gates = jnp.concatenate([w_rec[0], w_inp[0], w_rec[1], w_inp[1]], axis=-1)
    coef = (-8.0 * jax.nn.softplus(-decay)).reshape(2, blocks, width).swapaxes(0, 1)
    bf16 = functools.partial(pltpu.VMEM, dtype=jnp.bfloat16)
    f32 = functools.partial(pltpu.VMEM, dtype=jnp.float32)
    dma = pltpu.SemaphoreType.DMA
    stages = shards.shape[0]
    reach = chips // 2
    vmem = pl.BlockSpec(memory_space=pltpu.VMEM)
    return pl.pallas_call(
        functools.partial(layer_kernel, size),
        out_shape=jax.ShapeDtypeStruct((half, model), jnp.bfloat16),
        in_specs=[vmem] * 6,
        out_specs=vmem,
        scratch_shapes=[
            bf16((stages, model, shards.shape[2])),
            bf16((model, channels)),
            bf16((half, model)),
            bf16((2, half, model)),
            f32((blocks, length + 16, width)),
            bf16((2, blocks, half, width)),
        ]
        + [f32((width // group, length, group)) for i in range(4)]
        + [
            bf16((blocks, 2, half, width)),
            bf16((blocks, 2, half, width)),
            f32((half, model)),
            bf16((2, half, units)),
            bf16((chips, half, 2 * depth)),
            bf16((chips, half, 2 * depth)),
            dma((2, stages, reach)),
            dma((2, stages, reach, PIECES)),
            dma((stages, chips)),
            dma((stages, chips)),
            dma((stages,)),
            dma((1,)),
            dma((TOKEN_PIECES,)),
            dma((1,)),
            dma((1,)),
            dma((1,)),
            dma((1,)),
            dma((blocks,)),
            dma((blocks,)),
            dma((chips,)),
            dma((chips,)),
        ],
        compiler_params=pltpu.CompilerParams(
            collective_id=0, has_side_effects=True, vmem_limit_bytes=MOST_VMEM
        ),
        cost_estimate=pl.CostEstimate(
            flops=1 << 34, bytes_accessed=1 << 26, transcendentals=1 << 24
        ),
    )(tokens, shards, gains, conv, gates, coef)


def wide_device(
    tokens,
    pre_mix_gain,
    post_mix_gain,
    pre_ffn_gain,
    post_ffn_gain,
    w_branch,
    w_gelu,
    conv_weight,
    w_rec,
    w_inp,
    decay,
    out_weight_t,
    w_gate,
    w_up,
    down_weight_t,
):
    channels = conv_weight.shape[1]
    mix_shard = jnp.concatenate([w_branch, w_gelu, out_weight_t], axis=1)
    ffn_shard = jnp.concatenate([w_gate, w_up, down_weight_t], axis=1)
    stream = tokens.astype(jnp.float32)
    normed_in = normed(stream, pre_mix_gain).astype(jnp.bfloat16)
    mix_all = lax.all_gather(mix_shard, "fs", axis=0, tiled=True)
    whole = lax.all_gather(normed_in, "tp", axis=0, tiled=True)
    ffn_all = lax.all_gather(ffn_shard, "fs", axis=0, tiled=True)
    out_own = mix_all[:, 2 * channels :]
    hidden = mixer(whole, mix_all, conv_weight, w_rec, w_inp, decay)
    own_hidden = lax.all_to_all(hidden, "tp", split_axis=0, concat_axis=1, tiled=True)
    out_whole = lax.all_gather(out_own, "tp", axis=1, tiled=True)
    mixer_sum = matmul_t(own_hidden, out_whole)
    residual = (stream + normed(mixer_sum, post_mix_gain)).astype(jnp.bfloat16)
    middle = residual.astype(jnp.float32)
    normed_mid = normed(middle, pre_ffn_gain).astype(jnp.bfloat16)
    all_mid = lax.all_gather(normed_mid, "tp", axis=0, tiled=True)
    ffn_sum = lax.psum_scatter(
        ffn(all_mid, ffn_all), "tp", scatter_dimension=0, tiled=True
    ).astype(jnp.float32)
    return (middle + normed(ffn_sum, post_ffn_gain)).astype(jnp.bfloat16)


def solution(mesh):
    return jax.shard_map(
        paired_device if mesh.shape["tp"] == 2 else wide_device,
        mesh=mesh,
        in_specs=(
            P(("fs", "tp"), None),
            P(),
            P(),
            P(),
            P(),
            P("fs", "tp"),
            P("fs", "tp"),
            P(None, "tp"),
            P(None, "tp", None, None),
            P(None, "tp", None, None),
            P(None, "tp"),
            P("fs", "tp"),
            P("fs", "tp"),
            P("fs", "tp"),
            P("fs", "tp"),
        ),
        out_specs=P(("fs", "tp"), None),
        check_vma=False,
    )
```

time: 242 us -> 174 us (0.72)
  waiting for transfers between devices: 67.7 us -> 0 us
  Pallas kernels: 125 us -> 164 us
  between operations: 13.6 us -> 0.08 us
  other arithmetic: 17.5 us -> 6.05 us
  starting transfers between devices: 6.26 us -> 0 us
  matrix products: 4.58 us -> 0 us
    ppermute x7 -> x0, waiting for transfers between devices: 52.4 us -> none  [the longest x6 51.9 us: swap(): return lax.ppermute(values, 'tp', [(0, 1), (1, 0)])]
    pallas_call x5 -> x1, Pallas kernels: 125 us -> 164 us  [paired_device(): pl.pallas_call(functools.partial(layer_kernel, size), out_shape=jax.Shape...]
    all_gather x1 -> x0, waiting for transfers between devices: 15.3 us -> none  [per_device(): ffn_all = lax.all_gather(ffn_shard, 'fs', axis=0, tiled=True)]
    convert_element_type x3 -> x0, other arithmetic: 8.17 us -> none  [the longest x1 4.17 us: per_device(): return (middle + normed(ffn_sum, post_ffn_gain)).astype(jnp.bfloat16)]
    ppermute x7 -> x0, starting transfers between devices: 6.26 us -> none  [the longest x6 6.19 us: swap(): return lax.ppermute(values, 'tp', [(0, 1), (1, 0)])]
    reduce_sum x3 -> x0, other arithmetic: 5.76 us -> none  [normed(): factor = lax.rsqrt(jnp.mean(values * values, axis=-1, keepdims=True) + EPS)]
    dot_general x2 -> x0, matrix products: 4.58 us -> none  [matmul_t(): lax.dot_general(rows, weight_t, (((1,), (1,)), ((), ())), preferred_eleme...]
    another operation x0 -> x4, other arithmetic: none -> 3.83 us  [the longest x3 2.45 us: paired_device(): jnp.stack([jnp.concatenate([w_branch, w_gelu, out_weight_t], axis=1), jnp...]
  transfers between devices with their start and end apart: 8 -> 0, of which waited for: 5 -> 0; matrix products, arithmetic and copies ran while one was open for 5% -> 0% of each run, Pallas kernels for 30% -> 0%
where the time goes in v2:
time: 174 us
  Pallas kernels  164 us (94%)
  other arithmetic  6.05 us (3%)
  local copies, waits for them, and re-layouts  4.34 us (2%)
    pallas_call x1, Pallas kernels, paired_device(): pl.pallas_call(functools.partial(layer_kernel, size), out_shape=jax.Shape...  164 us

profile of v2, /device:TPU:0, one launch (start us, length us, event | category | flops | bytes accessed | tf_op | source)
XLA Modules:
  0.0 174.1 jit_solution(5567536899164568884)
XLA Ops:
  0.0 0.0 copy-start.1
  0.0 1.4 fusion
  1.4 1.4 pad_maximum_fusion.2.gains_ref
  2.7 1.1 maximum_bitcast_fusion
  3.8 0.0 copy-start
  3.8 1.1 fusion.1
  4.9 0.0 copy-done.1
  5.0 0.1 maximum_bitcast_fusion.1
  5.0 0.0 copy-done
  5.0 0.0 copy-start.2
  5.0 0.0 copy-start.3
  5.1 1.3 pad_maximum_fusion.shards_ref
  6.4 0.0 copy-done.2
  6.4 0.0 copy-done.3
  6.4 0.9 pad_maximum_fusion.1.gates_ref
  7.3 163.6 %shard_map.145 = bf16[512,2048]{1,0:T(8,128)(2,1)} custom-call(bf16[512,2048]{1,0:T(8,128)(2,1)} %tokens_ref.1, bf16[4,128,1536]{2,1,0:T(8,128)(2,1)} %pad_maximum_fusion.shards_ref, f32[4,2048]{1,0:T(4,128)} %pad_maximum_fusion.2.gains_ref, bf16[2,4,256]{2,1,0:T(4,128)(2,1)} %bitcast.31, bf16[4,128,512]{2,1,0:T(8,128)(2,1)} %pad_maximum_fusion.1.gates_ref, ...), custom_call_target="tpu_custom_call" | custom-call | flops 17179869184 | bytes 67108864 | tf_op jit(solution)/shard_map/pallas_call | solution.py:772
  170.9 3.2 %copy.17 = bf16[512,2048]{1,0:T(8,128)(2,1)} copy(bf16[512,2048]{1,0:T(8,128)(2,1)} %shard_map.145) | data formatting | bytes 4194304
  (2 shorter events, 0.1 us)
Async XLA Ops:
  0.0 4.9 %copy-start.1 = (bf16[128,1536]{1,0:T(8,128)(2,1)S(1)}, bf16[128,1536]{1,0:T(8,128)(2,1)}, u32[]{:S(2)}) copy-start(bf16[128,1536]{1,0:T(8,128)(2,1)} %param.28) | copy-start | bytes 1179652
  3.8 1.2 copy-start
  5.0 1.4 copy-start.2
  5.0 1.4 copy-start.3

commit v3 on v2

--- a/solution.py
+++ b/solution.py
@@ -11,7 +11,7 @@
 SEGMENTS = 8
 PIECES = 4
 TOKEN_PIECES = 4
-SCAN_TICKS = 8
+SCAN_TICKS = 9
 MOST_VMEM = 67043328
 VMEM_BYTES = 60 * 1024 * 1024
 
@@ -241,12 +241,26 @@
 def layer_kernel(
     size,
     tokens_ref,
-    shards_ref,
-    gains_ref,
+    branch_ref,
+    gelu_ref,
+    outw_ref,
+    gate_ref,
+    up_ref,
+    down_ref,
+    gain0_ref,
+    gain1_ref,
+    gain2_ref,
+    gain3_ref,
+    taps_ref,
+    rec_ref,
+    inp_ref,
+    decay_ref,
+    out_ref,
+    mine,
+    gains,
     conv_ref,
     gates_ref,
     coef_ref,
-    out_ref,
     full,
     far_out,
     other,
@@ -268,6 +282,9 @@
     near_send,
     near_recv,
     own_sem,
+    small_sem,
+    mine_sem,
+    out_sem,
     tok_send,
     tok_recv,
     cross_send,
@@ -281,12 +298,13 @@
 ):
     chips = size // 2
     reach = chips // 2
-    stages, depth, cols = shards_ref.shape
+    stages = full.shape[0]
+    depth, channels = branch_ref.shape
     prow = depth // PIECES
     half, model = tokens_ref.shape
-    blocks, width = conv_ref.shape[0], conv_ref.shape[2]
-    channels = blocks * width
+    blocks, width = pad.shape[0], pad.shape[2]
     group = gates_ref.shape[1]
+    groups = gates_ref.shape[0]
     units = hf.shape[2]
     span = 2 * depth
 
@@ -304,6 +322,49 @@
     partner = {"fs": me + 1 - 2 * core}
     across = {"tp": 1 - column}
 
+    cut = units // 2
+    own_rows = pl.ds(pl.multiple_of(me * depth, depth), depth)
+
+    def own_part(g, source, lanes, at, sem):
+        place_at = full.at[g, own_rows, pl.ds(at, lanes.size)]
+        return pltpu.make_async_copy(source.at[:, lanes], place_at, own_sem.at[sem])
+
+    every = pl.ds(0, channels)
+    low, high = pl.ds(0, cut), pl.ds(cut, cut)
+    own_copies = [
+        [own_part(0, source, every, i * channels, i) for i, source in enumerate((branch_ref, gelu_ref, outw_ref))],
+        [own_part(1, gate_ref, low, 0, 3), own_part(1, up_ref, low, cut, 4)],
+        [own_part(2, gate_ref, high, 0, 5), own_part(2, up_ref, high, cut, 6)],
+        [own_part(3, down_ref, pl.ds(0, units), 0, 7)],
+    ]
+    for copy in own_copies[0]:
+        copy.start()
+    chunk = 128
+    mine_copies = []
+    for i in range(half // chunk):
+        rows = pl.ds(i * chunk, chunk)
+        mine_copies.append(
+            pltpu.make_async_copy(tokens_ref.at[rows, :], mine.at[rows, :], mine_sem.at[i])
+        )
+    for i, copy in enumerate(mine_copies):
+        copy.start()
+    small = [(source, gains.at[i]) for i, source in enumerate((gain0_ref, gain1_ref, gain2_ref, gain3_ref))]
+    small += [(taps_ref, conv_ref), (decay_ref, coef_ref)]
+    for n in range(groups):
+        for d in range(2):
+            for i, source in enumerate((rec_ref, inp_ref)):
+                lanes = pl.ds((2 * d + i) * group, group)
+                small.append((source.at[d, n], gates_ref.at[n, :, lanes]))
+    small = [
+        pltpu.make_async_copy(source, place_at, small_sem.at[i])
+        for i, (source, place_at) in enumerate(small)
+    ]
+    for copy in small:
+        copy.start()
+    for copies in own_copies[1:]:
+        for copy in copies:
+            copy.start()
+
     barrier = pltpu.get_barrier_semaphore()
     for device in (*targets, partner, across):
         pl.semaphore_signal(barrier, inc=1, device_id=device, device_id_type=pl.DeviceIdType.MESH)
@@ -318,8 +379,8 @@
         return full.at[g, pl.ds(start, depth), :]
 
     def start_piece(g, p):
-        src = shards_ref.at[g, pl.ds(pl.multiple_of(p * prow, prow), prow), :]
-        dst = piece(g, me // 2, p)
+        src = piece(g, me // 2, p)
+        dst = src
         for way in range(2):
             remote(src, dst, ring_send.at[way, g, 0], ring_recv.at[way, g, 0, p], targets[way]).start()
         remote(src, dst, near_send.at[g, 0], near_recv.at[g, 0], partner).start()
@@ -382,24 +443,25 @@
     for i in range(TOKEN_PIECES):
         rows = pl.ds(i * token_rows, token_rows)
         remote(tokens_ref.at[rows, :], other.at[rows, :], tok_send.at[0], tok_recv.at[i], across).start()
+    for copy in own_copies[0]:
+        copy.wait()
     ticks(0, PIECES)
-    own_copies = [
-        pltpu.make_async_copy(shards_ref.at[g], shard_rows(g, me // 2, core), own_sem.at[g])
-        for g in range(stages)
-    ]
-    for copy in own_copies:
-        copy.start()
-
-    chunk = 128
+    for copy in (*small, *mine_copies):
+        copy.wait()
+    for copies in own_copies[1:]:
+        for copy in copies:
+            copy.wait()
+    slow = coef_ref[...]
+    coef_ref[...] = -8.0 * (jnp.maximum(-slow, 0.0) + jnp.log1p(jnp.exp(-jnp.abs(slow))))
 
     def norm_rows(source, h, at):
         rows = pl.ds(at, chunk)
         values = source[rows, :].astype(jnp.float32)
-        xm[h, rows, :] = normed(values, gains_ref[0:1, :]).astype(jnp.bfloat16)
+        xm[h, rows, :] = normed(values, gains[0]).astype(jnp.bfloat16)
 
     @pl.loop(0, half // chunk)
     def _(i):
-        norm_rows(tokens_ref, 0, pl.multiple_of(i * chunk, chunk))
+        norm_rows(mine, 0, pl.multiple_of(i * chunk, chunk))
 
     length = 2 * half
     for b in range(blocks):
@@ -408,8 +470,6 @@
 
     done0 = per_stage + head
     ticks(PIECES, done0)
-    for copy in own_copies:
-        copy.wait()
 
     @pl.loop(0, chips)
     def _(slot):
@@ -458,16 +518,20 @@
                 gelu_in = jnp.dot(x, full[0, :, lanes], preferred_element_type=jnp.float32)
                 gelu_in = gelu_in.astype(jnp.bfloat16).astype(jnp.float32)
                 gel[h, b, pl.ds(at, prows), :] = jax.nn.gelu(gelu_in).astype(jnp.bfloat16)
-            tick(done0 + h * 4 + i * 2)
-            tick(done0 + h * 4 + i * 2 + 1)
-
-    scan0 = done0 + 8
+
+            @pl.when(h * (half // prows) + i < 2 * (half // prows) - 1)
+            def _():
+                ticks(done0 + h * 4 + i * 2, done0 + h * 4 + i * 2 + 2)
+
+    scan0 = done0 + 2 * (2 * (half // prows) - 1)
     parts = width // group
     steps = length // SEGMENTS
     crows = 256
 
-    def hid_copy(b):
-        return remote(hid.at[b], got.at[b], hid_send.at[b], hid_recv.at[b], across)
+    def hid_copy(b, h):
+        return remote(
+            hid.at[b, h], got.at[b, h], hid_send.at[b, h], hid_recv.at[b, h], across
+        )
 
     @pl.loop(0, blocks)
     def _(b):
@@ -475,8 +539,9 @@
         count = 0
         for n in range(parts):
             lanes = slice(n * group, (n + 1) * group)
-            taps = conv_ref[b, :, lanes].astype(jnp.float32)
-            coef = coef_ref[b, :, lanes]
+            table = pl.ds(pl.multiple_of(b * width + n * group, group), group)
+            taps = conv_ref[:, table].astype(jnp.float32)
+            coef = coef_ref[:, table]
             for start in range(0, length, crows):
                 summed = taps[0:1] * pad[b, 6 + start : 6 + start + crows, lanes]
                 for j in range(1, 4):
@@ -548,9 +613,13 @@
                 hid[b, which, local, lanes] = (gate * (forward + backward)).astype(jnp.bfloat16)
             tick(at + count)
             count += 1
-        hid_copy(b).start()
+        tick(at + count)
+        count += 1
         assert count == SCAN_TICKS
-
+        hid_copy(b, 0).start()
+
+    for b in range(blocks):
+        hid_copy(b, 1).start()
     out0 = scan0 + blocks * SCAN_TICKS
 
     ref = far_out.at[pl.ds(0, chips * depth), :]
@@ -563,48 +632,56 @@
 
     ocols = 256
 
-    def mixed(h, use_own, use_far, e0):
-        mine = jnp.concatenate([hid[b, h] for b in range(blocks)], axis=1)
-        theirs = jnp.concatenate([got[b, 1 - h] for b in range(blocks)], axis=1)
-
-        @pl.loop(0, model // ocols)
+    def mixed(h, own_blocks, far_blocks, fresh, e0=0, count=0):
+        left = [hid[b, h] for b in own_blocks]
+        left = jnp.concatenate(left, axis=1) if left else None
+        right = [got[b, 1 - h] for b in far_blocks]
+        right = jnp.concatenate(right, axis=1) if right else None
+        parts_n = model // ocols
+
+        @pl.loop(0, parts_n)
         def _(n):
             rows = pl.ds(pl.multiple_of(n * ocols, ocols), ocols)
             lanes = rows
-            summed = 0.0
-            if use_own:
-                summed = matmul_t(mine, full[0, rows, 2 * channels : 3 * channels])
-            else:
-                summed = total[:, lanes]
-            if use_far:
-                summed = summed + matmul_t(theirs, far_out[rows, :])
+            summed = None if fresh else total[:, lanes]
+            if left is not None:
+                first = 2 * channels + own_blocks[0] * width
+                term = matmul_t(left, full[0, rows, first : first + len(own_blocks) * width])
+                summed = term if summed is None else summed + term
+            if right is not None:
+                first = far_blocks[0] * width
+                term = matmul_t(right, far_out[rows, first : first + len(far_blocks) * width])
+                summed = term if summed is None else summed + term
             total[:, lanes] = summed
-            if e0 is not None:
-
-                @pl.when(n % 2 == 1)
+            if count:
+                every_n = parts_n // count
+
+                @pl.when(n % every_n == every_n - 1)
                 def _():
-                    tick(e0 + n // 2)
+                    tick(e0 + n // every_n)
 
     def settle(h, source):
         @pl.loop(0, half // chunk)
         def _(i):
             rows = pl.ds(pl.multiple_of(i * chunk, chunk), chunk)
             stream = source[rows, :].astype(jnp.float32)
-            residual = stream + normed(total[rows, :], gains_ref[1:2, :])
+            residual = stream + normed(total[rows, :], gains[1])
             residual = residual.astype(jnp.bfloat16)
             if h == 0:
-                out_ref[rows, :] = residual
-            middle = normed(residual.astype(jnp.float32), gains_ref[2:3, :])
+                source[rows, :] = residual
+            middle = normed(residual.astype(jnp.float32), gains[2])
             xm[h, rows, :] = middle.astype(jnp.bfloat16)
 
-    mixed(1, True, False, out0)
+    all_blocks = tuple(range(blocks))
+    mixed(1, all_blocks, (), True, out0, 2)
     ref = far_out.at[pl.ds(0, chips * depth), :]
     remote(ref, ref, share_send.at[0], share_recv.at[0], partner).wait_recv()
-    for b in range(blocks):
-        hid_copy(b).wait_recv()
-    mixed(1, False, True, out0 + 4)
+    ffn0 = out0 + 2
+    for b in all_blocks:
+        hid_copy(b, 0).wait_recv()
+        mixed(1, (), (b,), False, ffn0, 2)
+        ffn0 += 2
     settle(1, other)
-    ffn0 = out0 + 8
 
     ucols = 256
     unit_chunks = units // 2 // ucols
@@ -620,7 +697,7 @@
 
     first_done = 2 * per_stage + head
     second_done = 3 * per_stage + head
-    ticks(ffn0, first_done) if ffn0 < first_done else None
+    ticks(min(ffn0, first_done), first_done)
     ffn1 = max(ffn0, first_done)
 
     @pl.loop(0, chips)
@@ -633,7 +710,7 @@
         tick(ffn1 + c)
 
     ffn2 = ffn1 + unit_chunks
-    ticks(ffn2, second_done)
+    ticks(min(ffn2, second_done), second_done)
 
     @pl.loop(0, chips)
     def _(slot):
@@ -680,8 +757,10 @@
         part[chip] = partial_of(1, chip).astype(jnp.bfloat16)
         back_copy(slot).start()
 
-    mixed(0, True, True, None)
-    settle(0, tokens_ref)
+    for b in all_blocks:
+        hid_copy(b, 1).wait_recv()
+    mixed(0, all_blocks, all_blocks, True)
+    settle(0, mine)
 
     @pl.loop(0, 2 * unit_chunks)
     def _(c):
@@ -701,8 +780,9 @@
         rows = pl.ds(pl.multiple_of(i * chunk, chunk), chunk)
         came = jnp.concatenate([back[chip, rows, :] for chip in range(chips)], axis=1)
         summed = total[rows, :] + came.astype(jnp.float32)
-        middle = out_ref[rows, :].astype(jnp.float32)
-        out_ref[rows, :] = (middle + normed(summed, gains_ref[3:4, :])).astype(jnp.bfloat16)
+        middle = mine[rows, :].astype(jnp.float32)
+        mine[rows, :] = (middle + normed(summed, gains[3])).astype(jnp.bfloat16)
+        pltpu.make_async_copy(mine.at[rows, :], out_ref.at[rows, :], out_sem.at[i]).start()
 
     for g in range(stages):
         ref = shard_rows(g, 0, 0)
@@ -714,12 +794,16 @@
                 ).wait_send()
         for slot in range(chips):
             remote(ref, ref, near_send.at[g, slot], near_recv.at[g, slot], partner).wait_send()
-    remote(tokens_ref, other, tok_send.at[0], tok_recv.at[0], across).wait_send()
+    remote(mine, other, tok_send.at[0], tok_recv.at[0], across).wait_send()
     ref = far_out.at[pl.ds(0, chips * depth), :]
     remote(ref, ref, cross_send.at[0], cross_recv.at[0], across).wait_send()
     remote(ref, ref, share_send.at[0], share_recv.at[0], partner).wait_send()
     for b in range(blocks):
-        hid_copy(b).wait_send()
+        for h in range(2):
+            hid_copy(b, h).wait_send()
+    for i in range(half // chunk):
+        rows = pl.ds(i * chunk, chunk)
+        pltpu.make_async_copy(mine.at[rows, :], out_ref.at[rows, :], out_sem.at[i]).wait()
     for slot in range(chips):
         back_copy(slot).wait_send()
 
@@ -750,32 +834,27 @@
     width = min(256, channels)
     blocks = channels // width
     length = 2 * half
-    cut = units // 2
-    shards = jnp.stack(
-        [
-            jnp.concatenate([w_branch, w_gelu, out_weight_t], axis=1),
-            jnp.concatenate([w_gate[:, :cut], w_up[:, :cut]], axis=1),
-            jnp.concatenate([w_gate[:, cut:], w_up[:, cut:]], axis=1),
-            down_weight_t,
-        ]
-    )
-    gains = jnp.stack([pre_mix_gain, post_mix_gain, pre_ffn_gain, post_ffn_gain])
-    conv = conv_weight.reshape(4, blocks, width).swapaxes(0, 1)
-    gates = jnp.concatenate([w_rec[0], w_inp[0], w_rec[1], w_inp[1]], axis=-1)
-    coef = (-8.0 * jax.nn.softplus(-decay)).reshape(2, blocks, width).swapaxes(0, 1)
     bf16 = functools.partial(pltpu.VMEM, dtype=jnp.bfloat16)
     f32 = functools.partial(pltpu.VMEM, dtype=jnp.float32)
     dma = pltpu.SemaphoreType.DMA
-    stages = shards.shape[0]
+    stages = 4
+    chunks = half // 128
+    groups = channels // group
     reach = chips // 2
-    vmem = pl.BlockSpec(memory_space=pltpu.VMEM)
+    hbm = pl.BlockSpec(memory_space=pl.ANY)
+    gains = (pre_mix_gain, post_mix_gain, pre_ffn_gain, post_ffn_gain)
     return pl.pallas_call(
         functools.partial(layer_kernel, size),
         out_shape=jax.ShapeDtypeStruct((half, model), jnp.bfloat16),
-        in_specs=[vmem] * 6,
-        out_specs=vmem,
+        in_specs=[hbm] * 15,
+        out_specs=hbm,
         scratch_shapes=[
-            bf16((stages, model, shards.shape[2])),
+            bf16((half, model)),
+            f32((4, 1, model)),
+            bf16(conv_weight.shape),
+            bf16((groups, group, 4 * group)),
+            f32(decay.shape),
+            bf16((stages, model, 3 * channels)),
             bf16((model, channels)),
             bf16((half, model)),
             bf16((2, half, model)),
@@ -794,15 +873,18 @@
             dma((2, stages, reach, PIECES)),
             dma((stages, chips)),
             dma((stages, chips)),
-            dma((stages,)),
+            dma((8,)),
+            dma((6 + 4 * groups,)),
+            dma((chunks,)),
+            dma((chunks,)),
             dma((1,)),
             dma((TOKEN_PIECES,)),
             dma((1,)),
             dma((1,)),
             dma((1,)),
             dma((1,)),
-            dma((blocks,)),
-            dma((blocks,)),
+            dma((blocks, 2)),
+            dma((blocks, 2)),
             dma((chips,)),
             dma((chips,)),
         ],
@@ -812,7 +894,20 @@
         cost_estimate=pl.CostEstimate(
             flops=1 << 34, bytes_accessed=1 << 26, transcendentals=1 << 24
         ),
-    )(tokens, shards, gains, conv, gates, coef)
+    )(
+        tokens,
+        w_branch,
+        w_gelu,
+        out_weight_t,
+        w_gate,
+        w_up,
+        down_weight_t,
+        *(gain.reshape(1, model) for gain in gains),
+        conv_weight,
+        w_rec,
+        w_inp,
+        decay,
+    )
 
 
 def wide_device(

time: 174 us -> 161 us (0.925)
  Pallas kernels: 164 us -> 157 us
  other arithmetic: 6.05 us -> 0 us
    pallas_call x1, Pallas kernels: 164 us -> 157 us  [paired_device(): pl.pallas_call(functools.partial(layer_kernel, size), out_shape=jax.Shape...]
    another operation x4 -> x0, other arithmetic: 3.83 us -> none  [the longest x3 2.45 us: paired_device(): jnp.stack([jnp.concatenate([w_branch, w_gelu, out_weight_t], axis=1), jnp...]
where the time goes in v3:
time: 161 us; the launch traced here: 160 us
  Pallas kernels  157 us (98%)
  local copies, waits for them, and re-layouts  3.16 us (2%)
    pallas_call x1, Pallas kernels, paired_device(): pl.pallas_call(functools.partial(layer_kernel, size), out_shape=jax.Shape...  157 us

profile of v3, /device:TPU:0, one launch (start us, length us, event | category | flops | bytes accessed | tf_op | source)
XLA Modules:
  0.0 160.5 jit_solution(9306926817676301817)
XLA Ops:
  0.0 157.3 %shard_map.145 = bf16[512,2048]{1,0:T(8,128)(2,1)} custom-call(bf16[512,2048]{1,0:T(8,128)(2,1)} %tokens_ref.1, bf16[128,512]{1,0:T(8,128)(2,1)} %branch_ref.1, bf16[128,512]{1,0:T(8,128)(2,1)} %gelu_ref.1, bf16[128,512]{1,0:T(8,128)(2,1)} %outw_ref.1, bf16[128,1536]{1,0:T(8,128)(2,1)} %gate_ref.1, bf16[128,1536]{1,0:T(8,128)(2,1)} %up_ref.1, ...), custom_call_target="tpu_custom_call" | custom-call | flops 17179869184 | bytes 67108864 | tf_op jit(solution)/shard_map/pallas_call | solution.py:846
  157.3 3.2 %copy.17 = bf16[512,2048]{1,0:T(8,128)(2,1)} copy(bf16[512,2048]{1,0:T(8,128)(2,1)} %shard_map.145) | data formatting | bytes 4194304

commit v4 on v3

--- a/solution.py
+++ b/solution.py
@@ -11,7 +11,8 @@
 SEGMENTS = 8
 PIECES = 4
 TOKEN_PIECES = 4
-SCAN_TICKS = 9
+SCAN_TICKS = 6
+PITCH_PAD = 8
 MOST_VMEM = 67043328
 VMEM_BYTES = 60 * 1024 * 1024
 
@@ -304,7 +305,6 @@
     half, model = tokens_ref.shape
     blocks, width = pad.shape[0], pad.shape[2]
     group = gates_ref.shape[1]
-    groups = gates_ref.shape[0]
     units = hf.shape[2]
     span = 2 * depth
 
@@ -340,21 +340,14 @@
     for copy in own_copies[0]:
         copy.start()
     chunk = 128
-    mine_copies = []
-    for i in range(half // chunk):
-        rows = pl.ds(i * chunk, chunk)
-        mine_copies.append(
-            pltpu.make_async_copy(tokens_ref.at[rows, :], mine.at[rows, :], mine_sem.at[i])
-        )
-    for i, copy in enumerate(mine_copies):
-        copy.start()
+    mine_copy = pltpu.make_async_copy(tokens_ref, mine, mine_sem.at[0])
+    mine_copy.start()
     small = [(source, gains.at[i]) for i, source in enumerate((gain0_ref, gain1_ref, gain2_ref, gain3_ref))]
     small += [(taps_ref, conv_ref), (decay_ref, coef_ref)]
-    for n in range(groups):
-        for d in range(2):
-            for i, source in enumerate((rec_ref, inp_ref)):
-                lanes = pl.ds((2 * d + i) * group, group)
-                small.append((source.at[d, n], gates_ref.at[n, :, lanes]))
+    for d in range(2):
+        for i, source in enumerate((rec_ref, inp_ref)):
+            lanes = pl.ds((2 * d + i) * group, group)
+            small.append((source.at[d], gates_ref.at[:, :, lanes]))
     small = [
         pltpu.make_async_copy(source, place_at, small_sem.at[i])
         for i, (source, place_at) in enumerate(small)
@@ -382,25 +375,25 @@
         src = piece(g, me // 2, p)
         dst = src
         for way in range(2):
-            remote(src, dst, ring_send.at[way, g, 0], ring_recv.at[way, g, 0, p], targets[way]).start()
-        remote(src, dst, near_send.at[g, 0], near_recv.at[g, 0], partner).start()
+            remote(src, dst, ring_send.at[way, g], ring_recv.at[way, g, 0, p], targets[way]).start()
+        remote(src, dst, near_send.at[g], near_recv.at[g, 0], partner).start()
 
     def pass_piece(g, s, p):
         for way in range(2):
             ref = piece(g, chip_at(-s if way == 0 else s), p)
             slot = 2 * s - 1 + way
             remote(
-                ref, ref, ring_send.at[way, g, s], ring_recv.at[way, g, s - 1, p], targets[way]
+                ref, ref, ring_send.at[way, g], ring_recv.at[way, g, s - 1, p], targets[way]
             ).wait_recv()
 
             def forward():
                 remote(
-                    ref, ref, ring_send.at[way, g, s], ring_recv.at[way, g, s, p], targets[way]
+                    ref, ref, ring_send.at[way, g], ring_recv.at[way, g, s, p], targets[way]
                 ).start()
 
             mine = p < PIECES // 2 if way == 0 else p >= PIECES // 2
             branch_on(either(s < reach - 1, mine), forward)
-            remote(ref, ref, near_send.at[g, slot], near_recv.at[g, slot], partner).start()
+            remote(ref, ref, near_send.at[g], near_recv.at[g, slot], partner).start()
 
     def last_piece(g, q):
         for way in range(2):
@@ -409,11 +402,11 @@
             remote(
                 ref,
                 ref,
-                ring_send.at[way, g, reach - 1],
+                ring_send.at[way, g],
                 ring_recv.at[way, g, reach - 1, p],
                 targets[way],
             ).wait_recv()
-            remote(ref, ref, near_send.at[g, chips - 1], near_recv.at[g, chips - 1], partner).start()
+            remote(ref, ref, near_send.at[g], near_recv.at[g, chips - 1], partner).start()
 
     head = PIECES + PIECES // 2
     per_stage = head + (reach - 1) * PIECES
@@ -437,7 +430,7 @@
 
     def near_wait(g, slot):
         ref = shard_rows(g, 0, 0)
-        remote(ref, ref, near_send.at[g, slot], near_recv.at[g, slot], partner).wait_recv()
+        remote(ref, ref, near_send.at[g], near_recv.at[g, slot], partner).wait_recv()
 
     token_rows = half // TOKEN_PIECES
     for i in range(TOKEN_PIECES):
@@ -446,7 +439,7 @@
     for copy in own_copies[0]:
         copy.wait()
     ticks(0, PIECES)
-    for copy in (*small, *mine_copies):
+    for copy in (*small, mine_copy):
         copy.wait()
     for copies in own_copies[1:]:
         for copy in copies:
@@ -526,11 +519,12 @@
     scan0 = done0 + 2 * (2 * (half // prows) - 1)
     parts = width // group
     steps = length // SEGMENTS
+    pitch = steps + PITCH_PAD
     crows = 256
 
     def hid_copy(b, h):
         return remote(
-            hid.at[b, h], got.at[b, h], hid_send.at[b, h], hid_recv.at[b, h], across
+            hid.at[b, h], got.at[b, h], hid_send.at[0], hid_recv.at[b, h], across
         )
 
     @pl.loop(0, blocks)
@@ -560,9 +554,12 @@
                     log_retain = rate * coef[d : d + 1]
                     retain = jnp.exp(log_retain)
                     left = one_minus_exp(2.0 * log_retain, retain * retain)
-                    a_ref[n, start : start + crows, :] = retain
-                    u_ref[n, start : start + crows, :] = jnp.sqrt(left) * inflow * wide
-                if (start // crows) % 2 == 1 and count < SCAN_TICKS:
+                    feed = jnp.sqrt(left) * inflow * wide
+                    for q in range(crows // steps):
+                        first = (start // steps + q) * pitch
+                        a_ref[n, first : first + steps, :] = retain[q * steps : (q + 1) * steps]
+                        u_ref[n, first : first + steps, :] = feed[q * steps : (q + 1) * steps]
+                if (start // crows) % 2 == 1:
                     tick(at + count)
                     count += 1
 
@@ -572,7 +569,7 @@
                 (carry[0], (a0, u0), t),
                 (carry[1], (a1, u1), steps - 1 - t),
             ):
-                where = pl.ds(when, SEGMENTS, stride=steps)
+                where = pl.ds(when, SEGMENTS, stride=pitch)
                 nstate, ndecayed = [], []
                 for n in range(parts):
                     retain = a_ref[n, where, :]
@@ -589,10 +586,11 @@
         one = tuple(jnp.ones((SEGMENTS, group), jnp.float32) for n in range(parts))
         ended = ((zero, one), (zero, one))
         for run in range(2):
-            low, high = run * steps // 2, (run + 1) * steps // 2
-            ended = lax.fori_loop(low, high, step, ended, unroll=8)
-            tick(at + count)
-            count += 1
+            first, last = run * steps // 2, (run + 1) * steps // 2
+            ended = lax.fori_loop(first, last, step, ended, unroll=8)
+            if run == 0:
+                tick(at + count)
+                count += 1
         per_half = SEGMENTS // 2
         for n in range(parts):
             lanes = slice(n * group, (n + 1) * group)
@@ -604,15 +602,13 @@
                     entry[d][s] = carry
                     carry = ended[d][0][n][s : s + 1] + ended[d][1][n][s : s + 1] * carry
             for s in range(SEGMENTS):
-                rows = slice(s * steps, (s + 1) * steps)
+                rows = slice(s * pitch, s * pitch + steps)
                 local = slice((s % per_half) * steps, (s % per_half + 1) * steps)
                 which = jnp.where(column == s // per_half, 0, 1)
                 forward = u0[n, rows, :] + a0[n, rows, :] * entry[0][s]
                 backward = u1[n, rows, :] + a1[n, rows, :] * entry[1][s]
                 gate = gel[which, b, local, lanes].astype(jnp.float32)
                 hid[b, which, local, lanes] = (gate * (forward + backward)).astype(jnp.bfloat16)
-            tick(at + count)
-            count += 1
         tick(at + count)
         count += 1
         assert count == SCAN_TICKS
@@ -621,14 +617,6 @@
     for b in range(blocks):
         hid_copy(b, 1).start()
     out0 = scan0 + blocks * SCAN_TICKS
-
-    ref = far_out.at[pl.ds(0, chips * depth), :]
-    remote(ref, ref, cross_send.at[0], cross_recv.at[0], across).wait_recv()
-
-    @pl.loop(0, chips)
-    def _(chip):
-        ref = far_out.at[pl.ds(pl.multiple_of((chip * 2 + core) * depth, depth), depth), :]
-        remote(ref, ref, share_send.at[0], share_recv.at[0], partner).start()
 
     ocols = 256
 
@@ -674,13 +662,25 @@
 
     all_blocks = tuple(range(blocks))
     mixed(1, all_blocks, (), True, out0, 2)
+    ticks(out0 + 2, out0 + 4)
+
     ref = far_out.at[pl.ds(0, chips * depth), :]
-    remote(ref, ref, share_send.at[0], share_recv.at[0], partner).wait_recv()
-    ffn0 = out0 + 2
+    remote(ref, ref, cross_send.at[0], cross_recv.at[0], across).wait_recv()
+
+    @pl.loop(0, chips)
+    def _(chip):
+        ref = far_out.at[pl.ds(pl.multiple_of((chip * 2 + core) * depth, depth), depth), :]
+        remote(ref, ref, share_send.at[0], share_recv.at[0], partner).start()
+
+    ffn0 = out0 + 4
     for b in all_blocks:
+        ticks(ffn0, ffn0 + b + 1)
         hid_copy(b, 0).wait_recv()
-        mixed(1, (), (b,), False, ffn0, 2)
-        ffn0 += 2
+        if b == 0:
+            ref = far_out.at[pl.ds(0, chips * depth), :]
+            remote(ref, ref, share_send.at[0], share_recv.at[0], partner).wait_recv()
+        mixed(1, (), (b,), False, ffn0 + b + 1, 1)
+        ffn0 += b + 2
     settle(1, other)
 
     ucols = 256
@@ -709,31 +709,51 @@
         expand(1, 1, c)
         tick(ffn1 + c)
 
-    ffn2 = ffn1 + unit_chunks
-    ticks(min(ffn2, second_done), second_done)
-
-    @pl.loop(0, chips)
-    def _(slot):
-        near_wait(2, slot)
-
-    @pl.loop(0, unit_chunks)
-    def _(c):
-        expand(2, 1, c)
-        tick(second_done + c)
-
     def feature_chip(slot):
         d = (slot + 1) // 2
         return chip_at(jnp.where(slot % 2 == 1, -d, d))
 
+    def expand_part(g, h, c, slots, fresh, last):
+        rows = [pl.ds(pl.multiple_of(feature_chip(slot) * span, span), span) for slot in slots]
+        x = jnp.concatenate([xm[h, :, at] for at in rows], axis=1)
+        summed = []
+        for side in range(2):
+            lanes = pl.ds(pl.multiple_of(side * cut + c * ucols, ucols), ucols)
+            w = jnp.concatenate([full[g, at, lanes] for at in rows], axis=0)
+            term = jnp.dot(x, w, preferred_element_type=jnp.float32)
+            if not fresh:
+                term = total[:, lanes] + term
+            if last:
+                summed.append(term)
+            else:
+                total[:, lanes] = term
+        if last:
+            lanes = pl.ds(pl.multiple_of((g - 1) * cut + c * ucols, ucols), ucols)
+            hf[h, :, lanes] = (jax.nn.silu(summed[0]) * summed[1]).astype(jnp.bfloat16)
+
+    ffn2 = ffn1 + unit_chunks
+    before = second_done - PIECES // 2
+    ticks(min(ffn2, before), before)
+    parts_b = (tuple(range(chips - 3)), (chips - 3, chips - 2), (chips - 1,))
+    for n, slots in enumerate(parts_b):
+        if n == len(parts_b) - 1:
+            ticks(before, second_done)
+        for slot in slots:
+            near_wait(2, slot)
+
+        @pl.loop(0, unit_chunks)
+        def _(c):
+            expand_part(2, 1, c, slots, n == 0, n == len(parts_b) - 1)
+
     def partial_of(h, chip):
         weight = full[stages - 1, pl.ds(pl.multiple_of(chip * span, span), span), :]
         return matmul_t(hf[h], weight)
 
     def back_copy(slot):
         chip = feature_chip(slot)
-        return remote(part.at[chip], back.at[chip], back_send.at[slot], back_recv.at[slot], across)
-
-    down0 = second_done + unit_chunks
+        return remote(part.at[chip], back.at[chip], back_send.at[0], back_recv.at[slot], across)
+
+    down0 = second_done
     distance1 = (stages - 1) * per_stage + head + PIECES
 
     @pl.loop(0, chips)
@@ -782,30 +802,23 @@
         summed = total[rows, :] + came.astype(jnp.float32)
         middle = mine[rows, :].astype(jnp.float32)
         mine[rows, :] = (middle + normed(summed, gains[3])).astype(jnp.bfloat16)
-        pltpu.make_async_copy(mine.at[rows, :], out_ref.at[rows, :], out_sem.at[i]).start()
+        pltpu.make_async_copy(mine.at[rows, :], out_ref.at[rows, :], out_sem.at[0]).start()
 
     for g in range(stages):
-        ref = shard_rows(g, 0, 0)
+        rows = full.at[g, pl.ds(0, (reach - 1) * depth + depth // 2), :]
         for way in range(2):
-            for s in range(reach):
-                sent = ref if s < reach - 1 else full.at[g, pl.ds(0, depth // 2), :]
-                remote(
-                    sent, sent, ring_send.at[way, g, s], ring_recv.at[way, g, s, 0], targets[way]
-                ).wait_send()
-        for slot in range(chips):
-            remote(ref, ref, near_send.at[g, slot], near_recv.at[g, slot], partner).wait_send()
+            remote(
+                rows, rows, ring_send.at[way, g], ring_recv.at[way, g, 0, 0], targets[way]
+            ).wait_send()
+        rows = full.at[g, pl.ds(0, chips * depth), :]
+        remote(rows, rows, near_send.at[g], near_recv.at[g, 0], partner).wait_send()
     remote(mine, other, tok_send.at[0], tok_recv.at[0], across).wait_send()
     ref = far_out.at[pl.ds(0, chips * depth), :]
     remote(ref, ref, cross_send.at[0], cross_recv.at[0], across).wait_send()
     remote(ref, ref, share_send.at[0], share_recv.at[0], partner).wait_send()
-    for b in range(blocks):
-        for h in range(2):
-            hid_copy(b, h).wait_send()
-    for i in range(half // chunk):
-        rows = pl.ds(i * chunk, chunk)
-        pltpu.make_async_copy(mine.at[rows, :], out_ref.at[rows, :], out_sem.at[i]).wait()
-    for slot in range(chips):
-        back_copy(slot).wait_send()
+    remote(hid, got, hid_send.at[0], hid_recv.at[0, 0], across).wait_send()
+    remote(part, back, back_send.at[0], back_recv.at[0], across).wait_send()
+    pltpu.make_async_copy(mine, out_ref, out_sem.at[0]).wait()
 
 
 def paired_device(
@@ -838,7 +851,6 @@
     f32 = functools.partial(pltpu.VMEM, dtype=jnp.float32)
     dma = pltpu.SemaphoreType.DMA
     stages = 4
-    chunks = half // 128
     groups = channels // group
     reach = chips // 2
     hbm = pl.BlockSpec(memory_space=pl.ANY)
@@ -861,7 +873,7 @@
             f32((blocks, length + 16, width)),
             bf16((2, blocks, half, width)),
         ]
-        + [f32((width // group, length, group)) for i in range(4)]
+        + [f32((width // group, length + SEGMENTS * PITCH_PAD, group)) for i in range(4)]
         + [
             bf16((blocks, 2, half, width)),
             bf16((blocks, 2, half, width)),
@@ -869,23 +881,23 @@
             bf16((2, half, units)),
             bf16((chips, half, 2 * depth)),
             bf16((chips, half, 2 * depth)),
-            dma((2, stages, reach)),
+            dma((2, stages)),
             dma((2, stages, reach, PIECES)),
-            dma((stages, chips)),
+            dma((stages,)),
             dma((stages, chips)),
             dma((8,)),
-            dma((6 + 4 * groups,)),
-            dma((chunks,)),
-            dma((chunks,)),
+            dma((10,)),
+            dma((1,)),
+            dma((1,)),
             dma((1,)),
             dma((TOKEN_PIECES,)),
             dma((1,)),
             dma((1,)),
             dma((1,)),
             dma((1,)),
+            dma((1,)),
             dma((blocks, 2)),
-            dma((blocks, 2)),
-            dma((chips,)),
+            dma((1,)),
             dma((chips,)),
         ],
         compiler_params=pltpu.CompilerParams(

time: 161 us -> 156 us (0.969)
  Pallas kernels: 157 us -> 152 us
    pallas_call x1, Pallas kernels: 157 us -> 152 us  [paired_device(): pl.pallas_call(functools.partial(layer_kernel, size), out_shape=jax.Shape...]
where the time goes in v4:
time: 156 us; the launch traced here: 155 us
  Pallas kernels  152 us (97%)
  local copies, waits for them, and re-layouts  3.16 us (2%)
    pallas_call x1, Pallas kernels, paired_device(): pl.pallas_call(functools.partial(layer_kernel, size), out_shape=jax.Shape...  152 us
    unnamed x1, local copies, waits for them, and re-layouts  3.16 us

profile of v4, /device:TPU:0, one launch (start us, length us, event | category | flops | bytes accessed | tf_op | source)
XLA Modules:
  0.0 155.4 jit_solution(1530318548146837175)
XLA Ops:
  0.0 152.3 %shard_map.145 = bf16[512,2048]{1,0:T(8,128)(2,1)} custom-call(bf16[512,2048]{1,0:T(8,128)(2,1)} %tokens_ref.1, bf16[128,512]{1,0:T(8,128)(2,1)} %branch_ref.1, bf16[128,512]{1,0:T(8,128)(2,1)} %gelu_ref.1, bf16[128,512]{1,0:T(8,128)(2,1)} %outw_ref.1, bf16[128,1536]{1,0:T(8,128)(2,1)} %gate_ref.1, bf16[128,1536]{1,0:T(8,128)(2,1)} %up_ref.1, ...), custom_call_target="tpu_custom_call" | custom-call | flops 17179869184 | bytes 67108864 | tf_op jit(solution)/shard_map/pallas_call | solution.py:858
  152.3 3.2 %copy.17 = bf16[512,2048]{1,0:T(8,128)(2,1)} copy(bf16[512,2048]{1,0:T(8,128)(2,1)} %shard_map.145) | data formatting | bytes 4194304

commit v5 on v4

--- a/solution.py
+++ b/solution.py
@@ -275,6 +275,7 @@
     hid,
     got,
     total,
+    squares,
     hf,
     part,
     back,
@@ -375,20 +376,24 @@
         src = piece(g, me // 2, p)
         dst = src
         for way in range(2):
-            remote(src, dst, ring_send.at[way, g], ring_recv.at[way, g, 0, p], targets[way]).start()
+            remote(src, dst, ring_send.at[way, g], ring_recv.at[g, 0, p], targets[way]).start()
         remote(src, dst, near_send.at[g], near_recv.at[g, 0], partner).start()
 
+    def landed(g, s, p):
+        rows = full.at[g, pl.ds(0, 2 * prow), :]
+        remote(rows, rows, ring_send.at[0, g], ring_recv.at[g, s, p], targets[0]).wait_recv()
+
     def pass_piece(g, s, p):
+        landed(g, s - 1, p)
         for way in range(2):
             ref = piece(g, chip_at(-s if way == 0 else s), p)
             slot = 2 * s - 1 + way
-            remote(
-                ref, ref, ring_send.at[way, g], ring_recv.at[way, g, s - 1, p], targets[way]
-            ).wait_recv()
+            low_half = way * (PIECES // 2)
 
             def forward():
+                index = jnp.where(s < reach - 1, p, p - low_half)
                 remote(
-                    ref, ref, ring_send.at[way, g], ring_recv.at[way, g, s, p], targets[way]
+                    ref, ref, ring_send.at[way, g], ring_recv.at[g, s, index], targets[way]
                 ).start()
 
             mine = p < PIECES // 2 if way == 0 else p >= PIECES // 2
@@ -396,16 +401,9 @@
             remote(ref, ref, near_send.at[g], near_recv.at[g, slot], partner).start()
 
     def last_piece(g, q):
+        landed(g, reach - 1, q)
         for way in range(2):
-            p = q + way * (PIECES // 2)
-            ref = piece(g, chip_at(reach), p)
-            remote(
-                ref,
-                ref,
-                ring_send.at[way, g],
-                ring_recv.at[way, g, reach - 1, p],
-                targets[way],
-            ).wait_recv()
+            ref = piece(g, chip_at(reach), q + way * (PIECES // 2))
             remote(ref, ref, near_send.at[g], near_recv.at[g, chips - 1], partner).start()
 
     head = PIECES + PIECES // 2
@@ -475,6 +473,7 @@
         remote(src, dst, cross_send.at[0], cross_recv.at[0], across).start()
 
     prows = 256
+    scan0 = done0 + 2 * (2 * (half // prows) - 1) + 1
 
     @pl.loop(0, 2)
     def _(h):
@@ -500,6 +499,10 @@
                 def _(q):
                     norm_rows(other, 1, pl.multiple_of(at + q * chunk, chunk))
 
+                @pl.when(i == half // prows - 1)
+                def _():
+                    tick(scan0 - 1)
+
             x = xm[h, pl.ds(at, prows), :]
             side = jnp.where(h == 0, column, 1 - column)
             base = pl.multiple_of(8 + side * half + at, 8)
@@ -516,7 +519,6 @@
             def _():
                 ticks(done0 + h * 4 + i * 2, done0 + h * 4 + i * 2 + 2)
 
-    scan0 = done0 + 2 * (2 * (half // prows) - 1)
     parts = width // group
     steps = length // SEGMENTS
     pitch = steps + PITCH_PAD
@@ -662,7 +664,7 @@
 
     all_blocks = tuple(range(blocks))
     mixed(1, all_blocks, (), True, out0, 2)
-    ticks(out0 + 2, out0 + 4)
+    tick(out0 + 2)
 
     ref = far_out.at[pl.ds(0, chips * depth), :]
     remote(ref, ref, cross_send.at[0], cross_recv.at[0], across).wait_recv()
@@ -672,16 +674,18 @@
         ref = far_out.at[pl.ds(pl.multiple_of((chip * 2 + core) * depth, depth), depth), :]
         remote(ref, ref, share_send.at[0], share_recv.at[0], partner).start()
 
-    ffn0 = out0 + 4
+    ffn0 = out0 + 3
     for b in all_blocks:
-        ticks(ffn0, ffn0 + b + 1)
+        ticks(ffn0, ffn0 + 2)
         hid_copy(b, 0).wait_recv()
         if b == 0:
             ref = far_out.at[pl.ds(0, chips * depth), :]
             remote(ref, ref, share_send.at[0], share_recv.at[0], partner).wait_recv()
-        mixed(1, (), (b,), False, ffn0 + b + 1, 1)
-        ffn0 += b + 2
+        mixed(1, (), (b,), False, ffn0 + 2, 1)
+        ffn0 += 3
     settle(1, other)
+    tick(ffn0)
+    ffn0 += 1
 
     ucols = 256
     unit_chunks = units // 2 // ucols
@@ -707,7 +711,10 @@
     @pl.loop(0, unit_chunks)
     def _(c):
         expand(1, 1, c)
-        tick(ffn1 + c)
+
+        @pl.when(c == 1)
+        def _():
+            tick(ffn1)
 
     def feature_chip(slot):
         d = (slot + 1) // 2
@@ -731,7 +738,7 @@
             lanes = pl.ds(pl.multiple_of((g - 1) * cut + c * ucols, ucols), ucols)
             hf[h, :, lanes] = (jax.nn.silu(summed[0]) * summed[1]).astype(jnp.bfloat16)
 
-    ffn2 = ffn1 + unit_chunks
+    ffn2 = ffn1 + 1
     before = second_done - PIECES // 2
     ticks(min(ffn2, before), before)
     parts_b = (tuple(range(chips - 3)), (chips - 3, chips - 2), (chips - 1,))
@@ -753,62 +760,86 @@
         chip = feature_chip(slot)
         return remote(part.at[chip], back.at[chip], back_send.at[0], back_recv.at[slot], across)
 
-    down0 = second_done
-    distance1 = (stages - 1) * per_stage + head + PIECES
-
-    @pl.loop(0, chips)
-    def _(slot):
-        @pl.when(slot == 1)
-        def _():
-            ticks(down0, distance1)
-
-        @pl.when(jnp.logical_and(slot % 2 == 1, jnp.logical_and(slot > 1, slot < chips - 1)))
-        def _():
-            @pl.loop(0, PIECES)
-            def _(i):
-                tick(distance1 + (slot // 2 - 1) * PIECES + i)
-
-        @pl.when(slot == chips - 1)
-        def _():
-            ticks(stages * per_stage + PIECES, stages * per_stage + head)
-
+    distance1 = (stages - 1) * per_stage + head
+
+    def send_back(slot):
         near_wait(stages - 1, slot)
         chip = feature_chip(slot)
         part[chip] = partial_of(1, chip).astype(jnp.bfloat16)
         back_copy(slot).start()
 
+    def send_pair(d):
+        @pl.loop(2 * d - 1, 2 * d + 1)
+        def _(slot):
+            send_back(slot)
+
+    send_back(0)
     for b in all_blocks:
         hid_copy(b, 1).wait_recv()
-    mixed(0, all_blocks, all_blocks, True)
+    mixed(0, all_blocks, (), True, distance1, PIECES)
+    send_pair(1)
+    mixed(0, (), all_blocks, False, distance1 + PIECES, 2)
     settle(0, mine)
-
-    @pl.loop(0, 2 * unit_chunks)
+    tick(distance1 + PIECES + 2)
+
+    @pl.loop(0, unit_chunks)
     def _(c):
-        expand(1 + c // unit_chunks, 0, c % unit_chunks)
+        expand(1, 0, c)
+
+        @pl.when(c == 1)
+        def _():
+            tick(distance1 + PIECES + 3)
+
+    send_pair(2)
+
+    @pl.loop(0, unit_chunks)
+    def _(c):
+        expand(2, 0, c)
+        tick(distance1 + 2 * PIECES + c)
+
+    ticks(distance1 + 2 * PIECES + unit_chunks, distance1 + 3 * PIECES)
+    send_pair(3)
+    ticks(stages * per_stage + PIECES, stages * per_stage + head)
+    send_back(chips - 1)
 
     @pl.loop(0, chips)
     def _(chip):
         lanes = pl.ds(pl.multiple_of(chip * span, span), span)
         total[:, lanes] = partial_of(0, chip).astype(jnp.bfloat16).astype(jnp.float32)
 
+    squares[...] = jnp.zeros_like(squares)
+
     @pl.loop(0, chips)
     def _(slot):
         back_copy(slot).wait_recv()
+        chip = feature_chip(slot)
+        lanes = pl.ds(pl.multiple_of(chip * span, span), span)
+
+        @pl.loop(0, half // chunk)
+        def _(i):
+            rows = pl.ds(pl.multiple_of(i * chunk, chunk), chunk)
+            summed = total[rows, lanes] + back[chip, rows, :].astype(jnp.float32)
+            total[rows, lanes] = summed
+            square = summed * summed
+            folded = square[:, :128]
+            for at in range(128, span, 128):
+                folded = folded + square[:, at : at + 128]
+            squares[rows, :] += folded
 
     @pl.loop(0, half // chunk)
     def _(i):
         rows = pl.ds(pl.multiple_of(i * chunk, chunk), chunk)
-        came = jnp.concatenate([back[chip, rows, :] for chip in range(chips)], axis=1)
-        summed = total[rows, :] + came.astype(jnp.float32)
+        mean = jnp.sum(squares[rows, :], axis=-1, keepdims=True) * (1.0 / model)
+        scaled = total[rows, :] * lax.rsqrt(mean + EPS) * gains[3]
         middle = mine[rows, :].astype(jnp.float32)
-        mine[rows, :] = (middle + normed(summed, gains[3])).astype(jnp.bfloat16)
+        mine[rows, :] = (middle + scaled).astype(jnp.bfloat16)
         pltpu.make_async_copy(mine.at[rows, :], out_ref.at[rows, :], out_sem.at[0]).start()
 
     for g in range(stages):
         rows = full.at[g, pl.ds(0, (reach - 1) * depth + depth // 2), :]
         for way in range(2):
             remote(
-                rows, rows, ring_send.at[way, g], ring_recv.at[way, g, 0, 0], targets[way]
+                rows, rows, ring_send.at[way, g], ring_recv.at[g, 0, 0], targets[way]
             ).wait_send()
         rows = full.at[g, pl.ds(0, chips * depth), :]
         remote(rows, rows, near_send.at[g], near_recv.at[g, 0], partner).wait_send()
@@ -878,11 +909,12 @@
             bf16((blocks, 2, half, width)),
             bf16((blocks, 2, half, width)),
             f32((half, model)),
+            f32((half, 128)),
             bf16((2, half, units)),
             bf16((chips, half, 2 * depth)),
             bf16((chips, half, 2 * depth)),
             dma((2, stages)),
-            dma((2, stages, reach, PIECES)),
+            dma((stages, reach, PIECES)),
             dma((stages,)),
             dma((stages, chips)),
             dma((8,)),

time: 156 us -> 154 us (0.987)
  no operation moved by 1% of the time
where the time goes in v5:
time: 154 us
  Pallas kernels  151 us (98%)
  local copies, waits for them, and re-layouts  3.16 us (2%)
    pallas_call x1, Pallas kernels, paired_device(): pl.pallas_call(functools.partial(layer_kernel, size), out_shape=jax.Shape...  151 us
    unnamed x1, local copies, waits for them, and re-layouts  3.16 us

profile of v5, /device:TPU:0, one launch (start us, length us, event | category | flops | bytes accessed | tf_op | source)
XLA Modules:
  0.0 154.1 jit_solution(8661506102287689884)
XLA Ops:
  0.0 150.9 %shard_map.145 = bf16[512,2048]{1,0:T(8,128)(2,1)} custom-call(bf16[512,2048]{1,0:T(8,128)(2,1)} %tokens_ref.1, bf16[128,512]{1,0:T(8,128)(2,1)} %branch_ref.1, bf16[128,512]{1,0:T(8,128)(2,1)} %gelu_ref.1, bf16[128,512]{1,0:T(8,128)(2,1)} %outw_ref.1, bf16[128,1536]{1,0:T(8,128)(2,1)} %gate_ref.1, bf16[128,1536]{1,0:T(8,128)(2,1)} %up_ref.1, ...), custom_call_target="tpu_custom_call" | custom-call | flops 17179869184 | bytes 67108864 | tf_op jit(solution)/shard_map/pallas_call | solution.py:889
  150.9 3.2 %copy.17 = bf16[512,2048]{1,0:T(8,128)(2,1)} copy(bf16[512,2048]{1,0:T(8,128)(2,1)} %shard_map.145) | data formatting | bytes 4194304

commit v6 on v5

--- a/solution.py
+++ b/solution.py
@@ -331,12 +331,23 @@
         return pltpu.make_async_copy(source.at[:, lanes], place_at, own_sem.at[sem])
 
     every = pl.ds(0, channels)
-    low, high = pl.ds(0, cut), pl.ds(cut, cut)
+    ucols = 256
+    unit_chunks = cut // ucols
+    unit_pairs = 2 * unit_chunks
+
+    def unit_parts(first, sem):
+        found = []
+        for c in range(unit_chunks):
+            for side, source in enumerate((gate_ref, up_ref)):
+                at = (2 * c + side) * ucols
+                found.append((source, pl.ds(first + c * ucols, ucols), at, sem + len(found)))
+        return found
+
     own_copies = [
         [own_part(0, source, every, i * channels, i) for i, source in enumerate((branch_ref, gelu_ref, outw_ref))],
-        [own_part(1, gate_ref, low, 0, 3), own_part(1, up_ref, low, cut, 4)],
-        [own_part(2, gate_ref, high, 0, 5), own_part(2, up_ref, high, cut, 6)],
-        [own_part(3, down_ref, pl.ds(0, units), 0, 7)],
+        [own_part(1, *pair) for pair in unit_parts(0, 3)],
+        [own_part(2, *pair) for pair in unit_parts(cut, 3 + unit_pairs)],
+        [own_part(3, down_ref, pl.ds(0, units), 0, 3 + 2 * unit_pairs)],
     ]
     for copy in own_copies[0]:
         copy.start()
@@ -388,22 +399,21 @@
         for way in range(2):
             ref = piece(g, chip_at(-s if way == 0 else s), p)
             slot = 2 * s - 1 + way
-            low_half = way * (PIECES // 2)
 
             def forward():
-                index = jnp.where(s < reach - 1, p, p - low_half)
+                index = jnp.where(s < reach - 1, p, p // 2)
                 remote(
                     ref, ref, ring_send.at[way, g], ring_recv.at[g, s, index], targets[way]
                 ).start()
 
-            mine = p < PIECES // 2 if way == 0 else p >= PIECES // 2
+            mine = p % 2 == way
             branch_on(either(s < reach - 1, mine), forward)
             remote(ref, ref, near_send.at[g], near_recv.at[g, slot], partner).start()
 
     def last_piece(g, q):
         landed(g, reach - 1, q)
         for way in range(2):
-            ref = piece(g, chip_at(reach), q + way * (PIECES // 2))
+            ref = piece(g, chip_at(reach), 2 * q + way)
             remote(ref, ref, near_send.at[g], near_recv.at[g, chips - 1], partner).start()
 
     head = PIECES + PIECES // 2
@@ -524,10 +534,22 @@
     pitch = steps + PITCH_PAD
     crows = 256
 
-    def hid_copy(b, h):
-        return remote(
-            hid.at[b, h], got.at[b, h], hid_send.at[0], hid_recv.at[b, h], across
-        )
+    quarter = half // 2
+
+    def hid_copies(b, h):
+        copies = []
+        for r in range(2):
+            rows = pl.ds(r * quarter, quarter)
+            copies.append(
+                remote(
+                    hid.at[b, h, rows, :],
+                    got.at[b, h, rows, :],
+                    hid_send.at[0],
+                    hid_recv.at[b, h, r],
+                    across,
+                )
+            )
+        return copies
 
     @pl.loop(0, blocks)
     def _(b):
@@ -614,18 +636,21 @@
         tick(at + count)
         count += 1
         assert count == SCAN_TICKS
-        hid_copy(b, 0).start()
+        for copy in hid_copies(b, 0):
+            copy.start()
 
     for b in range(blocks):
-        hid_copy(b, 1).start()
+        for copy in hid_copies(b, 1):
+            copy.start()
     out0 = scan0 + blocks * SCAN_TICKS
 
-    ocols = 256
-
-    def mixed(h, own_blocks, far_blocks, fresh, e0=0, count=0):
-        left = [hid[b, h] for b in own_blocks]
+
+    whole = slice(0, half)
+
+    def mixed(h, own_blocks, far_blocks, fresh, e0=0, count=0, tall=whole, ocols=512):
+        left = [hid[b, h, tall] for b in own_blocks]
         left = jnp.concatenate(left, axis=1) if left else None
-        right = [got[b, 1 - h] for b in far_blocks]
+        right = [got[b, 1 - h, tall] for b in far_blocks]
         right = jnp.concatenate(right, axis=1) if right else None
         parts_n = model // ocols
 
@@ -633,7 +658,7 @@
         def _(n):
             rows = pl.ds(pl.multiple_of(n * ocols, ocols), ocols)
             lanes = rows
-            summed = None if fresh else total[:, lanes]
+            summed = None if fresh else total[tall, lanes]
             if left is not None:
                 first = 2 * channels + own_blocks[0] * width
                 term = matmul_t(left, full[0, rows, first : first + len(own_blocks) * width])
@@ -642,7 +667,7 @@
                 first = far_blocks[0] * width
                 term = matmul_t(right, far_out[rows, first : first + len(far_blocks) * width])
                 summed = term if summed is None else summed + term
-            total[:, lanes] = summed
+            total[tall, lanes] = summed
             if count:
                 every_n = parts_n // count
 
@@ -650,8 +675,8 @@
                 def _():
                     tick(e0 + n // every_n)
 
-    def settle(h, source):
-        @pl.loop(0, half // chunk)
+    def settle(h, source, tall=whole):
+        @pl.loop(tall.start // chunk, tall.stop // chunk)
         def _(i):
             rows = pl.ds(pl.multiple_of(i * chunk, chunk), chunk)
             stream = source[rows, :].astype(jnp.float32)
@@ -675,29 +700,35 @@
         remote(ref, ref, share_send.at[0], share_recv.at[0], partner).start()
 
     ffn0 = out0 + 3
-    for b in all_blocks:
+    for b in all_blocks[:-1]:
         ticks(ffn0, ffn0 + 2)
-        hid_copy(b, 0).wait_recv()
+        for copy in hid_copies(b, 0):
+            copy.wait_recv()
         if b == 0:
             ref = far_out.at[pl.ds(0, chips * depth), :]
             remote(ref, ref, share_send.at[0], share_recv.at[0], partner).wait_recv()
         mixed(1, (), (b,), False, ffn0 + 2, 1)
         ffn0 += 3
-    settle(1, other)
-    tick(ffn0)
-    ffn0 += 1
-
-    ucols = 256
-    unit_chunks = units // 2 // ucols
+    for r, copy in enumerate(hid_copies(blocks - 1, 0)):
+        tall = slice(r * quarter, (r + 1) * quarter)
+        copy.wait_recv()
+        if r == 1:
+            tick(ffn0)
+            ffn0 += 1
+        mixed(1, (), (blocks - 1,), False, tall=tall, ocols=model // 2)
+        if r == 0:
+            tick(ffn0)
+            ffn0 += 1
+        settle(1, other, tall)
+
+    def activate(g, h, c, product):
+        lanes = pl.ds(pl.multiple_of((g - 1) * cut + c * ucols, ucols), ucols)
+        hidden = jax.nn.silu(product[:, :ucols]) * product[:, ucols:]
+        hf[h, :, lanes] = hidden.astype(jnp.bfloat16)
 
     def expand(g, h, c):
-        x = xm[h]
-        lanes = pl.ds(pl.multiple_of(c * ucols, ucols), ucols)
-        gate = jnp.dot(x, full[g, :, lanes], preferred_element_type=jnp.float32)
-        lanes = pl.ds(pl.multiple_of(units // 2 + c * ucols, ucols), ucols)
-        up = jnp.dot(x, full[g, :, lanes], preferred_element_type=jnp.float32)
-        lanes = pl.ds(pl.multiple_of((g - 1) * (units // 2) + c * ucols, ucols), ucols)
-        hf[h, :, lanes] = (jax.nn.silu(gate) * up).astype(jnp.bfloat16)
+        lanes = pl.ds(pl.multiple_of(2 * c * ucols, 2 * ucols), 2 * ucols)
+        activate(g, h, c, jnp.dot(xm[h], full[g, :, lanes], preferred_element_type=jnp.float32))
 
     first_done = 2 * per_stage + head
     second_done = 3 * per_stage + head
@@ -708,49 +739,61 @@
     def _(slot):
         near_wait(1, slot)
 
+    def feature_chip(slot):
+        d = (slot + 1) // 2
+        return chip_at(jnp.where(slot % 2 == 1, -d, d))
+
+    def expand_part(g, h, c, slots, fresh, last):
+        rows = [pl.ds(pl.multiple_of(feature_chip(slot) * span, span), span) for slot in slots]
+        x = jnp.concatenate([xm[h, :, at] for at in rows], axis=1)
+        lanes = pl.ds(pl.multiple_of(2 * c * ucols, 2 * ucols), 2 * ucols)
+        w = jnp.concatenate([full[g, at, lanes] for at in rows], axis=0)
+        term = jnp.dot(x, w, preferred_element_type=jnp.float32)
+        if not fresh:
+            term = total[:, lanes] + term
+        if last:
+            activate(g, h, c, term)
+        else:
+            total[:, lanes] = term
+
+    ffn2 = ffn1 + 2
+    before = second_done - PIECES // 2
+    parts_b = (tuple(range(chips - 3)), (chips - 3, chips - 2), (chips - 1,))
+
     @pl.loop(0, unit_chunks)
     def _(c):
         expand(1, 1, c)
 
+        @pl.when(c < 2)
+        def _():
+            tick(ffn1 + c)
+
+    for slot in parts_b[0]:
+        near_wait(2, slot)
+
+    @pl.loop(0, unit_chunks)
+    def _(c):
+        expand_part(2, 1, c, parts_b[0], True, False)
+
+        @pl.when(c == 0)
+        def _():
+            tick(ffn2)
+
         @pl.when(c == 1)
         def _():
-            tick(ffn1)
-
-    def feature_chip(slot):
-        d = (slot + 1) // 2
-        return chip_at(jnp.where(slot % 2 == 1, -d, d))
-
-    def expand_part(g, h, c, slots, fresh, last):
-        rows = [pl.ds(pl.multiple_of(feature_chip(slot) * span, span), span) for slot in slots]
-        x = jnp.concatenate([xm[h, :, at] for at in rows], axis=1)
-        summed = []
-        for side in range(2):
-            lanes = pl.ds(pl.multiple_of(side * cut + c * ucols, ucols), ucols)
-            w = jnp.concatenate([full[g, at, lanes] for at in rows], axis=0)
-            term = jnp.dot(x, w, preferred_element_type=jnp.float32)
-            if not fresh:
-                term = total[:, lanes] + term
-            if last:
-                summed.append(term)
-            else:
-                total[:, lanes] = term
-        if last:
-            lanes = pl.ds(pl.multiple_of((g - 1) * cut + c * ucols, ucols), ucols)
-            hf[h, :, lanes] = (jax.nn.silu(summed[0]) * summed[1]).astype(jnp.bfloat16)
-
-    ffn2 = ffn1 + 1
-    before = second_done - PIECES // 2
-    ticks(min(ffn2, before), before)
-    parts_b = (tuple(range(chips - 3)), (chips - 3, chips - 2), (chips - 1,))
-    for n, slots in enumerate(parts_b):
-        if n == len(parts_b) - 1:
-            ticks(before, second_done)
-        for slot in slots:
+            ticks(ffn2 + 1, before)
+
+        @pl.when(c == 2)
+        def _():
+            tick(before)
+
+    for n in (1, 2):
+        if n == 2:
+            tick(before + 1)
+        for slot in parts_b[n]:
             near_wait(2, slot)
-
-        @pl.loop(0, unit_chunks)
-        def _(c):
-            expand_part(2, 1, c, slots, n == 0, n == len(parts_b) - 1)
+        for c in range(unit_chunks):
+            expand_part(2, 1, c, parts_b[n], False, n == 2)
 
     def partial_of(h, chip):
         weight = full[stages - 1, pl.ds(pl.multiple_of(chip * span, span), span), :]
@@ -775,7 +818,8 @@
 
     send_back(0)
     for b in all_blocks:
-        hid_copy(b, 1).wait_recv()
+        for copy in hid_copies(b, 1):
+            copy.wait_recv()
     mixed(0, all_blocks, (), True, distance1, PIECES)
     send_pair(1)
     mixed(0, (), all_blocks, False, distance1 + PIECES, 2)
@@ -847,7 +891,7 @@
     ref = far_out.at[pl.ds(0, chips * depth), :]
     remote(ref, ref, cross_send.at[0], cross_recv.at[0], across).wait_send()
     remote(ref, ref, share_send.at[0], share_recv.at[0], partner).wait_send()
-    remote(hid, got, hid_send.at[0], hid_recv.at[0, 0], across).wait_send()
+    remote(hid, got, hid_send.at[0], hid_recv.at[0, 0, 0], across).wait_send()
     remote(part, back, back_send.at[0], back_recv.at[0], across).wait_send()
     pltpu.make_async_copy(mine, out_ref, out_sem.at[0]).wait()
 
@@ -917,7 +961,7 @@
             dma((stages, reach, PIECES)),
             dma((stages,)),
             dma((stages, chips)),
-            dma((8,)),
+            dma((4 + 4 * (units // 2 // 256),)),
             dma((10,)),
             dma((1,)),
             dma((1,)),
@@ -928,7 +972,7 @@
             dma((1,)),
             dma((1,)),
             dma((1,)),
-            dma((blocks, 2)),
+            dma((blocks, 2, 2)),
             dma((1,)),
             dma((chips,)),
         ],

time: 154 us -> 153 us (level)
  Pallas kernels: 151 us -> 149 us
where the time goes in v6:
time: 153 us
  Pallas kernels  149 us (97%)
  local copies, waits for them, and re-layouts  3.16 us (2%)
    pallas_call x1, Pallas kernels, paired_device(): pl.pallas_call(functools.partial(layer_kernel, size), out_shape=jax.Shape...  149 us
    unnamed x1, local copies, waits for them, and re-layouts  3.16 us

profile of v6, /device:TPU:0, one launch (start us, length us, event | category | flops | bytes accessed | tf_op | source)
XLA Modules:
  0.0 152.6 jit_solution(10790083173229099491)
XLA Ops:
  0.0 149.4 %shard_map.145 = bf16[512,2048]{1,0:T(8,128)(2,1)} custom-call(bf16[512,2048]{1,0:T(8,128)(2,1)} %tokens_ref.1, bf16[128,512]{1,0:T(8,128)(2,1)} %branch_ref.1, bf16[128,512]{1,0:T(8,128)(2,1)} %gelu_ref.1, bf16[128,512]{1,0:T(8,128)(2,1)} %outw_ref.1, bf16[128,1536]{1,0:T(8,128)(2,1)} %gate_ref.1, bf16[128,1536]{1,0:T(8,128)(2,1)} %up_ref.1, ...), custom_call_target="tpu_custom_call" | custom-call | flops 17179869184 | bytes 67108864 | tf_op jit(solution)/shard_map/pallas_call | solution.py:933
  149.4 3.2 %copy.17 = bf16[512,2048]{1,0:T(8,128)(2,1)} copy(bf16[512,2048]{1,0:T(8,128)(2,1)} %shard_map.145) | data formatting | bytes 4194304

commit v7 on v6

--- a/solution.py
+++ b/solution.py
@@ -326,28 +326,27 @@
     cut = units // 2
     own_rows = pl.ds(pl.multiple_of(me * depth, depth), depth)
 
-    def own_part(g, source, lanes, at, sem):
+    def own_part(g, source, lanes, at):
         place_at = full.at[g, own_rows, pl.ds(at, lanes.size)]
-        return pltpu.make_async_copy(source.at[:, lanes], place_at, own_sem.at[sem])
+        return pltpu.make_async_copy(source.at[:, lanes], place_at, own_sem.at[g])
 
     every = pl.ds(0, channels)
     ucols = 256
     unit_chunks = cut // ucols
-    unit_pairs = 2 * unit_chunks
-
-    def unit_parts(first, sem):
+
+    def unit_parts(first):
         found = []
         for c in range(unit_chunks):
             for side, source in enumerate((gate_ref, up_ref)):
                 at = (2 * c + side) * ucols
-                found.append((source, pl.ds(first + c * ucols, ucols), at, sem + len(found)))
+                found.append((source, pl.ds(first + c * ucols, ucols), at))
         return found
 
     own_copies = [
-        [own_part(0, source, every, i * channels, i) for i, source in enumerate((branch_ref, gelu_ref, outw_ref))],
-        [own_part(1, *pair) for pair in unit_parts(0, 3)],
-        [own_part(2, *pair) for pair in unit_parts(cut, 3 + unit_pairs)],
-        [own_part(3, down_ref, pl.ds(0, units), 0, 3 + 2 * unit_pairs)],
+        [own_part(0, source, every, i * channels) for i, source in enumerate((branch_ref, gelu_ref, outw_ref))],
+        [own_part(1, *pair) for pair in unit_parts(0)],
+        [own_part(2, *pair) for pair in unit_parts(cut)],
+        [own_part(3, down_ref, pl.ds(0, units), 0)],
     ]
     for copy in own_copies[0]:
         copy.start()
@@ -444,14 +443,16 @@
     for i in range(TOKEN_PIECES):
         rows = pl.ds(i * token_rows, token_rows)
         remote(tokens_ref.at[rows, :], other.at[rows, :], tok_send.at[0], tok_recv.at[i], across).start()
-    for copy in own_copies[0]:
-        copy.wait()
+    def own_wait(g):
+        rows = shard_rows(g, me // 2, core)
+        pltpu.make_async_copy(rows, rows, own_sem.at[g]).wait()
+
+    own_wait(0)
     ticks(0, PIECES)
     for copy in (*small, mine_copy):
         copy.wait()
-    for copies in own_copies[1:]:
-        for copy in copies:
-            copy.wait()
+    for g in range(1, stages):
+        own_wait(g)
     slow = coef_ref[...]
     coef_ref[...] = -8.0 * (jnp.maximum(-slow, 0.0) + jnp.log1p(jnp.exp(-jnp.abs(slow))))
 
@@ -805,11 +806,26 @@
 
     distance1 = (stages - 1) * per_stage + head
 
+    def last_copy(i):
+        chip = feature_chip(chips - 1)
+        rows = pl.ds(pl.multiple_of(i * chunk, chunk), chunk)
+        return remote(
+            part.at[chip, rows, :],
+            back.at[chip, rows, :],
+            back_send.at[0],
+            back_recv.at[chips - 1 + i],
+            across,
+        )
+
     def send_back(slot):
         near_wait(stages - 1, slot)
         chip = feature_chip(slot)
         part[chip] = partial_of(1, chip).astype(jnp.bfloat16)
-        back_copy(slot).start()
+        if isinstance(slot, int) and slot == chips - 1:
+            for i in range(half // chunk):
+                last_copy(i).start()
+        else:
+            back_copy(slot).start()
 
     def send_pair(d):
         @pl.loop(2 * d - 1, 2 * d + 1)
@@ -853,25 +869,30 @@
 
     squares[...] = jnp.zeros_like(squares)
 
-    @pl.loop(0, chips)
+    def add_back(slot, i):
+        chip = feature_chip(slot)
+        lanes = pl.ds(pl.multiple_of(chip * span, span), span)
+        rows = pl.ds(pl.multiple_of(i * chunk, chunk), chunk)
+        summed = total[rows, lanes] + back[chip, rows, :].astype(jnp.float32)
+        total[rows, lanes] = summed
+        square = summed * summed
+        folded = square[:, :128]
+        for at in range(128, span, 128):
+            folded = folded + square[:, at : at + 128]
+        squares[rows, :] += folded
+
+    @pl.loop(0, chips - 1)
     def _(slot):
         back_copy(slot).wait_recv()
-        chip = feature_chip(slot)
-        lanes = pl.ds(pl.multiple_of(chip * span, span), span)
 
         @pl.loop(0, half // chunk)
         def _(i):
-            rows = pl.ds(pl.multiple_of(i * chunk, chunk), chunk)
-            summed = total[rows, lanes] + back[chip, rows, :].astype(jnp.float32)
-            total[rows, lanes] = summed
-            square = summed * summed
-            folded = square[:, :128]
-            for at in range(128, span, 128):
-                folded = folded + square[:, at : at + 128]
-            squares[rows, :] += folded
+            add_back(slot, i)
 
     @pl.loop(0, half // chunk)
     def _(i):
+        last_copy(i).wait_recv()
+        add_back(chips - 1, i)
         rows = pl.ds(pl.multiple_of(i * chunk, chunk), chunk)
         mean = jnp.sum(squares[rows, :], axis=-1, keepdims=True) * (1.0 / model)
         scaled = total[rows, :] * lax.rsqrt(mean + EPS) * gains[3]
@@ -961,7 +982,7 @@
             dma((stages, reach, PIECES)),
             dma((stages,)),
             dma((stages, chips)),
-            dma((4 + 4 * (units // 2 // 256),)),
+            dma((stages,)),
             dma((10,)),
             dma((1,)),
             dma((1,)),
@@ -974,7 +995,7 @@
             dma((1,)),
             dma((blocks, 2, 2)),
             dma((1,)),
-            dma((chips,)),
+            dma((chips - 1 + half // 128,)),
         ],
         compiler_params=pltpu.CompilerParams(
             collective_id=0, has_side_effects=True, vmem_limit_bytes=MOST_VMEM

time: 153 us -> 152 us (level)
  no operation moved by 1% of the time
where the time goes in v7:
time: 152 us
  Pallas kernels  148 us (97%)
  local copies, waits for them, and re-layouts  3.16 us (2%)
    pallas_call x1, Pallas kernels, paired_device(): pl.pallas_call(functools.partial(layer_kernel, size), out_shape=jax.Shape...  148 us
    unnamed x1, local copies, waits for them, and re-layouts  3.16 us

profile of v7, /device:TPU:0, one launch (start us, length us, event | category | flops | bytes accessed | tf_op | source)
XLA Modules:
  0.0 151.6 jit_solution(471560669542177111)
XLA Ops:
  0.0 148.5 %shard_map.145 = bf16[512,2048]{1,0:T(8,128)(2,1)} custom-call(bf16[512,2048]{1,0:T(8,128)(2,1)} %tokens_ref.1, bf16[128,512]{1,0:T(8,128)(2,1)} %branch_ref.1, bf16[128,512]{1,0:T(8,128)(2,1)} %gelu_ref.1, bf16[128,512]{1,0:T(8,128)(2,1)} %outw_ref.1, bf16[128,1536]{1,0:T(8,128)(2,1)} %gate_ref.1, bf16[128,1536]{1,0:T(8,128)(2,1)} %up_ref.1, ...), custom_call_target="tpu_custom_call" | custom-call | flops 17179869184 | bytes 67108864 | tf_op jit(solution)/shard_map/pallas_call | solution.py:954
  148.5 3.2 %copy.17 = bf16[512,2048]{1,0:T(8,128)(2,1)} copy(bf16[512,2048]{1,0:T(8,128)(2,1)} %shard_map.145) | data formatting | bytes 4194304

commit v8 on v7

--- a/solution.py
+++ b/solution.py
@@ -917,6 +917,44 @@
     pltpu.make_async_copy(mine, out_ref, out_sem.at[0]).wait()
 
 
+def store_kernel(source_ref, out_ref, held, in_sem, out_sem):
+    count = held.shape[0]
+    rows = held.shape[1]
+    pieces = [pl.ds(i * rows, rows) for i in range(count)]
+    loads = [
+        pltpu.make_async_copy(source_ref.at[at, :], held.at[i], in_sem.at[i])
+        for i, at in enumerate(pieces)
+    ]
+    stores = [
+        pltpu.make_async_copy(held.at[i], out_ref.at[at, :], out_sem.at[i])
+        for i, at in enumerate(pieces)
+    ]
+    for load in loads:
+        load.start()
+    for load, store in zip(loads, stores):
+        load.wait()
+        store.start()
+    for store in stores:
+        store.wait()
+
+
+def store(values):
+    rows, model = values.shape
+    count = 8
+    hbm = pl.BlockSpec(memory_space=pl.ANY)
+    return pl.pallas_call(
+        store_kernel,
+        out_shape=jax.ShapeDtypeStruct(values.shape, values.dtype),
+        in_specs=[hbm],
+        out_specs=hbm,
+        scratch_shapes=[
+            pltpu.VMEM((count, rows // count, model), values.dtype),
+            pltpu.SemaphoreType.DMA((count,)),
+            pltpu.SemaphoreType.DMA((count,)),
+        ],
+    )(values)
+
+
 def paired_device(
     tokens,
     pre_mix_gain,
@@ -951,7 +989,7 @@
     reach = chips // 2
     hbm = pl.BlockSpec(memory_space=pl.ANY)
     gains = (pre_mix_gain, post_mix_gain, pre_ffn_gain, post_ffn_gain)
-    return pl.pallas_call(
+    result = pl.pallas_call(
         functools.partial(layer_kernel, size),
         out_shape=jax.ShapeDtypeStruct((half, model), jnp.bfloat16),
         in_specs=[hbm] * 15,
@@ -1017,6 +1055,7 @@
         w_inp,
         decay,
     )
+    return store(result)
 
 
 def wide_device(

time: 152 us -> 151 us (level)
  local copies, waits for them, and re-layouts: 3.16 us -> 0 us
  Pallas kernels: 148 us -> 151 us
    unnamed x1 -> x0, local copies, waits for them, and re-layouts: 3.16 us -> none
    pallas_call x0 -> x1, Pallas kernels: none -> 2.39 us  [store(): pl.pallas_call(store_kernel, out_shape=jax.ShapeDtypeStruct(values.shape,...]
where the time goes in v8:
time: 151 us
  Pallas kernels  151 us (100%)
    pallas_call x1, Pallas kernels, paired_device(): pl.pallas_call(functools.partial(layer_kernel, size), out_shape=jax.Shape...  148 us

profile of v8, /device:TPU:0, one launch (start us, length us, event | category | flops | bytes accessed | tf_op | source)
XLA Modules:
  0.0 151.0 jit_solution(13764823637972522083)
XLA Ops:
  0.0 148.5 %shard_map.145.source_ref = bf16[512,2048]{1,0:T(8,128)(2,1)} custom-call(bf16[512,2048]{1,0:T(8,128)(2,1)} %tokens_ref.1, bf16[128,512]{1,0:T(8,128)(2,1)} %branch_ref.1, bf16[128,512]{1,0:T(8,128)(2,1)} %gelu_ref.1, bf16[128,512]{1,0:T(8,128)(2,1)} %outw_ref.1, bf16[128,1536]{1,0:T(8,128)(2,1)} %gate_ref.1, bf16[128,1536]{1,0:T(8,128)(2,1)} %up_ref.1, ...), custom_call_target="tpu_custom_call" | custom-call | flops 17179869184 | bytes 67108864 | tf_op jit(solution)/shard_map/pallas_call | solution.py:992
  148.5 2.4 %shard_map.146 = bf16[512,2048]{1,0:T(8,128)(2,1)} custom-call(bf16[512,2048]{1,0:T(8,128)(2,1)} %shard_map.145.source_ref), custom_call_target="tpu_custom_call" | custom-call | tf_op jit(solution)/shard_map/pallas_call | solution.py:945
